TPU v7x, 32 devices: a whole 2x2x4 slice. The times are simulated.
32 devices in a mesh: ep: 8 (over z, x), tp: 4 (over y, core).
Axes of the slice: x: 2, y: 2, z: 4, core: 2. Of those that a mesh axis runs over, the one named last changes fastest.
Arguments:
- tokens: bfloat16 [128, 2048], P('ep'), may hold values from -6 to 6
- norm1_gain: float32 [2048], replicated, may hold values from 0.1 to 1.9
- query_weight: bfloat16 [2048, 512], P(None, 'tp'), may hold values from -0.125 to 0.125
- key_weight: bfloat16 [2048, 256], P(None, 'tp'), may hold values from -0.125 to 0.125
- value_weight: bfloat16 [2048, 256], P(None, 'tp'), may hold values from -0.125 to 0.125
- forget_weight: bfloat16 [2048, 8], P(None, 'tp'), may hold values from -0.125 to 0.125
- forget_bias: float32 [8], P('tp'), may hold values from 0.5 to 4
- out_weight: bfloat16 [512, 2048], P('tp'), may hold values from -0.25 to 0.25
- kv_cache: bfloat16 [128, 1024, 4, 128], P('ep', None, 'tp'), may hold values from -6 to 6
- log_gates: float32 [128, 8, 1024], P('ep', 'tp'), may hold values from -1024 to 0, as said below
- lengths: int32 [128], P('ep'), may hold values from 64 to 1024
- norm2_gain: float32 [2048], replicated, may hold values from 0.1 to 1.9
- routing: int32 [128, 4], P('ep'), may hold values from 0 to 7, all different within a row; in each aligned block of 16 rows (0 to 15, 16 to 31, ...) at most 16 rows name the same one
- route_weight: float32 [128, 4], P('ep'), may hold values from 0.1 to 0.6
- expert_gate: bfloat16 [8, 2048, 2048], P('ep', None, 'tp'), may hold values from -0.25 to 0.25
- expert_up: bfloat16 [8, 2048, 2048], P('ep', None, 'tp'), may hold values from -0.25 to 0.25
- expert_down: bfloat16 [8, 2048, 2048], P('ep', 'tp'), may hold values from -0.0625 to 0.0625
- dense_gate: bfloat16 [2048, 4096], P(None, 'ep'), may hold values from -0.25 to 0.25
- dense_up: bfloat16 [2048, 4096], P(None, 'ep'), may hold values from -0.25 to 0.25
- dense_down: bfloat16 [4096, 2048], P('ep'), may hold values from -0.09375 to 0.09375
- dense_mix: float32 [2048], replicated, may hold values from -0.125 to 0.125
Outputs:
- layer_out: bfloat16 [128, 2048], P(('ep', 'tp'))
Inputs may be any that keep to these rules, and one draw needn't show every extreme that they name: `log_gates`: Non-increasing along the positions. `routing`: each row names 4 different experts. Among the rows of one index of ep (aligned blocks of 16 rows) no expert is named by more than 16 rows, and in every draw some expert is named by exactly 16 rows of some block.
All inputs are finite; a program needn't handle non-finite values.
Results may differ from a plain program's by a relative error of at most 0.011.
Values may be sent and summed in bfloat16 or wider, within the bound.
No kernel may reach another device: no remote copies, remote signals or barrier semaphores. Data moves between devices by JAX's collectives and lax.ppermute only.
A program may use at most 128 MiB of HBM per device.

v0:
```python
import jax
import jax.numpy as jnp
from jax import lax
from jax.sharding import PartitionSpec as P

EPS = 1e-05
LIMIT = 7.0
ALPHA = 1.702


def clamped_unit(gate_pre, up_pre):
    capped = jnp.minimum(gate_pre, LIMIT)
    return capped * jax.nn.sigmoid(ALPHA * capped) * (jnp.clip(up_pre, -LIMIT, LIMIT) + 1.0)


def rms_scaled(values, gain_vec):
    return values * lax.rsqrt(jnp.mean(values * values, axis=-1, keepdims=True) + EPS) * gain_vec


def slot_tables(routes, experts, capacity):
    flat_ids = routes.reshape(-1)
    onehot = (flat_ids[:, None] == jnp.arange(experts, dtype=jnp.int32)[None, :]).astype(jnp.int32)
    earlier = jnp.cumsum(onehot, axis=0, dtype=jnp.int32) - onehot
    slot_ids = jnp.sum(earlier * onehot, axis=1, dtype=jnp.int32)
    matches = onehot[:, :, None] * (
        slot_ids[:, None, None] == jnp.arange(capacity, dtype=jnp.int32)[None, None, :]
    ).astype(jnp.int32)
    owners = jnp.arange(flat_ids.shape[0], dtype=jnp.int32) // routes.shape[1]
    source = jnp.sum(matches * owners[:, None, None], axis=0, dtype=jnp.int32)
    return (slot_ids, source)


def on_device(
    tokens,
    norm1_gain,
    query_weight,
    key_weight,
    value_weight,
    forget_weight,
    forget_bias,
    out_weight,
    kv_cache,
    log_gates,
    lengths,
    norm2_gain,
    routing,
    route_weight,
    expert_gate,
    expert_up,
    expert_down,
    dense_gate,
    dense_up,
    dense_down,
    dense_mix,
):
    seq_count, model_width = tokens.shape
    tp_count = lax.axis_size("tp")
    ep_count = lax.axis_size("ep")
    own_rows = seq_count // tp_count
    row_start = lax.axis_index("tp") * own_rows
    local_heads = forget_bias.shape[0]
    kv_local = kv_cache.shape[2]
    head_dim = kv_cache.shape[3] // 2
    per_kv = local_heads // kv_local
    cache_len = kv_cache.shape[1]
    score_scale = head_dim ** (-0.5)
    normed = rms_scaled(tokens.astype(jnp.float32), norm1_gain).astype(jnp.bfloat16)
    queries = jnp.dot(normed, query_weight, preferred_element_type=jnp.float32).astype(jnp.bfloat16)
    queries = queries.reshape(seq_count, kv_local, per_kv, head_dim)
    key_new = jnp.dot(normed, key_weight, preferred_element_type=jnp.float32).astype(jnp.bfloat16)
    key_new = key_new.reshape(seq_count, kv_local, head_dim)
    value_new = jnp.dot(normed, value_weight, preferred_element_type=jnp.float32).astype(
        jnp.bfloat16
    )
    value_new = value_new.reshape(seq_count, kv_local, head_dim)
    gate_new = jax.nn.log_sigmoid(
        jnp.dot(normed, forget_weight, preferred_element_type=jnp.float32) + forget_bias
    )
    scores = (
        jnp.einsum(
            "skgd,slkd->skgl", queries, kv_cache[..., :head_dim], preferred_element_type=jnp.float32
        )
        * score_scale
    )
    last_index = jnp.broadcast_to((lengths - 1)[:, None, None], (seq_count, local_heads, 1))
    last_gate = jnp.take_along_axis(log_gates, last_index, axis=2)
    gate_bias = (last_gate - log_gates + gate_new[:, :, None]).reshape(
        seq_count, kv_local, per_kv, cache_len
    )
    live_mask = (jnp.arange(cache_len, dtype=jnp.int32)[None, :] < lengths[:, None])[
        :, None, None, :
    ]
    cached = jnp.where(live_mask, jnp.exp(scores + gate_bias), 0.0)
    own_exp = jnp.exp(
        jnp.einsum("skgd,skd->skg", queries, key_new, preferred_element_type=jnp.float32)
        * score_scale
    )
    denominator = jnp.sum(cached, axis=-1) + own_exp
    weight_cache = (cached / denominator[..., None]).astype(jnp.bfloat16)
    weight_own = (own_exp / denominator).astype(jnp.bfloat16)
    attended = jnp.einsum(
        "skgl,slkd->skgd",
        weight_cache,
        kv_cache[..., head_dim:],
        preferred_element_type=jnp.float32,
    )
    attended = (
        attended
        + weight_own.astype(jnp.float32)[..., None] * value_new.astype(jnp.float32)[:, :, None, :]
    )
    attended = attended.astype(jnp.bfloat16).reshape(seq_count, local_heads * head_dim)
    partial_out = jnp.dot(attended, out_weight, preferred_element_type=jnp.float32)
    attn_out = lax.psum(partial_out, "tp").astype(jnp.bfloat16)
    residual = tokens.astype(jnp.float32) + attn_out.astype(jnp.float32)
    hidden_in = rms_scaled(residual, norm2_gain).astype(jnp.bfloat16)
    own_hidden = lax.dynamic_slice_in_dim(hidden_in, row_start, own_rows, 0)
    own_residual = lax.dynamic_slice_in_dim(residual, row_start, own_rows, 0)
    row_piece = lax.all_gather(own_hidden, "ep", axis=0, tiled=True)
    gate_pre = jnp.dot(row_piece, dense_gate, preferred_element_type=jnp.float32)
    up_pre = jnp.dot(row_piece, dense_up, preferred_element_type=jnp.float32)
    dense_act = clamped_unit(gate_pre, up_pre).astype(jnp.bfloat16)
    dense_val = lax.psum_scatter(
        jnp.dot(dense_act, dense_down, preferred_element_type=jnp.float32),
        "ep",
        scatter_dimension=0,
        tiled=True,
    )
    local_experts = expert_gate.shape[0]
    experts = local_experts * ep_count
    top_count = routing.shape[1]
    capacity = min(seq_count, seq_count * top_count * 3 // experts)
    slot_ids, source = slot_tables(routing, experts, capacity)
    dispatch = hidden_in[source.reshape(-1)].reshape(experts, capacity, model_width)
    received = lax.all_to_all(dispatch, "ep", split_axis=0, concat_axis=0, tiled=True)
    item_count = received.shape[1]
    grouped = received.reshape(ep_count, local_experts, item_count, model_width)
    gate_pre = jnp.einsum(
        "sjnd,jdf->sjnf", grouped, expert_gate, preferred_element_type=jnp.float32
    )
    up_pre = jnp.einsum("sjnd,jdf->sjnf", grouped, expert_up, preferred_element_type=jnp.float32)
    activation = clamped_unit(gate_pre, up_pre).astype(jnp.bfloat16)
    partial_units = jnp.einsum(
        "sjnf,jfd->sjnd", activation, expert_down, preferred_element_type=jnp.float32
    )
    partial_units = partial_units.reshape(ep_count * local_experts, item_count, model_width)
    slot_index = routing * capacity + slot_ids.reshape(seq_count, top_count)
    shares = lax.psum_scatter(
        partial_units.astype(jnp.bfloat16), "tp", scatter_dimension=2, tiled=True
    )
    returned = lax.all_to_all(shares, "ep", split_axis=0, concat_axis=0, tiled=True)
    share_width = returned.shape[2]
    picked = returned.reshape(experts * capacity, share_width)[slot_index.reshape(-1)]
    picked = picked.reshape(seq_count, top_count, share_width)
    moe_cols = jnp.sum(route_weight[..., None] * picked.astype(jnp.float32), axis=1)
    moe_val = lax.all_to_all(
        moe_cols.astype(jnp.bfloat16), "tp", split_axis=0, concat_axis=1, tiled=True
    ).astype(moe_cols.dtype)
    mix_gate = jax.nn.sigmoid(
        jnp.dot(own_hidden.astype(jnp.float32), dense_mix, precision=lax.Precision.HIGHEST)
    )
    return (own_residual + moe_val + mix_gate[:, None] * dense_val).astype(jnp.bfloat16)


def solution(mesh):
    return jax.shard_map(
        on_device,
        mesh=mesh,
        in_specs=(
            P("ep", None),
            P(),
            P(None, "tp"),
            P(None, "tp"),
            P(None, "tp"),
            P(None, "tp"),
            P("tp"),
            P("tp", None),
            P("ep", None, "tp", None),
            P("ep", "tp", None),
            P("ep"),
            P(),
            P("ep", None),
            P("ep", None),
            P("ep", None, "tp"),
            P("ep", None, "tp"),
            P("ep", "tp", None),
            P(None, "ep"),
            P(None, "ep"),
            P("ep", None),
            P(),
        ),
        out_specs=P(("ep", "tp"), None),
        check_vma=False,
    )
```

profile of v0, /device:TPU:0, one launch (start us, length us, event | category | flops | bytes accessed | tf_op | source)
XLA Modules:
  0.0 175.3 jit_solution(10059559181539150195)
XLA Ops:
  7.4 0.8 broadcast_add_fusion
  8.2 0.7 broadcast_compare_fusion
  8.8 0.7 iota_compare_fusion
  9.6 0.1 copy.44
  9.7 0.1 reshape.457
  9.9 1.8 %gather_fusion.2 = f32[32]{0:T(128)S(1)} fusion(f32[16,2,1024]{2,1,0:T(2,128)} %param.30, s32[32]{0:T(128)S(1)} %reshape.457), kind=kCustom, calls=%fused_computation.2 | custom fusion | bytes 640 | tf_op jit(solution)/shard_map/jit(take_along_axis)/gather | solution.py:86
  11.7 0.1 gather.13
  11.9 0.1 fusion.72
  12.1 0.2 convolution_convert_fusion.3
  12.3 0.1 reshape.424
  12.4 0.2 fusion.102
  12.6 0.1 copy.45
  12.7 0.2 fusion.55
  12.9 0.2 fusion.54
  13.2 0.1 fusion.98
  13.3 3.6 %fusion.123 = (f32[16,2]{1,0:T(8,128)S(1)}, f32[16,2,1024]{2,1,0:T(2,128)S(1)}) fusion(f32[16,2]{1,0:T(8,128)S(1)} %copy.45, f32[16,2,1024]{2,1,0:T(2,128)S(1)} %copy-done.1, f32[16,2]{1,0:T(8,128)S(1)} %fusion.97, bf16[16,2,64]{2,1,0:T(2,128)(2,1)S(1)} %reshape.424, bf16[16,1024,1,128]{3,1,2,0:T(8,128)(2,1)} %param.29, ...), kind=kOutput, calls=%fused_computation.138 | convolution fusion | flops 4390880 | bytes 4477312 | tf_op jit(solution)/shard_map/skgd,slkd->skgl/dot_general | solution.py:80
  17.0 1.4 fusion.51
  18.4 0.1 reshape.427
  18.5 0.2 fusion.124
  18.7 14.5 %all-reduce.5 = bf16[16,2048]{1,0:T(8,128)(2,1)S(1)} all-reduce(f32[16,2048]{1,0:T(8,128)S(1)} %fusion.124), channel_id=1, replica_groups=mesh['ep'=8,'tp'=4] {'tp'}, use_global_device_ids=true, to_apply=%region_2.3 | all-reduce | flops 32768 | bytes 196608 | tf_op jit(solution)/shard_map/psum | solution.py:113
  33.2 0.1 multiply_reduce_fusion.1
  33.3 0.1 copy.48
  33.4 0.1 eq.37
  33.7 0.1 reduce_window_sum.11
  33.8 0.2 select_reduce_fusion
  34.0 0.2 multiply_reduce_fusion.2
  34.3 0.1 multiply_convert_fusion
  34.4 0.9 gather_fusion
  35.3 19.1 %all_to_all.20 = bf16[8,16,2048]{2,1,0:T(8,128)(2,1)S(1)} all-to-all(bf16[8,16,2048]{2,1,0:T(8,128)(2,1)S(1)} %bitcast.124), channel_id=1, replica_groups=mesh['ep'=8,'tp'=4] {'ep'}, dimensions={0} | all-to-all | bytes 1048576 | tf_op jit(solution)/shard_map/all_to_all | solution.py:134
  54.4 2.0 %fusion.14 = f32[8,1,16,512]{3,2,0,1:T(8,128)S(1)} fusion(bf16[8,16,2048]{2,1,0:T(8,128)(2,1)S(1)} %all_to_all.20, bf16[1,2048,512]{2,1,0:T(8,128)(2,1)} %param.35), kind=kOutput, calls=%fused_computation.16 | convolution fusion | flops 268500992 | bytes 2883584 | tf_op jit(solution)/shard_map/sjnd,jdf->sjnf/dot_general | solution.py:137
  56.4 3.2 %convolution_convert_fusion = bf16[8,16,2048]{2,1,0:T(8,128)(2,1)} fusion(bf16[1,512,2048]{2,1,0:T(8,128)(2,1)S(1)} %copy-done, bf16[8,16,2048]{2,1,0:T(8,128)(2,1)S(1)} %all_to_all.20, bf16[1,2048,512]{2,1,0:T(8,128)(2,1)} %param.36, f32[8,1,16,512]{3,2,0,1:T(8,128)S(1)} %fusion.14), kind=kOutput, calls=%fused_computation.9 | convolution fusion | flops 537722880 | bytes 5505024 | tf_op jit(solution)/shard_map/sjnf,jfd->sjnd/dot_general | solution.py:142
  59.8 30.5 %all-gather = bf16[8,4,2048]{2,1,0:T(4,128)(2,1)S(1)} all-gather(bf16[1,4,2048]{2,1,0:T(4,128)(2,1)S(1)} %dynamic-slice_bitcast_fusion), channel_id=1, replica_groups=mesh['ep'=8,'tp'=4] {'ep'}, dimensions={0}, use_global_device_ids=true | all-gather | bytes 147456 | tf_op jit(solution)/shard_map/all_gather | solution.py:118
  90.3 2.0 %convolution_minimum_fusion = f32[32,512]{1,0:T(8,128)S(1)} fusion(bf16[32,2048]{1,0:T(8,128)(2,1)S(1)} %reshape.466, bf16[2048,512]{1,0:T(8,128)(2,1)} %param.38), kind=kOutput, calls=%fused_computation.29 | convolution fusion | flops 67125248 | bytes 2293760 | tf_op jit(solution)/shard_map/dot_general | solution.py:119
  92.4 3.9 %fusion.47 = f32[32,2048]{1,0:T(8,128)} fusion(bf16[512,2048]{1,0:T(8,128)(2,1)} %param.40, bf16[32,2048]{1,0:T(8,128)(2,1)S(1)} %reshape.466, bf16[2048,512]{1,0:T(8,128)(2,1)} %param.39, f32[32,512]{1,0:T(8,128)S(1)} %convolution_minimum_fusion), kind=kOutput, calls=%fused_computation.31 | convolution fusion | flops 134365184 | bytes 4653056 | tf_op jit(solution)/shard_map/dot_general | solution.py:123
  96.3 0.1 reshape.435
  96.4 0.1 reshape.436
  96.5 0.1 copy.47
  96.6 3.6 %all-to-all-start.1 = ((bf16[8,16,512]{2,1,0:T(8,128)(2,1)}), bf16[8,16,512]{2,1,0:T(8,128)(2,1)S(1)}, u32[]{:S(2)}, u32[]{:S(2)}) async-start(bf16[8,16,512]{2,1,0:T(8,128)(2,1)} %reduce-scatter.2.cloned.1.call-done), calls=%async_computation.2 | async-start | bytes 262144 | tf_op jit(solution)/shard_map/all_to_all | solution.py:150
  100.2 7.5 %all-to-all-done.1 = bf16[8,16,512]{2,1,0:T(8,128)(2,1)S(1)} async-done(((bf16[8,16,512]{2,1,0:T(8,128)(2,1)}), bf16[8,16,512]{2,1,0:T(8,128)(2,1)S(1)}, u32[]{:S(2)}, u32[]{:S(2)}) %all-to-all-start.1) | async-done | bytes 131104 | tf_op jit(solution)/shard_map/all_to_all | solution.py:150
  107.7 0.7 gather_fusion.1
  108.5 0.2 multiply_reduce_fusion
  108.6 0.6 convert_element_type.115
  109.2 3.3 %all-to-all-start.2 = ((bf16[4,4,512]{2,1,0:T(4,128)(2,1)}), bf16[4,4,512]{2,1,0:T(4,128)(2,1)S(1)}, u32[]{:S(2)}, u32[]{:S(2)}) async-start(bf16[4,4,512]{2,1,0:T(4,128)(2,1)} %convert_element_type.115), calls=%async_computation.3 | async-start | bytes 32768 | tf_op jit(solution)/shard_map/all_to_all | solution.py:155
  112.5 0.1 fusion.60
  112.7 0.6 dynamic-slice
  113.9 2.5 %all-to-all-done.2 = bf16[4,4,512]{2,1,0:T(4,128)(2,1)S(1)} async-done(((bf16[4,4,512]{2,1,0:T(4,128)(2,1)}), bf16[4,4,512]{2,1,0:T(4,128)(2,1)S(1)}, u32[]{:S(2)}, u32[]{:S(2)}) %all-to-all-start.2) | async-done | bytes 16416 | tf_op jit(solution)/shard_map/all_to_all | solution.py:155
  116.3 50.0 %all-reduce.4.cloned.1.call-done = f32[32,2048]{1,0:T(8,128)} async-done(((f32[32,2048]{1,0:T(8,128)}), f32[32,2048]{1,0:T(8,128)}) %all-reduce.4.cloned.1.call-update) | async-done | bytes 262160
  166.4 1.5 fusion.88
  (60 shorter events, 0.7 us)
Async XLA Ops:
  7.4 49.1 %copy-start = (bf16[1,512,2048]{2,1,0:T(8,128)(2,1)S(1)}, bf16[1,512,2048]{2,1,0:T(8,128)(2,1)}, u32[]{:S(2)}) copy-start(bf16[1,512,2048]{2,1,0:T(8,128)(2,1)} %param.37) | copy-start | bytes 6291460
  7.4 89.2 %reduce-scatter.2.cloned.1.call-start = ((), (), s32[]{:S(2)}) async-start(), calls=%async_computation.4 | async-start | bytes 655360 | tf_op jit(solution)/shard_map/reduce_scatter | solution.py:147
  9.8 2.1 %copy-start.2 = (bf16[16,2048]{1,0:T(8,128)(2,1)S(1)}, bf16[16,2048]{1,0:T(8,128)(2,1)}, u32[]{:S(2)}) copy-start(bf16[16,2048]{1,0:T(8,128)(2,1)} %param.21) | copy-start | bytes 196612
  9.8 2.2 %copy-start.4 = (bf16[2048,128]{1,0:T(8,128)(2,1)S(1)}, bf16[2048,128]{1,0:T(8,128)(2,1)}, u32[]{:S(2)}) copy-start(bf16[2048,128]{1,0:T(8,128)(2,1)} %param.23) | copy-start | bytes 1572868
  9.8 2.2 %copy-start.5 = (f32[2048]{0:T(1024)S(1)}, f32[2048]{0:T(1024)}, u32[]{:S(2)}) copy-start(f32[2048]{0:T(1024)} %param.22) | copy-start | bytes 24580
  9.9 2.5 %copy-start.12 = (bf16[2048,2]{0,1:T(2,128)(2,1)S(1)}, bf16[2048,2]{0,1:T(2,128)(2,1)}, u32[]{:S(2)}) copy-start(bf16[2048,2]{0,1:T(2,128)(2,1)} %param.26) | copy-start | bytes 24580
  9.9 2.5 %copy-start.14 = (f32[2]{0:T(128)S(1)}, f32[2]{0:T(128)}, u32[]{:S(2)}) copy-start(f32[2]{0:T(128)} %param.27) | copy-start | bytes 28
  9.9 2.8 %copy-start.10 = (bf16[2048,64]{0,1:T(8,128)(2,1)S(1)}, bf16[2048,64]{0,1:T(8,128)(2,1)}, u32[]{:S(2)}) copy-start(bf16[2048,64]{0,1:T(8,128)(2,1)} %param.24) | copy-start | bytes 786436
  9.9 3.0 %copy-start.11 = (bf16[2048,64]{0,1:T(8,128)(2,1)S(1)}, bf16[2048,64]{0,1:T(8,128)(2,1)}, u32[]{:S(2)}) copy-start(bf16[2048,64]{0,1:T(8,128)(2,1)} %param.25) | copy-start | bytes 786436
  9.9 3.4 %copy-start.1 = (f32[16,2,1024]{2,1,0:T(2,128)S(1)}, f32[16,2,1024]{2,1,0:T(2,128)}, u32[]{:S(2)}) copy-start(f32[16,2,1024]{2,1,0:T(2,128)} %param.30) | copy-start | bytes 393220
  13.3 3.7 %copy-start.9 = (bf16[16,1024,1,128]{3,1,2,0:T(8,128)(2,1)S(1)}, bf16[16,1024,1,128]{3,1,2,0:T(8,128)(2,1)}, u32[]{:S(2)}) copy-start(bf16[16,1024,1,128]{3,1,2,0:T(8,128)(2,1)} %param.29) | copy-start | bytes 12582916
  17.0 1.5 copy-start.3
  17.0 16.3 %copy-start.7 = (s32[16,4]{0,1:T(4,128)S(1)}, s32[16,4]{0,1:T(4,128)}, u32[]{:S(2)}) copy-start(s32[16,4]{0,1:T(4,128)} %param.33) | copy-start | bytes 772
  17.0 17.3 %copy-start.6 = (f32[2048]{0:T(1024)S(1)}, f32[2048]{0:T(1024)}, u32[]{:S(2)}) copy-start(f32[2048]{0:T(1024)} %param.32) | copy-start | bytes 24580
  59.7 106.7 %all-reduce.4.cloned.1.call-start = ((), (), s32[]{:S(2)}) async-start(), calls=%async_computation.5 | async-start | bytes 524288
  92.4 4.1 %copy-start.8 = (f32[16,4]{0,1:T(4,128)S(1)}, f32[16,4]{0,1:T(4,128)}, u32[]{:S(2)}) copy-start(f32[16,4]{0,1:T(4,128)} %param.34) | copy-start | bytes 772
  92.4 20.1 %copy-start.13 = (f32[2048]{0:T(1024)S(1)}, f32[2048]{0:T(1024)}, u32[]{:S(2)}) copy-start(f32[2048]{0:T(1024)} %param.41) | copy-start | bytes 24580
  92.4 20.3 %copy-start.15 = (u32[32]{0:T(128)S(1)}, u32[32]{0:T(128)}, u32[]{:S(2)}) copy-start(u32[32]{0:T(128)} %constant.108) | copy-start | bytes 388
  96.6 11.1 %all-to-all-start.1 = ((bf16[8,16,512]{2,1,0:T(8,128)(2,1)}), bf16[8,16,512]{2,1,0:T(8,128)(2,1)S(1)}, u32[]{:S(2)}, u32[]{:S(2)}) async-start(bf16[8,16,512]{2,1,0:T(8,128)(2,1)} %reduce-scatter.2.cloned.1.call-done), calls=%async_computation.2 | async-start | bytes 262144 | tf_op jit(solution)/shard_map/all_to_all | solution.py:150
  109.2 7.1 %all-to-all-start.2 = ((bf16[4,4,512]{2,1,0:T(4,128)(2,1)}), bf16[4,4,512]{2,1,0:T(4,128)(2,1)S(1)}, u32[]{:S(2)}, u32[]{:S(2)}) async-start(bf16[4,4,512]{2,1,0:T(4,128)(2,1)} %convert_element_type.115), calls=%async_computation.3 | async-start | bytes 32768 | tf_op jit(solution)/shard_map/all_to_all | solution.py:155
Sparse Core Ops, SparseCore 0:
  59.8 20.9 reduce-scatter.1
Sparse Core Ops, SparseCore 1:
  96.4 69.9 all-reduce.3
where the time goes:
time: 176 us; the launch traced here: 175 us
  blocking collectives  64.1 us (36%)
  waiting for transfers between devices  60 us (34%)
  matrix products  17.5 us (10%)
  between operations  15.8 us (9%)
  starting transfers between devices  6.94 us (4%)
  local copies, waits for them, and re-layouts  6 us (3%)
  other arithmetic  4.98 us (3%)
    unnamed x3, waiting for transfers between devices  50.1 us
    all_gather x1, blocking collectives, on_device(): row_piece = lax.all_gather(own_hidden, 'ep', axis=0, tiled=True)  30.5 us
    all_to_all x1, blocking collectives, on_device(): lax.all_to_all(dispatch, 'ep', split_axis=0, concat_axis=0, tiled=True)  19.1 us
    psum x1, blocking collectives, on_device(): attn_out = lax.psum(partial_out, 'tp').astype(jnp.bfloat16)  14.5 us
    all_to_all x1, waiting for transfers between devices, on_device(): lax.all_to_all(shares, 'ep', split_axis=0, concat_axis=0, tiled=True)  7.48 us
    dot_general x1, matrix products, on_device(): jnp.dot(dense_act, dense_down, preferred_element_type=jnp.float32)  3.85 us
    all_to_all x1, starting transfers between devices, on_device(): lax.all_to_all(shares, 'ep', split_axis=0, concat_axis=0, tiled=True)  3.64 us
    dot_general x1, matrix products, on_device(): jnp.einsum('skgd,slkd->skgl', queries, kv_cache[..., :head_dim], preferre...  3.63 us
  transfers between devices with their start and end apart: 4, of which 3 were waited for; matrix products, arithmetic and copies ran while one was open for 5% of the time, Pallas kernels for 0%

commit v1 on v0

v1 whole, which is shorter than its diff:
```python
import jax
import jax.numpy as jnp
from jax import lax
from jax.sharding import PartitionSpec as P

EPS = 1e-05
LIMIT = 7.0
ALPHA = 1.702
LANES = 128
BF16 = jnp.bfloat16
F32 = jnp.float32


def clamped_unit(gate_pre, up_pre):
    capped = jnp.minimum(gate_pre, LIMIT)
    return capped * jax.nn.sigmoid(ALPHA * capped) * (jnp.clip(up_pre, -LIMIT, LIMIT) + 1.0)


def rms_scaled(values, gain_vec):
    return values * lax.rsqrt(jnp.mean(values * values, axis=-1, keepdims=True) + EPS) * gain_vec


def swap_with(values, axis, offset):
    count = lax.axis_size(axis)
    return lax.ppermute(values, axis, [(i, i ^ offset) for i in range(count)])


def stages_of(count):
    groups = []
    bit = 1
    if bit < count:
        groups.append([bit])
        bit *= 2
    while bit < count:
        if 2 * bit < count:
            groups.append([bit, 2 * bit, 3 * bit])
            bit *= 4
        else:
            groups.append([bit])
            bit *= 2
    return groups


def relative_order(values, index, count):
    bit = 1
    while bit < count:
        pairs = values.reshape((count // (2 * bit), 2, bit) + values.shape[1:])
        swapped = jnp.where((index & bit) != 0, pairs[:, ::-1], pairs)
        values = swapped.reshape(values.shape)
        bit *= 2
    return values


def attention(tokens, norm1_gain, query_weight, key_weight, value_weight, forget_weight, forget_bias, kv_cache, log_gates, lengths):
    seq_count = tokens.shape[0]
    local_heads = forget_bias.shape[0]
    kv_local = kv_cache.shape[2]
    head_dim = kv_cache.shape[3] // 2
    per_kv = local_heads // kv_local
    cache_len = kv_cache.shape[1]
    score_scale = head_dim ** (-0.5)
    normed = rms_scaled(tokens.astype(F32), norm1_gain).astype(BF16)
    queries = jnp.dot(normed, query_weight, preferred_element_type=F32).astype(BF16)
    queries = queries.reshape(seq_count, kv_local, per_kv, head_dim)
    key_new = jnp.dot(normed, key_weight, preferred_element_type=F32).astype(BF16)
    key_new = key_new.reshape(seq_count, kv_local, head_dim)
    value_new = jnp.dot(normed, value_weight, preferred_element_type=F32).astype(BF16)
    value_new = value_new.reshape(seq_count, kv_local, head_dim)
    gate_new = jax.nn.log_sigmoid(
        jnp.dot(normed, forget_weight, preferred_element_type=F32) + forget_bias
    )
    scores = (
        jnp.einsum("skgd,slkd->skgl", queries, kv_cache[..., :head_dim], preferred_element_type=F32)
        * score_scale
    )
    places = jnp.arange(cache_len, dtype=jnp.int32)[None, None, :]
    last_gate = jnp.sum(
        jnp.where(places == (lengths - 1)[:, None, None], log_gates, 0.0), axis=2, keepdims=True
    )
    gate_bias = (last_gate - log_gates + gate_new[:, :, None]).reshape(
        seq_count, kv_local, per_kv, cache_len
    )
    live_mask = (places < lengths[:, None, None])[:, :, None, :]
    cached = jnp.where(live_mask, jnp.exp(scores + gate_bias), 0.0)
    own_exp = jnp.exp(
        jnp.einsum("skgd,skd->skg", queries, key_new, preferred_element_type=F32) * score_scale
    )
    denominator = jnp.sum(cached, axis=-1) + own_exp
    weight_cache = (cached / denominator[..., None]).astype(BF16)
    weight_own = (own_exp / denominator).astype(BF16)
    attended = jnp.einsum(
        "skgl,slkd->skgd", weight_cache, kv_cache[..., head_dim:], preferred_element_type=F32
    )
    attended = attended + weight_own.astype(F32)[..., None] * value_new.astype(F32)[:, :, None, :]
    return attended.astype(BF16).reshape(seq_count, local_heads * head_dim)


def two_halves(values):
    high = lax.reduce_precision(values, 8, 7)
    return high.astype(BF16), (values - high).astype(BF16)


def on_device(
    tokens,
    norm1_gain,
    query_weight,
    key_weight,
    value_weight,
    forget_weight,
    forget_bias,
    out_weight,
    kv_cache,
    log_gates,
    lengths,
    norm2_gain,
    routing,
    route_weight,
    expert_gate,
    expert_up,
    expert_down,
    dense_gate,
    dense_up,
    dense_down,
    dense_mix,
):
    seq_count, width = tokens.shape
    tp_count = lax.axis_size("tp")
    ep_count = lax.axis_size("ep")
    tp_index = lax.axis_index("tp")
    ep_index = lax.axis_index("ep")
    own = seq_count // tp_count
    outer = tp_count // 2
    experts = expert_gate.shape[0] * ep_count

    attended = attention(
        tokens, norm1_gain, query_weight, key_weight, value_weight,
        forget_weight, forget_bias, kv_cache, log_gates, lengths,
    )

    def grouped(values):
        ordered = relative_order(values.reshape((tp_count, own) + values.shape[1:]), tp_index, tp_count)
        return ordered.reshape((outer, 2, own) + values.shape[1:])

    chosen = routing[:, :, None] == jnp.arange(experts, dtype=jnp.int32)[None, None, :]
    weights = jnp.sum(jnp.where(chosen, route_weight[:, :, None], 0.0), axis=1)
    weights = grouped(weights)[:, 0].reshape(outer * own, experts)
    tokens_near = grouped(tokens)[:, 0].astype(F32)

    attended = grouped(attended).reshape(seq_count, -1)
    partial = jnp.dot(attended, out_weight, preferred_element_type=F32)
    partial = partial.reshape(outer, 2, own, width)
    total = partial[:, 0] + swap_with(partial[:, 1].astype(BF16), "tp", 1).astype(F32)
    for (offset,) in [[1 << b] for b in range((outer - 1).bit_length())]:
        rounded = total.astype(BF16)
        received = swap_with(rounded, "tp", 2 * offset)
        received = received.reshape((outer // (2 * offset), 2, offset, own, width))[:, ::-1]
        total = rounded.astype(F32) + received.reshape(total.shape).astype(F32)
    residual = (tokens_near + total.astype(BF16).astype(F32)).reshape(outer * own, width)
    hidden_f32 = rms_scaled(residual, norm2_gain)
    hidden = hidden_f32.astype(BF16)
    mix_gate = jax.nn.sigmoid(jnp.sum(hidden.astype(F32) * dense_mix, axis=-1, keepdims=True))
    scales = jnp.concatenate([weights, mix_gate], axis=1)
    side = jnp.concatenate(two_halves(scales), axis=1)
    side_width = -(-side.shape[1] // LANES) * LANES
    side = jnp.pad(side, ((0, 0), (0, side_width - side.shape[1])))
    rows = jnp.concatenate([hidden, side], axis=1)[None]

    for offsets in stages_of(ep_count)[::-1]:
        rows = jnp.concatenate([rows] + [swap_with(rows, "ep", k) for k in offsets], axis=0)
    rows = jnp.stack([rows, swap_with(rows, "tp", 1)])
    total_rows = rows.size // rows.shape[-1]
    rows = rows.reshape(total_rows, width + side_width)

    everyone = rows[:, :width]
    side = rows[:, width:].astype(F32)
    scales = side[:, : experts + 1] + side[:, experts + 1 : 2 * (experts + 1)]
    mix_all = scales[:, experts:]
    units = dense_gate.shape[1] // tp_count
    start = tp_index * units
    acts, downs = [], []
    for j in range(expert_gate.shape[0]):
        here = ep_index * expert_gate.shape[0] + j
        scale = jnp.sum(
            jnp.where(jnp.arange(experts + 1)[None, :] == here, scales, 0.0), axis=1, keepdims=True
        )
        gate_pre = jnp.dot(everyone, expert_gate[j], preferred_element_type=F32)
        up_pre = jnp.dot(everyone, expert_up[j], preferred_element_type=F32)
        acts.append((scale * clamped_unit(gate_pre, up_pre)).astype(BF16))
        downs.append(expert_down[j])
    gate_pre = jnp.dot(
        everyone, lax.dynamic_slice_in_dim(dense_gate, start, units, 1), preferred_element_type=F32
    )
    up_pre = jnp.dot(
        everyone, lax.dynamic_slice_in_dim(dense_up, start, units, 1), preferred_element_type=F32
    )
    acts.append((mix_all * clamped_unit(gate_pre, up_pre)).astype(BF16))
    downs.append(lax.dynamic_slice_in_dim(dense_down, start, units, 0))
    mixed = sum(jnp.dot(a, d, preferred_element_type=F32) for a, d in zip(acts, downs))

    mixed = mixed.reshape(2, ep_count, outer, own, width)
    mixed = mixed[0] + swap_with(mixed[1].astype(BF16), "tp", 1).astype(F32)
    bit = outer // 2
    while bit >= 1:
        received = swap_with(mixed[:, bit : 2 * bit].astype(BF16), "tp", 2 * bit)
        mixed = mixed[:, :bit] + received.astype(F32)
        bit //= 2
    mixed = mixed[:, 0]
    for offsets in stages_of(ep_count):
        mixed = mixed.reshape((len(offsets) + 1, -1) + mixed.shape[1:])
        pieces = [swap_with(mixed[i + 1].astype(BF16), "ep", k) for i, k in enumerate(offsets)]
        mixed = mixed[0] + sum(p.astype(F32) for p in pieces)
    return (residual[:own] + mixed[0]).astype(BF16)


def solution(mesh):
    return jax.shard_map(
        on_device,
        mesh=mesh,
        in_specs=(
            P("ep", None),
            P(),
            P(None, "tp"),
            P(None, "tp"),
            P(None, "tp"),
            P(None, "tp"),
            P("tp"),
            P("tp", None),
            P("ep", None, "tp", None),
            P("ep", "tp", None),
            P("ep"),
            P(),
            P("ep", None),
            P("ep", None),
            P("ep", None, "tp"),
            P("ep", None, "tp"),
            P("ep", "tp", None),
            P(None, "ep"),
            P(None, "ep"),
            P("ep", None),
            P(),
        ),
        out_specs=P(("ep", "tp"), None),
        check_vma=False,
    )
```

time: 176 us -> 68.8 us (0.39)
  blocking collectives: 64.1 us -> 0 us
  waiting for transfers between devices: 60 us -> 23.6 us
  between operations: 15.8 us -> 0.34 us
  starting transfers between devices: 6.94 us -> 17.5 us
  local copies, waits for them, and re-layouts: 6 us -> 3.18 us
    unnamed x3 -> x0, waiting for transfers between devices: 50.1 us -> none
    all_gather x1 -> x0, blocking collectives: 30.5 us -> none  [on_device(): row_piece = lax.all_gather(own_hidden, 'ep', axis=0, tiled=True)]
    ppermute x0 -> x13, waiting for transfers between devices: none -> 23.6 us  [swap_with(): return lax.ppermute(values, axis, [(i, i ^ offset) for i in range(count)])]
    all_to_all x1 -> x0, blocking collectives: 19.1 us -> none  [on_device(): lax.all_to_all(dispatch, 'ep', split_axis=0, concat_axis=0, tiled=True)]
    ppermute x0 -> x13, starting transfers between devices: none -> 17.5 us  [swap_with(): return lax.ppermute(values, axis, [(i, i ^ offset) for i in range(count)])]
    psum x1 -> x0, blocking collectives: 14.5 us -> none  [on_device(): attn_out = lax.psum(partial_out, 'tp').astype(jnp.bfloat16)]
    all_to_all x2 -> x0, waiting for transfers between devices: 9.95 us -> none  [the longest x1 7.48 us: on_device(): lax.all_to_all(shares, 'ep', split_axis=0, concat_axis=0, tiled=True)]
    all_to_all x2 -> x0, starting transfers between devices: 6.9 us -> none  [the longest x1 3.64 us: on_device(): lax.all_to_all(shares, 'ep', split_axis=0, concat_axis=0, tiled=True)]
  transfers between devices with their start and end apart: 4 -> 13, of which waited for: 3 -> 11; matrix products, arithmetic and copies ran while one was open for 5% -> 1% of each run, Pallas kernels for 0% -> 0%
where the time goes in v1:
time: 68.8 us; the launch traced here: 68.4 us
  waiting for transfers between devices  23.6 us (34%)
  matrix products  19 us (28%)
  starting transfers between devices  17.5 us (25%)
  other arithmetic  4.79 us (7%)
  local copies, waits for them, and re-layouts  3.18 us (5%)
    ppermute x13, waiting for transfers between devices, swap_with(): return lax.ppermute(values, axis, [(i, i ^ offset) for i in range(count)])  23.6 us
    ppermute x13, starting transfers between devices, swap_with(): return lax.ppermute(values, axis, [(i, i ^ offset) for i in range(count)])  17.5 us
    dot_general x2, matrix products, on_device(): jnp.dot(a, d, preferred_element_type=F32)  6.49 us
    dot_general x1, matrix products, attention(): jnp.einsum('skgd,slkd->skgl', queries, kv_cache[..., :head_dim], preferre...  3.51 us
    dot_general x1, matrix products, on_device(): gate_pre = jnp.dot(everyone, expert_gate[j], preferred_element_type=F32)  2.04 us
  transfers between devices with their start and end apart: 13, of which 11 were waited for; matrix products, arithmetic and copies ran while one was open for 1% of the time, Pallas kernels for 0%

profile of v1, /device:TPU:0, one launch (start us, length us, event | category | flops | bytes accessed | tf_op | source)
XLA Modules:
  0.0 68.4 jit_solution(6450926508852346009)
XLA Ops:
  0.0 1.1 %fusion.73 = f32[16]{0:T(128)S(1)} fusion(bf16[16,2048]{1,0:T(8,128)(2,1)} %param.21), kind=kLoop, calls=%fused_computation.66 | loop fusion | flops 98288 | bytes 65600 | tf_op jit(solution)/shard_map/reduce_sum | solution.py:20
  1.1 1.3 %convolution_convert_fusion.2 = bf16[16,128]{1,0:T(8,128)(2,1)S(1)} fusion(bf16[2048,128]{1,0:T(8,128)(2,1)} %param.23, bf16[16,2048]{1,0:T(8,128)(2,1)} %param.21, f32[2048]{0:T(1024)} %param.22, f32[16]{0:T(128)S(1)} %add_rsqrt_fusion.1), kind=kOutput, calls=%fused_computation.37 | convolution fusion | flops 8521728 | bytes 602176 | tf_op jit(solution)/shard_map/dot_general | solution.py:63
  2.5 1.1 %fusion.117 = f32[16,2]{0,1:T(2,128)S(1)} fusion(bf16[2048,2]{0,1:T(2,128)(2,1)} %param.26, f32[2]{0:T(128)} %param.27, bf16[16,2048]{1,0:T(8,128)(2,1)} %param.21, f32[2048]{0:T(1024)} %param.22, f32[16]{0:T(128)S(1)} %add_rsqrt_fusion.1), kind=kOutput, calls=%fused_computation.150 | convolution fusion | flops 262432 | bytes 82120 | tf_op jit(solution)/shard_map/dot_general | solution.py:70
  3.7 0.7 broadcast_add_fusion
  4.4 0.7 %iota_compare_fusion = (pred[16,1024]{1,0:T(8,128)(4,1)S(1)}, pred[16,1024]{1,0:T(8,128)(4,1)S(1)}) fusion(s32[16]{0:T(128)S(1)} %broadcast_add_fusion, s32[16]{0:T(128)} %param.31), kind=kLoop, calls=%fused_computation.105 | loop fusion | flops 32768 | bytes 32896 | tf_op jit(solution)/shard_map/eq | solution.py:78
  5.1 1.3 %fusion.52 = bf16[16,64,1]{1,0,2:T(8,128)(2,1)S(1)} fusion(bf16[2048,64]{0,1:T(8,128)(2,1)} %param.24, bf16[16,2048]{1,0:T(8,128)(2,1)} %param.21, f32[2048]{0:T(1024)} %param.22, f32[16]{0:T(128)S(1)} %add_rsqrt_fusion.1), kind=kOutput, calls=%fused_computation.38 | convolution fusion | flops 4326400 | bytes 337984 | tf_op jit(solution)/shard_map/dot_general | solution.py:65
  6.5 3.5 %fusion.38 = f32[16,2,1024]{2,1,0:T(2,128)S(1)} fusion(bf16[16,2,64]{2,1,0:T(2,128)(2,1)S(1)} %reshape.227, bf16[16,1024,1,128]{3,1,2,0:T(8,128)(2,1)} %param.29), kind=kOutput, calls=%fused_computation.25 | convolution fusion | flops 4227072 | bytes 4329472 | tf_op jit(solution)/shard_map/skgd,slkd->skgl/dot_general | solution.py:73
  10.0 0.1 fusion.107
  10.1 0.2 fusion.51
  10.4 0.4 fusion.137
  10.8 1.4 %fusion.48 = bf16[16,2,64]{2,1,0:T(2,128)(2,1)S(1)} fusion(bf16[16,1024,1,128]{3,1,2,0:T(8,128)(2,1)S(1)} %copy-done.1, f32[16,2,1024]{2,1,0:T(2,128)S(1)} %get-tuple-element.19, f32[16,2]{1,0:T(8,128)S(1)} %get-tuple-element.15, f32[16,64]{1,0:T(8,128)S(1)} %fusion.51, f32[16,2]{1,0:T(8,128)S(1)} %get-tuple-element.14), kind=kOutput, calls=%fused_computation.33 | convolution fusion | flops 4265984 | bytes 4333824 | tf_op jit(solution)/shard_map/skgl,slkd->skgd/dot_general | solution.py:91
  12.2 0.1 reshape_reshape_reshape.4
  12.3 0.2 fusion.54
  12.5 0.6 collective-permute-start
  13.4 0.6 collective-permute-done
  14.0 2.9 %collective-permute-start.1 = (bf16[2,4,2048]{2,1,0:T(4,128)(2,1)S(1)}, bf16[2,4,2048]{2,1,0:T(4,128)(2,1)S(1)}, u32[]{:S(2)}, u32[]{:S(2)}) collective-permute-start(bf16[2,4,2048]{2,1,0:T(4,128)(2,1)S(1)} %fusion.87), channel_id=1, source_target_pairs={{0,2},{1,3},{2,0},{3,1},{4,6},{5,7},{6,4},{7,5},{8,10},{9,11},{10,... | collective-permute-start | bytes 98312 | tf_op jit(solution)/shard_map/ppermute | solution.py:25
  16.9 1.9 %collective-permute-done.1 = bf16[2,4,2048]{2,1,0:T(4,128)(2,1)S(1)} collective-permute-done((bf16[2,4,2048]{2,1,0:T(4,128)(2,1)S(1)}, bf16[2,4,2048]{2,1,0:T(4,128)(2,1)S(1)}, u32[]{:S(2)}, u32[]{:S(2)}) %collective-permute-start.1) | collective-permute-done | bytes 32800 | tf_op jit(solution)/shard_map/ppermute | solution.py:25
  18.8 0.1 multiply_reduce_fusion.1
  19.0 0.2 multiply_reduce_fusion
  19.6 2.1 %collective-permute-start.2 = (bf16[1,8,2176]{2,1,0:T(8,128)(2,1)S(1)}, bf16[1,8,2176]{2,1,0:T(8,128)(2,1)S(1)}, u32[]{:S(2)}, u32[]{:S(2)}) collective-permute-start(bf16[1,8,2176]{2,1,0:T(8,128)(2,1)S(1)} %maximum_bitcast_fusion), channel_id=1, source_target_pairs={{0,8},{4,12},{8,0},{12,4},{16,24},{20,28},{24,16},{28,20},{1,9},{5... | collective-permute-start | bytes 104456 | tf_op jit(solution)/shard_map/ppermute | solution.py:25
  21.6 2.6 %collective-permute-start.3 = (bf16[1,8,2176]{2,1,0:T(8,128)(2,1)S(1)}, bf16[1,8,2176]{2,1,0:T(8,128)(2,1)S(1)}, u32[]{:S(2)}, u32[]{:S(2)}) collective-permute-start(bf16[1,8,2176]{2,1,0:T(8,128)(2,1)S(1)} %maximum_bitcast_fusion), channel_id=1, source_target_pairs={{0,16},{4,20},{8,24},{12,28},{16,0},{20,4},{24,8},{28,12},{1,17},{... | collective-permute-start | bytes 104456 | tf_op jit(solution)/shard_map/ppermute | solution.py:25
  24.2 2.5 %collective-permute-done.3 = bf16[1,8,2176]{2,1,0:T(8,128)(2,1)S(1)} collective-permute-done((bf16[1,8,2176]{2,1,0:T(8,128)(2,1)S(1)}, bf16[1,8,2176]{2,1,0:T(8,128)(2,1)S(1)}, u32[]{:S(2)}, u32[]{:S(2)}) %collective-permute-start.3) | collective-permute-done | bytes 34848 | tf_op jit(solution)/shard_map/ppermute | solution.py:25
  26.8 3.2 %collective-permute-done.4 = bf16[1,8,2176]{2,1,0:T(8,128)(2,1)S(1)} collective-permute-done((bf16[1,8,2176]{2,1,0:T(8,128)(2,1)S(1)}, bf16[1,8,2176]{2,1,0:T(8,128)(2,1)S(1)}, u32[]{:S(2)}, u32[]{:S(2)}) %collective-permute-start.4) | collective-permute-done | bytes 34848 | tf_op jit(solution)/shard_map/ppermute | solution.py:25
  30.0 1.6 %collective-permute-start.5 = (bf16[4,8,2176]{2,1,0:T(8,128)(2,1)S(1)}, bf16[4,8,2176]{2,1,0:T(8,128)(2,1)S(1)}, u32[]{:S(2)}, u32[]{:S(2)}) collective-permute-start(bf16[4,8,2176]{2,1,0:T(8,128)(2,1)S(1)} %pad_maximum_fusion.1), channel_id=1, source_target_pairs={{0,4},{4,0},{8,12},{12,8},{16,20},{20,16},{24,28},{28,24},{1,5},{5... | collective-permute-start | bytes 417800 | tf_op jit(solution)/shard_map/ppermute | solution.py:25
  31.6 3.5 %collective-permute-done.5 = bf16[4,8,2176]{2,1,0:T(8,128)(2,1)S(1)} collective-permute-done((bf16[4,8,2176]{2,1,0:T(8,128)(2,1)S(1)}, bf16[4,8,2176]{2,1,0:T(8,128)(2,1)S(1)}, u32[]{:S(2)}, u32[]{:S(2)}) %collective-permute-start.5) | collective-permute-done | bytes 139296 | tf_op jit(solution)/shard_map/ppermute | solution.py:25
  35.2 1.5 %collective-permute-done.6 = bf16[8,8,2176]{2,1,0:T(8,128)(2,1)S(1)} collective-permute-done((bf16[8,8,2176]{2,1,0:T(8,128)(2,1)S(1)}, bf16[8,8,2176]{2,1,0:T(8,128)(2,1)S(1)}, u32[]{:S(2)}, u32[]{:S(2)}) %collective-permute-start.6) | collective-permute-done | bytes 278560 | tf_op jit(solution)/shard_map/ppermute | solution.py:25
  36.8 2.0 %fusion.13 = f32[128,512]{1,0:T(8,128)S(1)} fusion(bf16[1,2048,512]{2,1,0:T(8,128)(2,1)} %param.35, bf16[128,2176]{1,0:T(8,128)(2,1)S(1)} %bitcast.100), kind=kOutput, calls=%fused_computation.14 | convolution fusion | flops 268500992 | bytes 2883584 | tf_op jit(solution)/shard_map/dot_general | solution.py:186
  38.9 0.2 select_reduce_fusion.1
  39.1 0.2 slice_reduce_fusion
  39.2 1.3 %convolution_minimum_fusion = f32[128,128]{1,0:T(8,128)S(1)} fusion(bf16[2048,512]{1,0:T(8,128)(2,1)} %param.38, s32[]{:T(128)S(6)} %select_n.92, bf16[128,2176]{1,0:T(8,128)(2,1)S(1)} %bitcast.101), kind=kOutput, calls=%fused_computation.29 | convolution fusion | flops 67125248 | bytes 1114116 | tf_op jit(solution)/shard_map/dot_general | solution.py:190
  40.6 3.4 %fusion.7 = f32[128,2048]{1,0:T(8,128)} fusion(bf16[1,512,2048]{2,1,0:T(8,128)(2,1)S(1)} %copy-done, bf16[1,2048,512]{2,1,0:T(8,128)(2,1)} %param.36, bf16[128,2176]{1,0:T(8,128)(2,1)S(1)} %bitcast.102, f32[128,512]{1,0:T(8,128)S(1)} %fusion.13, f32[128]{0:T(128)S(1)} %get-tuple-element.7), kind=kOutput, calls=%fused_computation.8 | convolution fusion | flops 537526272 | bytes 6029824 | tf_op jit(solution)/shard_map/dot_general | solution.py:198
  44.0 3.1 %convolution_add_fusion = f32[128,2048]{1,0:T(8,128)} fusion(f32[128,2048]{1,0:T(8,128)} %fusion.7, bf16[512,2048]{1,0:T(8,128)(2,1)} %param.40, s32[]{:T(128)S(6)} %select_n.92, bf16[2048,512]{1,0:T(8,128)(2,1)} %param.39, bf16[128,2176]{1,0:T(8,128)(2,1)S(1)} %bitcast.103, f32[128,128]{1,0:T(8,128)S(1)} %convolution_minimum_fusion, ...), kind=kOutput, calls=%fused_computation.7 | convolution fusion | flops 134643712 | bytes 3737088 | tf_op jit(solution)/shard_map/dot_general | solution.py:198
  47.1 1.1 %slice.182 = bf16[64,2048]{1,0:T(8,128)(2,1)S(1)} slice(f32[128,2048]{1,0:T(8,128)} %convolution_add_fusion), slice={[64:128], [0:2048]} | slice | bytes 524288 | tf_op jit(solution)/shard_map/slice | solution.py:201
  48.2 0.1 convert_element_type.159
  48.3 0.8 %copy.60 = bf16[8,2,4,2048]{3,2,0,1:T(4,128)(2,1)} copy(bf16[8,2,4,2048]{3,2,1,0:T(4,128)(2,1)S(1)} %convert_element_type.159) | data formatting | bytes 524288 | tf_op jit(solution)/shard_map/convert_element_type | solution.py:201
  49.1 0.1 collective-permute-start.7
  49.3 0.1 squeeze.31
  49.4 1.5 %collective-permute-done.7 = bf16[8,2,4,2048]{3,2,0,1:T(4,128)(2,1)S(1)} collective-permute-done((bf16[8,2,4,2048]{3,2,0,1:T(4,128)(2,1)}, bf16[8,2,4,2048]{3,2,0,1:T(4,128)(2,1)S(1)}, u32[]{:S(2)}, u32[]{:S(2)}) %collective-permute-start.7) | collective-permute-done | bytes 262176 | tf_op jit(solution)/shard_map/ppermute | solution.py:25
  50.9 0.1 copy_add_fusion
  51.1 1.6 %collective-permute-start.8 = (bf16[8,1,4,2048]{3,2,0,1:T(4,128)(2,1)S(1)}, bf16[8,1,4,2048]{3,2,0,1:T(4,128)(2,1)S(1)}, u32[]{:S(2)}, u32[]{:S(2)}) collective-permute-start(bf16[8,1,4,2048]{3,2,0,1:T(4,128)(2,1)S(1)} %slice.183), channel_id=1, source_target_pairs={{0,2},{1,3},{2,0},{3,1},{4,6},{5,7},{6,4},{7,5},{8,10},{9,11},{10,... | collective-permute-start | bytes 393224 | tf_op jit(solution)/shard_map/ppermute | solution.py:25
  52.7 4.0 %collective-permute-done.8 = bf16[8,1,4,2048]{3,2,0,1:T(4,128)(2,1)S(1)} collective-permute-done((bf16[8,1,4,2048]{3,2,0,1:T(4,128)(2,1)S(1)}, bf16[8,1,4,2048]{3,2,0,1:T(4,128)(2,1)S(1)}, u32[]{:S(2)}, u32[]{:S(2)}) %collective-permute-start.8) | collective-permute-done | bytes 131104 | tf_op jit(solution)/shard_map/ppermute | solution.py:25
  56.8 1.6 %collective-permute-start.9 = (bf16[4,4,2048]{2,1,0:T(4,128)(2,1)S(1)}, bf16[4,4,2048]{2,1,0:T(4,128)(2,1)S(1)}, u32[]{:S(2)}, u32[]{:S(2)}) collective-permute-start(bf16[4,4,2048]{2,1,0:T(4,128)(2,1)S(1)} %fusion.85), channel_id=1, source_target_pairs={{0,4},{4,0},{8,12},{12,8},{16,20},{20,16},{24,28},{28,24},{1,5},{5... | collective-permute-start | bytes 196616 | tf_op jit(solution)/shard_map/ppermute | solution.py:25
  58.4 2.8 %collective-permute-done.9 = bf16[4,4,2048]{2,1,0:T(4,128)(2,1)S(1)} collective-permute-done((bf16[4,4,2048]{2,1,0:T(4,128)(2,1)S(1)}, bf16[4,4,2048]{2,1,0:T(4,128)(2,1)S(1)}, u32[]{:S(2)}, u32[]{:S(2)}) %collective-permute-start.9) | collective-permute-done | bytes 65568 | tf_op jit(solution)/shard_map/ppermute | solution.py:25
  61.3 0.9 %collective-permute-start.11 = (bf16[1,4,2048]{2,1,0:T(4,128)(2,1)S(1)}, bf16[1,4,2048]{2,1,0:T(4,128)(2,1)S(1)}, u32[]{:S(2)}, u32[]{:S(2)}) collective-permute-start(bf16[1,4,2048]{2,1,0:T(4,128)(2,1)S(1)} %get-tuple-element.13), channel_id=1, source_target_pairs={{0,16},{4,20},{8,24},{12,28},{16,0},{20,4},{24,8},{28,12},{1,17},{... | collective-permute-start | bytes 49160 | tf_op jit(solution)/shard_map/ppermute | solution.py:25
  62.2 3.4 %collective-permute-start.12 = (bf16[1,4,2048]{2,1,0:T(4,128)(2,1)S(1)}, bf16[1,4,2048]{2,1,0:T(4,128)(2,1)S(1)}, u32[]{:S(2)}, u32[]{:S(2)}) collective-permute-start(bf16[1,4,2048]{2,1,0:T(4,128)(2,1)S(1)} %get-tuple-element.12), channel_id=1, source_target_pairs={{0,24},{4,28},{8,16},{12,20},{16,8},{20,12},{24,0},{28,4},{1,25},{... | collective-permute-start | bytes 49160 | tf_op jit(solution)/shard_map/ppermute | solution.py:25
  65.7 0.3 collective-permute-done.11
  66.0 1.8 %collective-permute-done.12 = bf16[1,4,2048]{2,1,0:T(4,128)(2,1)S(1)} collective-permute-done((bf16[1,4,2048]{2,1,0:T(4,128)(2,1)S(1)}, bf16[1,4,2048]{2,1,0:T(4,128)(2,1)S(1)}, u32[]{:S(2)}, u32[]{:S(2)}) %collective-permute-start.12) | collective-permute-done | bytes 16416 | tf_op jit(solution)/shard_map/ppermute | solution.py:25
  67.8 0.6 fusion.104
  (69 shorter events, 1.5 us)
Async XLA Ops:
  0.0 40.6 %copy-start = (bf16[1,512,2048]{2,1,0:T(8,128)(2,1)S(1)}, bf16[1,512,2048]{2,1,0:T(8,128)(2,1)}, u32[]{:S(2)}) copy-start(bf16[1,512,2048]{2,1,0:T(8,128)(2,1)} %param.37) | copy-start | bytes 6291460
  5.1 5.0 %copy-start.9 = (bf16[2048,64]{0,1:T(8,128)(2,1)S(1)}, bf16[2048,64]{0,1:T(8,128)(2,1)}, u32[]{:S(2)}) copy-start(bf16[2048,64]{0,1:T(8,128)(2,1)} %param.25) | copy-start | bytes 786436
  6.4 3.7 %copy-start.2 = (bf16[16,2048]{1,0:T(8,128)(2,1)S(1)}, bf16[16,2048]{1,0:T(8,128)(2,1)}, u32[]{:S(2)}) copy-start(bf16[16,2048]{1,0:T(8,128)(2,1)} %param.21) | copy-start | bytes 196612
  6.4 3.7 %copy-start.5 = (f32[2048]{0:T(1024)S(1)}, f32[2048]{0:T(1024)}, u32[]{:S(2)}) copy-start(f32[2048]{0:T(1024)} %param.22) | copy-start | bytes 24580
  6.4 4.0 %copy-start.10 = (f32[16,2,1024]{2,1,0:T(2,128)S(1)}, f32[16,2,1024]{2,1,0:T(2,128)}, u32[]{:S(2)}) copy-start(f32[16,2,1024]{2,1,0:T(2,128)} %param.30) | copy-start | bytes 393220
  6.4 4.3 %copy-start.1 = (bf16[16,1024,1,128]{3,1,2,0:T(8,128)(2,1)S(1)}, bf16[16,1024,1,128]{3,1,2,0:T(8,128)(2,1)}, u32[]{:S(2)}) copy-start(bf16[16,1024,1,128]{3,1,2,0:T(8,128)(2,1)} %param.29) | copy-start | bytes 12582916
  10.8 1.6 %copy-start.3 = (bf16[128,2048]{1,0:T(8,128)(2,1)S(1)}, bf16[128,2048]{1,0:T(8,128)(2,1)}, u32[]{:S(2)}) copy-start(bf16[128,2048]{1,0:T(8,128)(2,1)} %param.28) | copy-start | bytes 1572868
  10.8 2.5 %copy-start.7 = (f32[16,4]{0,1:T(4,128)S(1)}, f32[16,4]{0,1:T(4,128)}, u32[]{:S(2)}) copy-start(f32[16,4]{0,1:T(4,128)} %param.34) | copy-start | bytes 772
  10.8 2.5 %copy-start.8 = (s32[16,4]{0,1:T(4,128)S(1)}, s32[16,4]{0,1:T(4,128)}, u32[]{:S(2)}) copy-start(s32[16,4]{0,1:T(4,128)} %param.33) | copy-start | bytes 772
  10.8 8.2 %copy-start.4 = (f32[2048]{0:T(1024)S(1)}, f32[2048]{0:T(1024)}, u32[]{:S(2)}) copy-start(f32[2048]{0:T(1024)} %param.32) | copy-start | bytes 24580
  10.8 8.2 %copy-start.6 = (f32[2048]{0:T(1024)S(1)}, f32[2048]{0:T(1024)}, u32[]{:S(2)}) copy-start(f32[2048]{0:T(1024)} %param.41) | copy-start | bytes 24580
  12.5 1.4 %collective-permute-start = (bf16[2,4,2048]{2,1,0:T(4,128)(2,1)S(1)}, bf16[2,4,2048]{2,1,0:T(4,128)(2,1)S(1)}, u32[]{:S(2)}, u32[]{:S(2)}) collective-permute-start(bf16[2,4,2048]{2,1,0:T(4,128)(2,1)S(1)} %fusion.96), channel_id=1, source_target_pairs={{0,1},{1,0},{2,3},{3,2},{4,5},{5,4},{6,7},{7,6},{8,9},{9,8},{10,11... | collective-permute-start | bytes 98312 | tf_op jit(solution)/shard_map/ppermute | solution.py:25
  14.0 4.8 %collective-permute-start.1 = (bf16[2,4,2048]{2,1,0:T(4,128)(2,1)S(1)}, bf16[2,4,2048]{2,1,0:T(4,128)(2,1)S(1)}, u32[]{:S(2)}, u32[]{:S(2)}) collective-permute-start(bf16[2,4,2048]{2,1,0:T(4,128)(2,1)S(1)} %fusion.87), channel_id=1, source_target_pairs={{0,2},{1,3},{2,0},{3,1},{4,6},{5,7},{6,4},{7,5},{8,10},{9,11},{10,... | collective-permute-start | bytes 98312 | tf_op jit(solution)/shard_map/ppermute | solution.py:25
  19.6 4.7 %collective-permute-start.2 = (bf16[1,8,2176]{2,1,0:T(8,128)(2,1)S(1)}, bf16[1,8,2176]{2,1,0:T(8,128)(2,1)S(1)}, u32[]{:S(2)}, u32[]{:S(2)}) collective-permute-start(bf16[1,8,2176]{2,1,0:T(8,128)(2,1)S(1)} %maximum_bitcast_fusion), channel_id=1, source_target_pairs={{0,8},{4,12},{8,0},{12,4},{16,24},{20,28},{24,16},{28,20},{1,9},{5... | collective-permute-start | bytes 104456 | tf_op jit(solution)/shard_map/ppermute | solution.py:25
  21.6 5.1 %collective-permute-start.3 = (bf16[1,8,2176]{2,1,0:T(8,128)(2,1)S(1)}, bf16[1,8,2176]{2,1,0:T(8,128)(2,1)S(1)}, u32[]{:S(2)}, u32[]{:S(2)}) collective-permute-start(bf16[1,8,2176]{2,1,0:T(8,128)(2,1)S(1)} %maximum_bitcast_fusion), channel_id=1, source_target_pairs={{0,16},{4,20},{8,24},{12,28},{16,0},{20,4},{24,8},{28,12},{1,17},{... | collective-permute-start | bytes 104456 | tf_op jit(solution)/shard_map/ppermute | solution.py:25
  24.2 5.7 %collective-permute-start.4 = (bf16[1,8,2176]{2,1,0:T(8,128)(2,1)S(1)}, bf16[1,8,2176]{2,1,0:T(8,128)(2,1)S(1)}, u32[]{:S(2)}, u32[]{:S(2)}) collective-permute-start(bf16[1,8,2176]{2,1,0:T(8,128)(2,1)S(1)} %maximum_bitcast_fusion), channel_id=1, source_target_pairs={{0,24},{4,28},{8,16},{12,20},{16,8},{20,12},{24,0},{28,4},{1,25},{... | collective-permute-start | bytes 104456 | tf_op jit(solution)/shard_map/ppermute | solution.py:25
  30.0 5.1 %collective-permute-start.5 = (bf16[4,8,2176]{2,1,0:T(8,128)(2,1)S(1)}, bf16[4,8,2176]{2,1,0:T(8,128)(2,1)S(1)}, u32[]{:S(2)}, u32[]{:S(2)}) collective-permute-start(bf16[4,8,2176]{2,1,0:T(8,128)(2,1)S(1)} %pad_maximum_fusion.1), channel_id=1, source_target_pairs={{0,4},{4,0},{8,12},{12,8},{16,20},{20,16},{24,28},{28,24},{1,5},{5... | collective-permute-start | bytes 417800 | tf_op jit(solution)/shard_map/ppermute | solution.py:25
  35.1 1.6 %collective-permute-start.6 = (bf16[8,8,2176]{2,1,0:T(8,128)(2,1)S(1)}, bf16[8,8,2176]{2,1,0:T(8,128)(2,1)S(1)}, u32[]{:S(2)}, u32[]{:S(2)}) collective-permute-start(bf16[8,8,2176]{2,1,0:T(8,128)(2,1)S(1)} %constant_dynamic-update-slice_fusion), channel_id=1, source_target_pairs={{0,1},{1,0},{2,3},{3,2},{4,5},{5,4},{6,7},{7,6},{8,9},{9,8},{10,11... | collective-permute-start | bytes 835592 | tf_op jit(solution)/shard_map/ppermute | solution.py:25
  47.1 2.2 %slice-start = ((f32[128,2048]{1,0:T(8,128)}), f32[64,2048]{1,0:T(8,128)S(1)}, s32[]{:S(2)}) async-start(f32[128,2048]{1,0:T(8,128)} %convolution_add_fusion), calls=%async_computation | async-start | bytes 1048576 | tf_op jit(solution)/shard_map/slice | solution.py:201
  49.1 1.7 %collective-permute-start.7 = (bf16[8,2,4,2048]{3,2,0,1:T(4,128)(2,1)}, bf16[8,2,4,2048]{3,2,0,1:T(4,128)(2,1)S(1)}, u32[]{:S(2)}, u32[]{:S(2)}) collective-permute-start(bf16[8,2,4,2048]{3,2,0,1:T(4,128)(2,1)} %copy.60), channel_id=1, source_target_pairs={{0,1},{1,0},{2,3},{3,2},{4,5},{5,4},{6,7},{7,6},{8,9},{9,8},{10,11... | collective-permute-start | bytes 786440 | tf_op jit(solution)/shard_map/ppermute | solution.py:25
  51.1 5.6 %collective-permute-start.8 = (bf16[8,1,4,2048]{3,2,0,1:T(4,128)(2,1)S(1)}, bf16[8,1,4,2048]{3,2,0,1:T(4,128)(2,1)S(1)}, u32[]{:S(2)}, u32[]{:S(2)}) collective-permute-start(bf16[8,1,4,2048]{3,2,0,1:T(4,128)(2,1)S(1)} %slice.183), channel_id=1, source_target_pairs={{0,2},{1,3},{2,0},{3,1},{4,6},{5,7},{6,4},{7,5},{8,10},{9,11},{10,... | collective-permute-start | bytes 393224 | tf_op jit(solution)/shard_map/ppermute | solution.py:25
  56.8 4.3 %collective-permute-start.9 = (bf16[4,4,2048]{2,1,0:T(4,128)(2,1)S(1)}, bf16[4,4,2048]{2,1,0:T(4,128)(2,1)S(1)}, u32[]{:S(2)}, u32[]{:S(2)}) collective-permute-start(bf16[4,4,2048]{2,1,0:T(4,128)(2,1)S(1)} %fusion.85), channel_id=1, source_target_pairs={{0,4},{4,0},{8,12},{12,8},{16,20},{20,16},{24,28},{28,24},{1,5},{5... | collective-permute-start | bytes 196616 | tf_op jit(solution)/shard_map/ppermute | solution.py:25
  61.2 4.5 %collective-permute-start.10 = (bf16[1,4,2048]{2,1,0:T(4,128)(2,1)S(1)}, bf16[1,4,2048]{2,1,0:T(4,128)(2,1)S(1)}, u32[]{:S(2)}, u32[]{:S(2)}) collective-permute-start(bf16[1,4,2048]{2,1,0:T(4,128)(2,1)S(1)} %get-tuple-element.11), channel_id=1, source_target_pairs={{0,8},{4,12},{8,0},{12,4},{16,24},{20,28},{24,16},{28,20},{1,9},{5... | collective-permute-start | bytes 49160 | tf_op jit(solution)/shard_map/ppermute | solution.py:25
  61.3 4.7 %collective-permute-start.11 = (bf16[1,4,2048]{2,1,0:T(4,128)(2,1)S(1)}, bf16[1,4,2048]{2,1,0:T(4,128)(2,1)S(1)}, u32[]{:S(2)}, u32[]{:S(2)}) collective-permute-start(bf16[1,4,2048]{2,1,0:T(4,128)(2,1)S(1)} %get-tuple-element.13), channel_id=1, source_target_pairs={{0,16},{4,20},{8,24},{12,28},{16,0},{20,4},{24,8},{28,12},{1,17},{... | collective-permute-start | bytes 49160 | tf_op jit(solution)/shard_map/ppermute | solution.py:25
  62.2 5.5 %collective-permute-start.12 = (bf16[1,4,2048]{2,1,0:T(4,128)(2,1)S(1)}, bf16[1,4,2048]{2,1,0:T(4,128)(2,1)S(1)}, u32[]{:S(2)}, u32[]{:S(2)}) collective-permute-start(bf16[1,4,2048]{2,1,0:T(4,128)(2,1)S(1)} %get-tuple-element.12), channel_id=1, source_target_pairs={{0,24},{4,28},{8,16},{12,20},{16,8},{20,12},{24,0},{28,4},{1,25},{... | collective-permute-start | bytes 49160 | tf_op jit(solution)/shard_map/ppermute | solution.py:25

commit v2 on v1

v2 whole, which is shorter than its diff:
```python
import functools

import jax
import jax.numpy as jnp
from jax import lax
from jax.experimental import pallas as pl
from jax.experimental.pallas import tpu as pltpu
from jax.sharding import PartitionSpec as P

EPS = 1e-05
LIMIT = 7.0
ALPHA = 1.702
LANES = 128
ROW_BLOCK = 128
COLUMN_BLOCK = 512
FFN_VMEM = 16 * 1024 * 1024
ATTENTION_VMEM = 16 * 1024 * 1024
LOAD_VMEM = 1024 * 1024
SEQ_BLOCK = 8
LOAD_COST = 4 * 10**9
BF16 = jnp.bfloat16
F32 = jnp.float32


def clamped_unit(gate_pre, up_pre):
    capped = jnp.minimum(gate_pre, LIMIT)
    return capped * jax.nn.sigmoid(ALPHA * capped) * (jnp.clip(up_pre, -LIMIT, LIMIT) + 1.0)


def rms_scaled(values, gain_vec):
    return values * lax.rsqrt(jnp.mean(values * values, axis=-1, keepdims=True) + EPS) * gain_vec


def swap_with(values, axis, offset):
    count = lax.axis_size(axis)
    return lax.ppermute(values, axis, [(i, i ^ offset) for i in range(count)])


def stages_of(count):
    groups = []
    bit = 1
    if bit < count:
        groups.append([bit])
        bit *= 2
    while bit < count:
        if 2 * bit < count:
            groups.append([bit, 2 * bit, 3 * bit])
            bit *= 4
        else:
            groups.append([bit])
            bit *= 2
    return groups


def relative_order(values, index, count):
    bit = 1
    while bit < count:
        pairs = values.reshape((count // (2 * bit), 2, bit) + values.shape[1:])
        swapped = jnp.where((index & bit) != 0, pairs[:, ::-1], pairs)
        values = swapped.reshape(values.shape)
        bit *= 2
    return values


def attention_kernel(
    own, heads, lengths_hbm, bias_hbm, tokens_hbm, gain_hbm, query_hbm, key_hbm, value_hbm, forget_hbm,
    cache_hbm, gates_hbm, out_hbm, keep_ref, send_ref, near_ref,
    tokens_buf, gain_buf, query_buf, pair_buf, forget_buf, cache_buf, gates_buf, out_buf,
    lengths_ref, bias_ref, sems, cache_sems,
):
    seq_count, width = tokens_buf.shape
    cache_len, lanes = cache_buf.shape[1:]
    head_dim = lanes // 2
    rows = seq_count * heads
    tp_count = seq_count // own
    outer = tp_count // 2
    pairs = [
        (tokens_hbm, tokens_buf),
        (gain_hbm, gain_buf),
        (query_hbm, query_buf),
        (key_hbm, pair_buf.at[pl.ds(0, head_dim), :]),
        (value_hbm, pair_buf.at[pl.ds(head_dim, head_dim), :]),
        (forget_hbm, forget_buf),
        (gates_hbm, gates_buf),
        (lengths_hbm, lengths_ref),
        (bias_hbm, bias_ref),
        (out_hbm, out_buf),
    ]
    copies = [pltpu.make_async_copy(src, dst, sems.at[i]) for i, (src, dst) in enumerate(pairs)]
    cache_copies = [
        pltpu.make_async_copy(cache_hbm.at[s], cache_buf.at[s], cache_sems.at[s]) for s in range(seq_count)
    ]
    for copy in copies[:-1]:
        copy.start()
    for copy in cache_copies:
        copy.start()
    copies[-1].start()

    def one_hot(condition):
        return jnp.where(condition, 1.0, 0.0).astype(BF16)

    copies[0].wait()
    copies[1].wait()
    tokens = tokens_buf[...].astype(F32)
    normed = rms_scaled(tokens, gain_buf[...]).astype(BF16)
    spread = one_hot(
        lax.broadcasted_iota(jnp.int32, (rows, seq_count), 0) // heads
        == lax.broadcasted_iota(jnp.int32, (rows, seq_count), 1)
    )
    normed = jnp.dot(spread, normed, preferred_element_type=F32).astype(BF16)
    order = one_hot(
        chosen_rows(seq_count, seq_count, own, outer)
        == lax.broadcasted_iota(jnp.int32, (seq_count, seq_count), 1)
    )
    near_ref[...] = jnp.dot(order, tokens_buf[...], preferred_element_type=F32)[: seq_count // 2]

    transposed = (((1,), (1,)), ((), ()))
    copies[2].wait()
    queries = jnp.dot(normed, query_buf[...], preferred_element_type=F32).astype(BF16).astype(F32)
    copies[3].wait()
    copies[4].wait()
    own_pair = lax.dot_general(normed, pair_buf[...], transposed, preferred_element_type=F32)
    own_pair = own_pair.astype(BF16).astype(F32)
    copies[5].wait()
    copies[7].wait()
    copies[8].wait()
    forget = lax.dot_general(normed, forget_buf[...], transposed, preferred_element_type=F32)

    lane = lax.broadcasted_iota(jnp.int32, (rows, lanes), 1)
    head = lax.rem(lax.broadcasted_iota(jnp.int32, (rows, lanes), 0), heads)
    queries = jnp.where(head == 0, queries, pltpu.roll(queries, head_dim, 1))
    queries = jnp.where(lane < head_dim, queries, 0.0)
    own_score = jnp.sum(queries * own_pair, axis=1, keepdims=True)
    queries = queries.astype(BF16)

    column = lax.broadcasted_iota(jnp.int32, (rows, heads), 1)
    forget_head = lax.rem(lax.broadcasted_iota(jnp.int32, (rows, heads), 0), heads)
    forget = jnp.sum(jnp.where(column == forget_head, forget, 0.0), axis=1, keepdims=True)
    head_one = lax.rem(lax.broadcasted_iota(jnp.int32, (rows, 1), 0), heads)
    forget = forget + jnp.where(head_one == 0, bias_ref[0], bias_ref[1])
    gate_new = jnp.minimum(forget, 0.0) - jnp.log(1.0 + jnp.exp(-jnp.abs(forget)))

    group = SEQ_BLOCK
    span = group * heads
    scale = head_dim ** (-0.5)
    sequence = lax.broadcasted_iota(jnp.int32, (span, 1), 0) // heads
    place = lax.broadcasted_iota(jnp.int32, (span, cache_len), 1)
    copies[6].wait()
    outputs = []
    for first in range(0, seq_count, group):
        at = slice(first * heads, first * heads + span)
        scores = jnp.zeros((span, cache_len), F32)
        length = jnp.zeros((span, 1), jnp.int32)
        for i in range(group):
            cache_copies[first + i].wait()
            found = lax.dot_general(
                queries[at], cache_buf[first + i], transposed, preferred_element_type=F32
            )
            scores = jnp.where(sequence == i, found, scores)
            length = jnp.where(sequence == i, lengths_ref[first + i], length)
        gates = jnp.concatenate([gates_buf[first + i] for i in range(group)], axis=0)
        last = jnp.sum(jnp.where(place == length - 1, gates, 0.0), axis=1, keepdims=True)
        scores = scores * scale + (last - gates + gate_new[at])
        cached = jnp.where(place < length, jnp.exp(scores), 0.0)
        own_exp = jnp.exp(own_score[at] * scale)
        denominator = jnp.sum(cached, axis=1, keepdims=True) + own_exp
        probs = (cached / denominator).astype(BF16)
        probs_own = (own_exp / denominator).astype(BF16).astype(F32)
        mixed = jnp.zeros((span, lanes), F32)
        for i in range(group):
            found = jnp.dot(probs, cache_buf[first + i], preferred_element_type=F32)
            mixed = jnp.where(sequence == i, found, mixed)
        outputs.append(mixed + probs_own * own_pair[at])
    attended = jnp.concatenate(outputs, axis=0)
    attended = jnp.where(head == 0, pltpu.roll(attended, head_dim, 1), attended)
    attended = jnp.where((lane < head_dim) == (head == 0), attended, 0.0).astype(BF16)
    gather = one_hot(
        chosen_rows(seq_count, rows, own, outer)
        == lax.broadcasted_iota(jnp.int32, (seq_count, rows), 1) // heads
    )
    attended = jnp.dot(gather, attended, preferred_element_type=F32).astype(BF16)
    copies[9].wait()
    partial = jnp.dot(attended, out_buf[...], preferred_element_type=F32)
    keep_ref[...] = partial[: seq_count // 2]
    send_ref[...] = partial[seq_count // 2 :].astype(BF16)


def in_hbm(*arrays):
    return [pltpu.with_memory_space_constraint(array, pltpu.HBM) for array in arrays]


def chosen_rows(seq_count, columns, own, outer):
    place = lax.broadcasted_iota(jnp.int32, (seq_count, columns), 0)
    low = place // (outer * own)
    high = lax.rem(place // own, outer)
    owner = lax.axis_index("tp") ^ (high * 2 + low)
    return owner * own + lax.rem(place, own)


def attention(
    tokens, norm1_gain, query_weight, key_weight, value_weight, forget_weight, forget_bias,
    out_weight, kv_cache, log_gates, lengths, own,
):
    seq_count, width = tokens.shape
    heads = forget_bias.shape[0]
    cache_len, kv_local, lanes = kv_cache.shape[1:]
    assert kv_local == 1 and heads == 2 and lanes == LANES
    half = seq_count // 2
    near = pl.BlockSpec(memory_space=pltpu.VMEM)
    far = pl.BlockSpec(memory_space=pl.ANY)
    return pl.pallas_call(
        functools.partial(attention_kernel, own, heads),
        out_shape=(
            pltpu.VMEM((half, width), F32),
            pltpu.VMEM((half, width), BF16),
            pltpu.VMEM((half, width), F32),
        ),
        in_specs=[far] * 11,
        out_specs=(near,) * 3,
        scratch_shapes=[
            pltpu.VMEM((seq_count, width), BF16),
            pltpu.VMEM((1, width), F32),
            pltpu.VMEM(query_weight.shape, BF16),
            pltpu.VMEM((lanes, width), BF16),
            pltpu.VMEM((heads, width), BF16),
            pltpu.VMEM((seq_count, cache_len, lanes), BF16),
            pltpu.VMEM(log_gates.shape, F32),
            pltpu.VMEM(out_weight.shape, BF16),
            pltpu.SMEM((seq_count,), jnp.int32),
            pltpu.SMEM((heads,), F32),
            pltpu.SemaphoreType.DMA((10,)),
            pltpu.SemaphoreType.DMA((seq_count,)),
        ],
        compiler_params=pltpu.CompilerParams(vmem_limit_bytes=ATTENTION_VMEM),
        name="attention",
    )(
        *in_hbm(
            lengths, forget_bias, tokens, norm1_gain.reshape(1, width), query_weight, key_weight.T, value_weight.T, forget_weight.T,
            kv_cache.reshape(seq_count, cache_len, lanes), log_gates, out_weight,
        ),
    )


def load_kernel(count, units, after_ref, *refs):
    del after_ref
    sources, targets, sems = refs[:count], refs[count:-1], refs[-1]
    pairs = list(zip(sources[:3], targets[:3]))
    if count > 3:
        start = pl.multiple_of(lax.axis_index("tp") * units, units)
        here = pl.ds(start, units)
        pairs += [
            (sources[3].at[:, here], targets[3].at[:, pl.ds(0, units)]),
            (sources[4].at[:, here], targets[3].at[:, pl.ds(units, units)]),
            (sources[5].at[here, :], targets[4]),
        ]
    copies = [pltpu.make_async_copy(src, dst, sems.at[i]) for i, (src, dst) in enumerate(pairs)]
    for copy in copies:
        copy.start()
    for copy in copies:
        copy.wait()


def load_weights(after, expert_weights, dense_weights, units):
    width = dense_weights[0].shape[0]
    near = pl.BlockSpec(memory_space=pltpu.VMEM)
    far = pl.BlockSpec(memory_space=pltpu.HBM)
    shapes = [weight.shape for weight in expert_weights]
    sources = list(expert_weights)
    split = units % LANES == 0
    if split:
        shapes += [(width, 2 * units), (units, width)]
        sources += dense_weights
    count = len(sources)
    loaded = pl.pallas_call(
        functools.partial(load_kernel, count, units),
        out_shape=tuple(pltpu.VMEM(shape, BF16) for shape in shapes),
        in_specs=[near] + [far] * count,
        out_specs=(near,) * len(shapes),
        scratch_shapes=[pltpu.SemaphoreType.DMA((count,))],
        compiler_params=pltpu.CompilerParams(vmem_limit_bytes=LOAD_VMEM),
        cost_estimate=pl.CostEstimate(flops=LOAD_COST, bytes_accessed=8 * width * width, transcendentals=0),
        name="load",
    )(after, *in_hbm(*sources))
    if split:
        return list(loaded)
    gate, up, down = dense_weights
    fill = -gate.shape[1] % LANES
    both = jnp.concatenate([jnp.pad(gate, ((0, 0), (0, fill))), jnp.pad(up, ((0, 0), (0, fill)))], axis=1)
    return [*loaded, both, jnp.pad(down, ((0, fill), (0, 0)))]


def ffn_kernel(
    experts, part, rows_ref, gate_ref, up_ref, down_ref, both_ref, dense_down_ref, keep_ref, send_ref
):
    local, width = gate_ref.shape[:2]
    units = dense_down_ref.shape[0]
    half = rows_ref.shape[0] // 2
    first = lax.axis_index("ep") * local

    def products(at):
        values = rows_ref[at, :width]
        side = rows_ref[at, width:].astype(F32)
        lane = lax.broadcasted_iota(jnp.int32, side.shape, 1)

        def pick(column):
            hit = (lane == column) | (lane == column + experts + 1)
            return jnp.sum(jnp.where(hit, side, 0.0), axis=1, keepdims=True)

        both = jnp.dot(values, both_ref[...], preferred_element_type=F32)
        act = pick(experts) * clamped_unit(both[:, :units], both[:, units:])
        if part != units:
            unit = lax.broadcasted_iota(jnp.int32, act.shape, 1)
            start = lax.axis_index("tp") * part
            act = jnp.where((unit >= start) & (unit < start + part), act, 0.0)
        acts = [act.astype(BF16)]
        for j in range(local):
            gate_pre = jnp.dot(values, gate_ref[j], preferred_element_type=F32)
            up_pre = jnp.dot(values, up_ref[j], preferred_element_type=F32)
            acts.append((pick(first + j) * clamped_unit(gate_pre, up_pre)).astype(BF16))
        step = min(width, COLUMN_BLOCK)
        for column in range(0, width, step):
            cols = slice(column, column + step)
            mixed = jnp.dot(acts[0], dense_down_ref[:, cols], preferred_element_type=F32)
            for j in range(local):
                mixed = mixed + jnp.dot(acts[1 + j], down_ref[j, :, cols], preferred_element_type=F32)
            yield cols, mixed

    if 2 * half <= ROW_BLOCK:
        for cols, mixed in products(slice(0, 2 * half)):
            keep_ref[:, cols] = mixed[:half]
            send_ref[:, cols] = mixed[half:].astype(BF16)
        return
    block = min(half, ROW_BLOCK)

    @pl.loop(0, half // block)
    def _(index):
        at = pl.ds(pl.multiple_of(index * block, block), block)
        for cols, mixed in products(at):
            keep_ref[at, cols] = mixed
        for cols, mixed in products(pl.ds(pl.multiple_of(index * block + half, block), block)):
            send_ref[at, cols] = mixed.astype(BF16)


def ffn(rows, weights, experts, part):
    total = rows.shape[0]
    width = weights[0].shape[1]
    near = pl.BlockSpec(memory_space=pltpu.VMEM)
    return pl.pallas_call(
        functools.partial(ffn_kernel, experts, part),
        out_shape=(
            jax.ShapeDtypeStruct((total // 2, width), F32),
            jax.ShapeDtypeStruct((total // 2, width), BF16),
        ),
        in_specs=[near] * 6,
        out_specs=(near, near),
        compiler_params=pltpu.CompilerParams(vmem_limit_bytes=FFN_VMEM),
        name="ffn",
    )(rows, *weights)


def two_halves(values):
    high = lax.reduce_precision(values, 8, 7)
    return high.astype(BF16), (values - high).astype(BF16)


def on_device(
    tokens,
    norm1_gain,
    query_weight,
    key_weight,
    value_weight,
    forget_weight,
    forget_bias,
    out_weight,
    kv_cache,
    log_gates,
    lengths,
    norm2_gain,
    routing,
    route_weight,
    expert_gate,
    expert_up,
    expert_down,
    dense_gate,
    dense_up,
    dense_down,
    dense_mix,
):
    seq_count, width = tokens.shape
    tp_count = lax.axis_size("tp")
    ep_count = lax.axis_size("ep")
    tp_index = lax.axis_index("tp")
    ep_index = lax.axis_index("ep")
    own = seq_count // tp_count
    outer = tp_count // 2
    experts = expert_gate.shape[0] * ep_count

    keep, sent, tokens_near = attention(
        tokens, norm1_gain, query_weight, key_weight, value_weight, forget_weight, forget_bias,
        out_weight, kv_cache, log_gates, lengths, own,
    )

    def grouped(values):
        ordered = relative_order(values.reshape((tp_count, own) + values.shape[1:]), tp_index, tp_count)
        return ordered.reshape((outer, 2, own) + values.shape[1:])

    chosen = routing[:, :, None] == jnp.arange(experts, dtype=jnp.int32)[None, None, :]
    weights = jnp.sum(jnp.where(chosen, route_weight[:, :, None], 0.0), axis=1)
    weights = grouped(weights)[:, 0].reshape(outer * own, experts)
    total = (keep + swap_with(sent, "tp", 1).astype(F32)).reshape(outer, own, width)
    for (offset,) in [[1 << b] for b in range((outer - 1).bit_length())]:
        rounded = total.astype(BF16)
        received = swap_with(rounded, "tp", 2 * offset)
        received = received.reshape((outer // (2 * offset), 2, offset, own, width))[:, ::-1]
        total = rounded.astype(F32) + received.reshape(total.shape).astype(F32)
    residual = tokens_near + total.astype(BF16).astype(F32).reshape(outer * own, width)
    hidden_f32 = rms_scaled(residual, norm2_gain)
    hidden = hidden_f32.astype(BF16)
    mix_gate = jax.nn.sigmoid(jnp.sum(hidden.astype(F32) * dense_mix, axis=-1, keepdims=True))
    scales = jnp.concatenate([weights, mix_gate], axis=1)
    side = jnp.concatenate(two_halves(scales), axis=1)
    side_width = -(-side.shape[1] // LANES) * LANES
    side = jnp.pad(side, ((0, 0), (0, side_width - side.shape[1])))
    rows = jnp.concatenate([hidden, side], axis=1)[None]
    units = dense_gate.shape[1] // tp_count
    weights_near = load_weights(
        side, [expert_gate, expert_up, expert_down], [dense_gate, dense_up, dense_down], units
    )

    for step, offsets in enumerate(stages_of(ep_count)[::-1]):
        if step == 1:
            rows, *weights_near = lax.optimization_barrier((rows, *weights_near))
        rows = jnp.concatenate([rows] + [swap_with(rows, "ep", k) for k in offsets], axis=0)
    rows = jnp.stack([rows, swap_with(rows, "tp", 1)])
    total_rows = rows.size // rows.shape[-1]
    rows = rows.reshape(total_rows, width + side_width)

    keep, sent = ffn(rows, weights_near, experts, units)

    mixed = (keep + swap_with(sent, "tp", 1).astype(F32)).reshape(ep_count, outer, own, width)
    bit = outer // 2
    while bit >= 1:
        received = swap_with(mixed[:, bit : 2 * bit].astype(BF16), "tp", 2 * bit)
        mixed = mixed[:, :bit] + received.astype(F32)
        bit //= 2
    mixed = mixed[:, 0]
    for offsets in stages_of(ep_count):
        mixed = mixed.reshape((len(offsets) + 1, -1) + mixed.shape[1:])
        pieces = [swap_with(mixed[i + 1].astype(BF16), "ep", k) for i, k in enumerate(offsets)]
        mixed = mixed[0] + sum(p.astype(F32) for p in pieces)
    return (residual[:own] + mixed[0]).astype(BF16)


def solution(mesh):
    return jax.shard_map(
        on_device,
        mesh=mesh,
        in_specs=(
            P("ep", None),
            P(),
            P(None, "tp"),
            P(None, "tp"),
            P(None, "tp"),
            P(None, "tp"),
            P("tp"),
            P("tp", None),
            P("ep", None, "tp", None),
            P("ep", "tp", None),
            P("ep"),
            P(),
            P("ep", None),
            P("ep", None),
            P("ep", None, "tp"),
            P("ep", None, "tp"),
            P("ep", "tp", None),
            P(None, "ep"),
            P(None, "ep"),
            P("ep", None),
            P(),
        ),
        out_specs=P(("ep", "tp"), None),
        check_vma=False,
    )
```

time: 68.8 us -> 52.8 us (0.77)
  matrix products: 19 us -> 0 us
  Pallas kernels: 0 us -> 12.2 us
  other arithmetic: 4.79 us -> 1.45 us
  local copies, waits for them, and re-layouts: 3.18 us -> 0.54 us
  waiting for transfers between devices: 23.6 us -> 21.6 us
  starting transfers between devices: 17.5 us -> 16.7 us
    dot_general x12 -> x0, matrix products: 19 us -> none  [the longest x2 6.49 us: on_device(): jnp.dot(a, d, preferred_element_type=F32)]
    pallas_call x0 -> x3, Pallas kernels: none -> 12.2 us  [the longest x1 7.37 us: attention(): pl.pallas_call(functools.partial(attention_kernel, own, heads), out_shape...]
    ppermute x13, waiting for transfers between devices: 23.6 us -> 21.6 us  [swap_with(): return lax.ppermute(values, axis, [(i, i ^ offset) for i in range(count)])]
    slice x4 -> x0, local copies, waits for them, and re-layouts: 1.31 us -> none  [the longest x3 1.13 us: on_device(): mixed = mixed[0] + swap_with(mixed[1].astype(BF16), 'tp', 1).astype(F32)]
    reduce_sum x2 -> x1, other arithmetic: 1.24 us -> 0.13 us  [rms_scaled(): jnp.mean(values * values, axis=-1, keepdims=True) + EPS]
    sub x2 -> x0, other arithmetic: 1.04 us -> none  [the longest x1 0.67 us: attention(): lengths - 1]
    convert_element_type x3 -> x2, local copies, waits for them, and re-layouts: 0.93 us -> 0.05 us  [the longest x1 0.03 us: on_device(): total = rounded.astype(F32) + received.reshape(total.shape).astype(F32)]
    ppermute x13, starting transfers between devices: 17.5 us -> 16.7 us  [swap_with(): return lax.ppermute(values, axis, [(i, i ^ offset) for i in range(count)])]
  transfers between devices with their start and end apart: 13 -> 13, of which waited for: 11 -> 11; matrix products, arithmetic and copies ran while one was open for 1% -> 0% of each run, Pallas kernels for 0% -> 6%
where the time goes in v2:
time: 52.8 us; the launch traced here: 52.7 us
  waiting for transfers between devices  21.6 us (41%)
  starting transfers between devices  16.7 us (32%)
  Pallas kernels  12.2 us (23%)
  other arithmetic  1.45 us (3%)
  local copies, waits for them, and re-layouts  0.54 us (1%)
    ppermute x13, waiting for transfers between devices, swap_with(): return lax.ppermute(values, axis, [(i, i ^ offset) for i in range(count)])  21.6 us
    ppermute x13, starting transfers between devices, swap_with(): return lax.ppermute(values, axis, [(i, i ^ offset) for i in range(count)])  16.7 us
    pallas_call x1, Pallas kernels, attention(): pl.pallas_call(functools.partial(attention_kernel, own, heads), out_shape...  7.37 us
    pallas_call x1, Pallas kernels, load_weights(): pl.pallas_call(functools.partial(load_kernel, count, units), out_shape=tu...  3.29 us
    pallas_call x1, Pallas kernels, ffn(): pl.pallas_call(functools.partial(ffn_kernel, experts, part), out_shape=(j...  1.55 us
  transfers between devices with their start and end apart: 13, of which 11 were waited for; matrix products, arithmetic and copies ran while one was open for 0% of the time, Pallas kernels for 6%

profile of v2, /device:TPU:0, one launch (start us, length us, event | category | flops | bytes accessed | tf_op | source)
XLA Modules:
  0.0 52.7 jit_solution(2521796195362377015)
XLA Ops:
  0.0 0.0 copy-start.2
  0.0 0.0 copy-start.3
  0.0 0.0 copy-start
  0.0 0.0 copy-start.1
  0.0 7.4 %attention.1 = (f32[8,2048]{1,0:T(8,128)S(1)}, bf16[8,2048]{1,0:T(8,128)(2,1)S(1)}, f32[8,2048]{1,0:T(8,128)S(1)}) custom-call(s32[16]{0:T(128)} %lengths_hbm.1, f32[2]{0:T(128)} %bias_hbm.1, bf16[16,2048]{1,0:T(8,128)(2,1)} %tokens_hbm.1, f32[1,2048]{1,0:T(1,128)} %bitcast.39, bf16[2048,128]{1,0:T(8,128)(2,1)} %query_hbm.1, bf16[64,2048]{1,0:T(8,128)(2,1)} %bitcast.35, ...), custom_call_target="tpu_custom_call" | custom-call | tf_op jit(solution)/shard_map/attention/pallas_call | solution.py:211
  7.4 0.6 %collective-permute-start = (bf16[8,2048]{1,0:T(8,128)(2,1)S(1)}, bf16[8,2048]{1,0:T(8,128)(2,1)S(1)}, u32[]{:S(2)}, u32[]{:S(2)}) collective-permute-start(bf16[8,2048]{1,0:T(8,128)(2,1)S(1)} %get-tuple-element.23), channel_id=1, source_target_pairs={{0,1},{1,0},{2,3},{3,2},{4,5},{5,4},{6,7},{7,6},{8,9},{9,8},{10,11... | collective-permute-start | bytes 98312 | tf_op jit(solution)/shard_map/ppermute | solution.py:36
  7.9 0.0 copy-done.2
  7.9 0.0 copy-done.3
  8.0 0.1 copy.27
  8.0 0.8 %collective-permute-done = bf16[8,2048]{1,0:T(8,128)(2,1)S(1)} collective-permute-done((bf16[8,2048]{1,0:T(8,128)(2,1)S(1)}, bf16[8,2048]{1,0:T(8,128)(2,1)S(1)}, u32[]{:S(2)}, u32[]{:S(2)}) %collective-permute-start) | collective-permute-done | bytes 32800 | tf_op jit(solution)/shard_map/ppermute | solution.py:36
  8.8 2.9 %collective-permute-start.1 = (bf16[2,4,2048]{2,1,0:T(4,128)(2,1)S(1)}, bf16[2,4,2048]{2,1,0:T(4,128)(2,1)S(1)}, u32[]{:S(2)}, u32[]{:S(2)}) collective-permute-start(bf16[2,4,2048]{2,1,0:T(4,128)(2,1)S(1)} %convert_element_type.81), channel_id=1, source_target_pairs={{0,2},{1,3},{2,0},{3,1},{4,6},{5,7},{6,4},{7,5},{8,10},{9,11},{10,... | collective-permute-start | bytes 98312 | tf_op jit(solution)/shard_map/ppermute | solution.py:36
  11.8 1.9 %collective-permute-done.1 = bf16[2,4,2048]{2,1,0:T(4,128)(2,1)S(1)} collective-permute-done((bf16[2,4,2048]{2,1,0:T(4,128)(2,1)S(1)}, bf16[2,4,2048]{2,1,0:T(4,128)(2,1)S(1)}, u32[]{:S(2)}, u32[]{:S(2)}) %collective-permute-start.1) | collective-permute-done | bytes 32800 | tf_op jit(solution)/shard_map/ppermute | solution.py:36
  13.7 0.1 multiply_reduce_fusion.1
  13.8 0.0 copy-done
  13.8 0.0 copy-done.1
  13.8 0.2 multiply_reduce_fusion
  14.1 0.1 copy.28
  14.1 0.1 reduce-precision_convert_fusion
  14.2 0.1 fusion.10.after_ref
  14.3 4.1 %collective-permute-start.4 = (bf16[1,8,2176]{2,1,0:T(8,128)(2,1)S(1)}, bf16[1,8,2176]{2,1,0:T(8,128)(2,1)S(1)}, u32[]{:S(2)}, u32[]{:S(2)}) collective-permute-start(bf16[1,8,2176]{2,1,0:T(8,128)(2,1)S(1)} %maximum_bitcast_fusion), channel_id=1, source_target_pairs={{0,24},{4,28},{8,16},{12,20},{16,8},{20,12},{24,0},{28,4},{1,25},{... | collective-permute-start | bytes 104456 | tf_op jit(solution)/shard_map/ppermute | solution.py:36
  18.4 0.0 collective-permute-start.3
  18.4 0.6 %collective-permute-start.2 = (bf16[1,8,2176]{2,1,0:T(8,128)(2,1)S(1)}, bf16[1,8,2176]{2,1,0:T(8,128)(2,1)S(1)}, u32[]{:S(2)}, u32[]{:S(2)}) collective-permute-start(bf16[1,8,2176]{2,1,0:T(8,128)(2,1)S(1)} %maximum_bitcast_fusion), channel_id=1, source_target_pairs={{0,8},{4,12},{8,0},{12,4},{16,24},{20,28},{24,16},{28,20},{1,9},{5... | collective-permute-start | bytes 104456 | tf_op jit(solution)/shard_map/ppermute | solution.py:36
  19.1 3.3 %load.1 = (bf16[1,2048,512]{2,1,0:T(8,128)(2,1)S(1)}, bf16[1,2048,512]{2,1,0:T(8,128)(2,1)S(1)}, bf16[1,512,2048]{2,1,0:T(8,128)(2,1)S(1)}, bf16[2048,256]{1,0:T(8,128)(2,1)S(1)}, bf16[128,2048]{1,0:T(8,128)(2,1)S(1)}) custom-call(bf16[8,128]{1,0:T(8,128)(2,1)S(1)} %fusion.10.after_ref, bf16[1,2048,512]{2,1,0:T(8,128)(2,1)} %refs_0_.1, ...), custom_call_target="tpu_custom_call" | custom-call | flops 4000000000 | bytes 33554432 | tf_op jit(solution)/shard_map/load/pallas_call | solution.py:274
  22.4 0.0 collective-permute-done.4
  22.4 0.9 %collective-permute-done.3 = bf16[1,8,2176]{2,1,0:T(8,128)(2,1)S(1)} collective-permute-done((bf16[1,8,2176]{2,1,0:T(8,128)(2,1)S(1)}, bf16[1,8,2176]{2,1,0:T(8,128)(2,1)S(1)}, u32[]{:S(2)}, u32[]{:S(2)}) %collective-permute-start.3) | collective-permute-done | bytes 34848 | tf_op jit(solution)/shard_map/ppermute | solution.py:36
  23.3 0.0 collective-permute-done.2
  23.3 1.6 %collective-permute-start.5 = (bf16[4,8,2176]{2,1,0:T(8,128)(2,1)S(1)}, bf16[4,8,2176]{2,1,0:T(8,128)(2,1)S(1)}, u32[]{:S(2)}, u32[]{:S(2)}) collective-permute-start(bf16[4,8,2176]{2,1,0:T(8,128)(2,1)S(1)} %pad_maximum_fusion.1), channel_id=1, source_target_pairs={{0,4},{4,0},{8,12},{12,8},{16,20},{20,16},{24,28},{28,24},{1,5},{5... | collective-permute-start | bytes 417800 | tf_op jit(solution)/shard_map/ppermute | solution.py:36
  24.9 3.6 %collective-permute-done.5 = bf16[4,8,2176]{2,1,0:T(8,128)(2,1)S(1)} collective-permute-done((bf16[4,8,2176]{2,1,0:T(8,128)(2,1)S(1)}, bf16[4,8,2176]{2,1,0:T(8,128)(2,1)S(1)}, u32[]{:S(2)}, u32[]{:S(2)}) %collective-permute-start.5) | collective-permute-done | bytes 139296 | tf_op jit(solution)/shard_map/ppermute | solution.py:36
  28.4 0.1 collective-permute-start.6
  28.5 1.5 %collective-permute-done.6 = bf16[8,8,2176]{2,1,0:T(8,128)(2,1)S(1)} collective-permute-done((bf16[8,8,2176]{2,1,0:T(8,128)(2,1)S(1)}, bf16[8,8,2176]{2,1,0:T(8,128)(2,1)S(1)}, u32[]{:S(2)}, u32[]{:S(2)}) %collective-permute-start.6) | collective-permute-done | bytes 278560 | tf_op jit(solution)/shard_map/ppermute | solution.py:36
  30.1 0.1 pad_maximum_fusion
  30.1 1.6 %ffn.1 = (f32[64,2048]{1,0:T(8,128)S(1)}, bf16[64,2048]{1,0:T(8,128)(2,1)S(1)}) custom-call(bf16[128,2176]{1,0:T(8,128)(2,1)S(1)} %bitcast.31, bf16[1,2048,512]{2,1,0:T(8,128)(2,1)S(1)} %get-tuple-element.30.gate_ref, bf16[1,2048,512]{2,1,0:T(8,128)(2,1)S(1)} %get-tuple-element.31.up_ref, bf16[1,512,2048]{2,1,0:T(8,128)(2,1)S(1)} %get-tuple-element.32.down_ref, ...), custom_call_target="tpu_custom_call" | custom-call | tf_op jit(solution)/shard_map/ffn/pallas_call | solution.py:348
  31.7 0.2 collective-permute-start.7
  31.9 1.4 %collective-permute-done.7 = bf16[64,2048]{1,0:T(8,128)(2,1)S(1)} collective-permute-done((bf16[64,2048]{1,0:T(8,128)(2,1)S(1)}, bf16[64,2048]{1,0:T(8,128)(2,1)S(1)}, u32[]{:S(2)}, u32[]{:S(2)}) %collective-permute-start.7) | collective-permute-done | bytes 262176 | tf_op jit(solution)/shard_map/ppermute | solution.py:36
  33.3 0.1 reshape.83
  33.6 1.6 %collective-permute-start.8 = (bf16[8,1,4,2048]{3,2,0,1:T(4,128)(2,1)S(1)}, bf16[8,1,4,2048]{3,2,0,1:T(4,128)(2,1)S(1)}, u32[]{:S(2)}, u32[]{:S(2)}) collective-permute-start(bf16[8,1,4,2048]{3,2,0,1:T(4,128)(2,1)S(1)} %copy.35), channel_id=1, source_target_pairs={{0,2},{1,3},{2,0},{3,1},{4,6},{5,7},{6,4},{7,5},{8,10},{9,11},{10,... | collective-permute-start | bytes 393224 | tf_op jit(solution)/shard_map/ppermute | solution.py:36
  35.2 4.0 %collective-permute-done.8 = bf16[8,1,4,2048]{3,2,0,1:T(4,128)(2,1)S(1)} collective-permute-done((bf16[8,1,4,2048]{3,2,0,1:T(4,128)(2,1)S(1)}, bf16[8,1,4,2048]{3,2,0,1:T(4,128)(2,1)S(1)}, u32[]{:S(2)}, u32[]{:S(2)}) %collective-permute-start.8) | collective-permute-done | bytes 131104 | tf_op jit(solution)/shard_map/ppermute | solution.py:36
  39.2 0.1 copy_add_fusion
  39.3 1.6 %collective-permute-start.9 = (bf16[4,4,2048]{2,1,0:T(4,128)(2,1)S(1)}, bf16[4,4,2048]{2,1,0:T(4,128)(2,1)S(1)}, u32[]{:S(2)}, u32[]{:S(2)}) collective-permute-start(bf16[4,4,2048]{2,1,0:T(4,128)(2,1)S(1)} %fusion.1), channel_id=1, source_target_pairs={{0,4},{4,0},{8,12},{12,8},{16,20},{20,16},{24,28},{28,24},{1,5},{5... | collective-permute-start | bytes 196616 | tf_op jit(solution)/shard_map/ppermute | solution.py:36
  40.9 2.8 %collective-permute-done.9 = bf16[4,4,2048]{2,1,0:T(4,128)(2,1)S(1)} collective-permute-done((bf16[4,4,2048]{2,1,0:T(4,128)(2,1)S(1)}, bf16[4,4,2048]{2,1,0:T(4,128)(2,1)S(1)}, u32[]{:S(2)}, u32[]{:S(2)}) %collective-permute-start.9) | collective-permute-done | bytes 65568 | tf_op jit(solution)/shard_map/ppermute | solution.py:36
  43.7 0.6 %collective-permute-start.10 = (bf16[1,4,2048]{2,1,0:T(4,128)(2,1)S(1)}, bf16[1,4,2048]{2,1,0:T(4,128)(2,1)S(1)}, u32[]{:S(2)}, u32[]{:S(2)}) collective-permute-start(bf16[1,4,2048]{2,1,0:T(4,128)(2,1)S(1)} %get-tuple-element.43), channel_id=1, source_target_pairs={{0,8},{4,12},{8,0},{12,4},{16,24},{20,28},{24,16},{28,20},{1,9},{5... | collective-permute-start | bytes 49160 | tf_op jit(solution)/shard_map/ppermute | solution.py:36
  44.3 3.0 %collective-permute-start.12 = (bf16[1,4,2048]{2,1,0:T(4,128)(2,1)S(1)}, bf16[1,4,2048]{2,1,0:T(4,128)(2,1)S(1)}, u32[]{:S(2)}, u32[]{:S(2)}) collective-permute-start(bf16[1,4,2048]{2,1,0:T(4,128)(2,1)S(1)} %get-tuple-element.44), channel_id=1, source_target_pairs={{0,24},{4,28},{8,16},{12,20},{16,8},{20,12},{24,0},{28,4},{1,25},{... | collective-permute-start | bytes 49160 | tf_op jit(solution)/shard_map/ppermute | solution.py:36
  47.3 0.0 collective-permute-start.11
  47.3 0.2 collective-permute-done.10
  47.5 2.3 %collective-permute-done.12 = bf16[1,4,2048]{2,1,0:T(4,128)(2,1)S(1)} collective-permute-done((bf16[1,4,2048]{2,1,0:T(4,128)(2,1)S(1)}, bf16[1,4,2048]{2,1,0:T(4,128)(2,1)S(1)}, u32[]{:S(2)}, u32[]{:S(2)}) %collective-permute-start.12) | collective-permute-done | bytes 16416 | tf_op jit(solution)/shard_map/ppermute | solution.py:36
  49.9 2.2 %collective-permute-done.11 = bf16[1,4,2048]{2,1,0:T(4,128)(2,1)S(1)} collective-permute-done((bf16[1,4,2048]{2,1,0:T(4,128)(2,1)S(1)}, bf16[1,4,2048]{2,1,0:T(4,128)(2,1)S(1)}, u32[]{:S(2)}, u32[]{:S(2)}) %collective-permute-start.11) | collective-permute-done | bytes 16416 | tf_op jit(solution)/shard_map/ppermute | solution.py:36
  52.1 0.6 %fusion.4 = bf16[4,2048]{1,0:T(4,128)(2,1)} fusion(f32[4,4,2048]{2,1,0:T(4,128)S(1)} %get-tuple-element.38, f32[8,2048]{1,0:T(8,128)S(1)} %get-tuple-element.42, bf16[1,4,2048]{2,1,0:T(4,128)(2,1)S(1)} %collective-permute-done.12, bf16[1,4,2048]{2,1,0:T(4,128)(2,1)S(1)} %collective-permute-done.11, bf16[1,4,2048]{2,1,0:T(4,128)(2,1)S(1)} %collective-permute-done.10), kind=kLoop, calls=%fused_computation.19 | loop fusion | flops 65536 | bytes 131072 | tf_op jit(solution)/shard_map/convert_element_type | solution.py:451
  (20 shorter events, 0.4 us)
Async XLA Ops:
  0.0 7.9 %copy-start.2 = (f32[16,4]{0,1:T(4,128)S(1)}, f32[16,4]{0,1:T(4,128)}, u32[]{:S(2)}) copy-start(f32[16,4]{0,1:T(4,128)} %param.34) | copy-start | bytes 772
  0.0 7.9 %copy-start.3 = (s32[16,4]{0,1:T(4,128)S(1)}, s32[16,4]{0,1:T(4,128)}, u32[]{:S(2)}) copy-start(s32[16,4]{0,1:T(4,128)} %param.33) | copy-start | bytes 772
  0.0 13.8 %copy-start = (f32[2048]{0:T(1024)S(1)}, f32[2048]{0:T(1024)}, u32[]{:S(2)}) copy-start(f32[2048]{0:T(1024)} %param.41) | copy-start | bytes 24580
  0.0 13.8 %copy-start.1 = (f32[2048]{0:T(1024)S(1)}, f32[2048]{0:T(1024)}, u32[]{:S(2)}) copy-start(f32[2048]{0:T(1024)} %param.32) | copy-start | bytes 24580
  7.4 1.4 %collective-permute-start = (bf16[8,2048]{1,0:T(8,128)(2,1)S(1)}, bf16[8,2048]{1,0:T(8,128)(2,1)S(1)}, u32[]{:S(2)}, u32[]{:S(2)}) collective-permute-start(bf16[8,2048]{1,0:T(8,128)(2,1)S(1)} %get-tuple-element.23), channel_id=1, source_target_pairs={{0,1},{1,0},{2,3},{3,2},{4,5},{5,4},{6,7},{7,6},{8,9},{9,8},{10,11... | collective-permute-start | bytes 98312 | tf_op jit(solution)/shard_map/ppermute | solution.py:36
  8.8 4.8 %collective-permute-start.1 = (bf16[2,4,2048]{2,1,0:T(4,128)(2,1)S(1)}, bf16[2,4,2048]{2,1,0:T(4,128)(2,1)S(1)}, u32[]{:S(2)}, u32[]{:S(2)}) collective-permute-start(bf16[2,4,2048]{2,1,0:T(4,128)(2,1)S(1)} %convert_element_type.81), channel_id=1, source_target_pairs={{0,2},{1,3},{2,0},{3,1},{4,6},{5,7},{6,4},{7,5},{8,10},{9,11},{10,... | collective-permute-start | bytes 98312 | tf_op jit(solution)/shard_map/ppermute | solution.py:36
  14.3 8.1 %collective-permute-start.4 = (bf16[1,8,2176]{2,1,0:T(8,128)(2,1)S(1)}, bf16[1,8,2176]{2,1,0:T(8,128)(2,1)S(1)}, u32[]{:S(2)}, u32[]{:S(2)}) collective-permute-start(bf16[1,8,2176]{2,1,0:T(8,128)(2,1)S(1)} %maximum_bitcast_fusion), channel_id=1, source_target_pairs={{0,24},{4,28},{8,16},{12,20},{16,8},{20,12},{24,0},{28,4},{1,25},{... | collective-permute-start | bytes 104456 | tf_op jit(solution)/shard_map/ppermute | solution.py:36
  18.4 4.8 %collective-permute-start.3 = (bf16[1,8,2176]{2,1,0:T(8,128)(2,1)S(1)}, bf16[1,8,2176]{2,1,0:T(8,128)(2,1)S(1)}, u32[]{:S(2)}, u32[]{:S(2)}) collective-permute-start(bf16[1,8,2176]{2,1,0:T(8,128)(2,1)S(1)} %maximum_bitcast_fusion), channel_id=1, source_target_pairs={{0,16},{4,20},{8,24},{12,28},{16,0},{20,4},{24,8},{28,12},{1,17},{... | collective-permute-start | bytes 104456 | tf_op jit(solution)/shard_map/ppermute | solution.py:36
  18.4 4.8 %collective-permute-start.2 = (bf16[1,8,2176]{2,1,0:T(8,128)(2,1)S(1)}, bf16[1,8,2176]{2,1,0:T(8,128)(2,1)S(1)}, u32[]{:S(2)}, u32[]{:S(2)}) collective-permute-start(bf16[1,8,2176]{2,1,0:T(8,128)(2,1)S(1)} %maximum_bitcast_fusion), channel_id=1, source_target_pairs={{0,8},{4,12},{8,0},{12,4},{16,24},{20,28},{24,16},{28,20},{1,9},{5... | collective-permute-start | bytes 104456 | tf_op jit(solution)/shard_map/ppermute | solution.py:36
  23.3 5.1 %collective-permute-start.5 = (bf16[4,8,2176]{2,1,0:T(8,128)(2,1)S(1)}, bf16[4,8,2176]{2,1,0:T(8,128)(2,1)S(1)}, u32[]{:S(2)}, u32[]{:S(2)}) collective-permute-start(bf16[4,8,2176]{2,1,0:T(8,128)(2,1)S(1)} %pad_maximum_fusion.1), channel_id=1, source_target_pairs={{0,4},{4,0},{8,12},{12,8},{16,20},{20,16},{24,28},{28,24},{1,5},{5... | collective-permute-start | bytes 417800 | tf_op jit(solution)/shard_map/ppermute | solution.py:36
  28.4 1.6 %collective-permute-start.6 = (bf16[8,8,2176]{2,1,0:T(8,128)(2,1)S(1)}, bf16[8,8,2176]{2,1,0:T(8,128)(2,1)S(1)}, u32[]{:S(2)}, u32[]{:S(2)}) collective-permute-start(bf16[8,8,2176]{2,1,0:T(8,128)(2,1)S(1)} %constant_dynamic-update-slice_fusion), channel_id=1, source_target_pairs={{0,1},{1,0},{2,3},{3,2},{4,5},{5,4},{6,7},{7,6},{8,9},{9,8},{10,11... | collective-permute-start | bytes 835592 | tf_op jit(solution)/shard_map/ppermute | solution.py:36
  31.7 1.6 %collective-permute-start.7 = (bf16[64,2048]{1,0:T(8,128)(2,1)S(1)}, bf16[64,2048]{1,0:T(8,128)(2,1)S(1)}, u32[]{:S(2)}, u32[]{:S(2)}) collective-permute-start(bf16[64,2048]{1,0:T(8,128)(2,1)S(1)} %get-tuple-element.36), channel_id=1, source_target_pairs={{0,1},{1,0},{2,3},{3,2},{4,5},{5,4},{6,7},{7,6},{8,9},{9,8},{10,11... | collective-permute-start | bytes 786440 | tf_op jit(solution)/shard_map/ppermute | solution.py:36
  33.6 5.6 %collective-permute-start.8 = (bf16[8,1,4,2048]{3,2,0,1:T(4,128)(2,1)S(1)}, bf16[8,1,4,2048]{3,2,0,1:T(4,128)(2,1)S(1)}, u32[]{:S(2)}, u32[]{:S(2)}) collective-permute-start(bf16[8,1,4,2048]{3,2,0,1:T(4,128)(2,1)S(1)} %copy.35), channel_id=1, source_target_pairs={{0,2},{1,3},{2,0},{3,1},{4,6},{5,7},{6,4},{7,5},{8,10},{9,11},{10,... | collective-permute-start | bytes 393224 | tf_op jit(solution)/shard_map/ppermute | solution.py:36
  39.3 4.3 %collective-permute-start.9 = (bf16[4,4,2048]{2,1,0:T(4,128)(2,1)S(1)}, bf16[4,4,2048]{2,1,0:T(4,128)(2,1)S(1)}, u32[]{:S(2)}, u32[]{:S(2)}) collective-permute-start(bf16[4,4,2048]{2,1,0:T(4,128)(2,1)S(1)} %fusion.1), channel_id=1, source_target_pairs={{0,4},{4,0},{8,12},{12,8},{16,20},{20,16},{24,28},{28,24},{1,5},{5... | collective-permute-start | bytes 196616 | tf_op jit(solution)/shard_map/ppermute | solution.py:36
  43.7 3.8 %collective-permute-start.10 = (bf16[1,4,2048]{2,1,0:T(4,128)(2,1)S(1)}, bf16[1,4,2048]{2,1,0:T(4,128)(2,1)S(1)}, u32[]{:S(2)}, u32[]{:S(2)}) collective-permute-start(bf16[1,4,2048]{2,1,0:T(4,128)(2,1)S(1)} %get-tuple-element.43), channel_id=1, source_target_pairs={{0,8},{4,12},{8,0},{12,4},{16,24},{20,28},{24,16},{28,20},{1,9},{5... | collective-permute-start | bytes 49160 | tf_op jit(solution)/shard_map/ppermute | solution.py:36
  44.3 5.5 %collective-permute-start.12 = (bf16[1,4,2048]{2,1,0:T(4,128)(2,1)S(1)}, bf16[1,4,2048]{2,1,0:T(4,128)(2,1)S(1)}, u32[]{:S(2)}, u32[]{:S(2)}) collective-permute-start(bf16[1,4,2048]{2,1,0:T(4,128)(2,1)S(1)} %get-tuple-element.44), channel_id=1, source_target_pairs={{0,24},{4,28},{8,16},{12,20},{16,8},{20,12},{24,0},{28,4},{1,25},{... | collective-permute-start | bytes 49160 | tf_op jit(solution)/shard_map/ppermute | solution.py:36
  47.3 4.8 %collective-permute-start.11 = (bf16[1,4,2048]{2,1,0:T(4,128)(2,1)S(1)}, bf16[1,4,2048]{2,1,0:T(4,128)(2,1)S(1)}, u32[]{:S(2)}, u32[]{:S(2)}) collective-permute-start(bf16[1,4,2048]{2,1,0:T(4,128)(2,1)S(1)} %get-tuple-element.45), channel_id=1, source_target_pairs={{0,16},{4,20},{8,24},{12,28},{16,0},{20,4},{24,8},{28,12},{1,17},{... | collective-permute-start | bytes 49160 | tf_op jit(solution)/shard_map/ppermute | solution.py:36

commit v3 on v2

--- a/solution.py
+++ b/solution.py
@@ -34,6 +34,16 @@
 def swap_with(values, axis, offset):
     count = lax.axis_size(axis)
     return lax.ppermute(values, axis, [(i, i ^ offset) for i in range(count)])
+
+
+def swap_both(values, ep_offset, tp_offset):
+    ep_count, tp_count = lax.axis_size("ep"), lax.axis_size("tp")
+    pairs = [
+        (e * tp_count + t, (e ^ ep_offset) * tp_count + (t ^ tp_offset))
+        for e in range(ep_count)
+        for t in range(tp_count)
+    ]
+    return lax.ppermute(values, ("ep", "tp"), pairs)
 
 
 def stages_of(count):
@@ -92,15 +102,15 @@
     ]
     for copy in copies[:-1]:
         copy.start()
+
+    def one_hot(condition):
+        return jnp.where(condition, 1.0, 0.0).astype(BF16)
+
+    copies[0].wait()
+    copies[1].wait()
     for copy in cache_copies:
         copy.start()
     copies[-1].start()
-
-    def one_hot(condition):
-        return jnp.where(condition, 1.0, 0.0).astype(BF16)
-
-    copies[0].wait()
-    copies[1].wait()
     tokens = tokens_buf[...].astype(F32)
     normed = rms_scaled(tokens, gain_buf[...]).astype(BF16)
     spread = one_hot(
@@ -153,6 +163,7 @@
         length = jnp.zeros((span, 1), jnp.int32)
         for i in range(group):
             cache_copies[first + i].wait()
+        for i in range(group):
             found = lax.dot_general(
                 queries[at], cache_buf[first + i], transposed, preferred_element_type=F32
             )
@@ -438,15 +449,20 @@
     keep, sent = ffn(rows, weights_near, experts, units)
 
     mixed = (keep + swap_with(sent, "tp", 1).astype(F32)).reshape(ep_count, outer, own, width)
-    bit = outer // 2
-    while bit >= 1:
-        received = swap_with(mixed[:, bit : 2 * bit].astype(BF16), "tp", 2 * bit)
-        mixed = mixed[:, :bit] + received.astype(F32)
-        bit //= 2
-    mixed = mixed[:, 0]
-    for offsets in stages_of(ep_count):
+    stages = stages_of(ep_count)
+    mixed = mixed.reshape(2, ep_count // 2, outer, own, width)
+    pieces = [
+        swap_both(mixed[e, :, t].astype(BF16), e, 2 * t)
+        for e in range(2)
+        for t in range(outer)
+        if e or t
+    ]
+    mixed = mixed[0, :, 0] + sum(p.astype(F32) for p in pieces)
+    for offsets in stages[1:]:
         mixed = mixed.reshape((len(offsets) + 1, -1) + mixed.shape[1:])
-        pieces = [swap_with(mixed[i + 1].astype(BF16), "ep", k) for i, k in enumerate(offsets)]
+        pieces = [
+            swap_with(mixed[i + 1].astype(BF16), "ep", k) for i, k in reversed(list(enumerate(offsets)))
+        ]
         mixed = mixed[0] + sum(p.astype(F32) for p in pieces)
     return (residual[:own] + mixed[0]).astype(BF16)
 

time: 52.8 us -> 47.5 us (0.90)
  waiting for transfers between devices: 21.6 us -> 17 us
  Pallas kernels: 12.2 us -> 10.3 us
  starting transfers between devices: 16.7 us -> 18.1 us
    ppermute x13 -> x11, waiting for transfers between devices: 21.6 us -> 13.2 us  [swap_with(): return lax.ppermute(values, axis, [(i, i ^ offset) for i in range(count)])]
    ppermute x0 -> x3, waiting for transfers between devices: none -> 3.79 us  [swap_both(): return lax.ppermute(values, ('ep', 'tp'), pairs)]
    ppermute x0 -> x3, starting transfers between devices: none -> 3.55 us  [swap_both(): return lax.ppermute(values, ('ep', 'tp'), pairs)]
    ppermute x13 -> x11, starting transfers between devices: 16.7 us -> 14.5 us  [swap_with(): return lax.ppermute(values, axis, [(i, i ^ offset) for i in range(count)])]
    pallas_call x1, Pallas kernels: 7.37 us -> 5.47 us  [attention(): pl.pallas_call(functools.partial(attention_kernel, own, heads), out_shape...]
  transfers between devices with their start and end apart: 13 -> 14, of which waited for: 11 -> 11; matrix products, arithmetic and copies ran while one was open for 0% -> 0% of each run, Pallas kernels for 6% -> 7%
where the time goes in v3:
time: 47.5 us; the launch traced here: 47.4 us
  starting transfers between devices  18.1 us (38%)
  waiting for transfers between devices  17 us (36%)
  Pallas kernels  10.3 us (22%)
  other arithmetic  1.39 us (3%)
  local copies, waits for them, and re-layouts  0.5 us (1%)
    ppermute x11, starting transfers between devices, swap_with(): return lax.ppermute(values, axis, [(i, i ^ offset) for i in range(count)])  14.5 us
    ppermute x11, waiting for transfers between devices, swap_with(): return lax.ppermute(values, axis, [(i, i ^ offset) for i in range(count)])  13.2 us
    pallas_call x1, Pallas kernels, attention(): pl.pallas_call(functools.partial(attention_kernel, own, heads), out_shape...  5.47 us
    ppermute x3, waiting for transfers between devices, swap_both(): return lax.ppermute(values, ('ep', 'tp'), pairs)  3.79 us
    ppermute x3, starting transfers between devices, swap_both(): return lax.ppermute(values, ('ep', 'tp'), pairs)  3.55 us
    pallas_call x1, Pallas kernels, load_weights(): pl.pallas_call(functools.partial(load_kernel, count, units), out_shape=tu...  3.29 us
    pallas_call x1, Pallas kernels, ffn(): pl.pallas_call(functools.partial(ffn_kernel, experts, part), out_shape=(j...  1.55 us
  transfers between devices with their start and end apart: 14, of which 11 were waited for; matrix products, arithmetic and copies ran while one was open for 0% of the time, Pallas kernels for 7%

profile of v3, /device:TPU:0, one launch (start us, length us, event | category | flops | bytes accessed | tf_op | source)
XLA Modules:
  0.0 47.4 jit_solution(13442275953292510951)
XLA Ops:
  0.0 0.0 copy-start.2
  0.0 0.0 copy-start.3
  0.0 5.5 %attention.1 = (f32[8,2048]{1,0:T(8,128)S(1)}, bf16[8,2048]{1,0:T(8,128)(2,1)S(1)}, f32[8,2048]{1,0:T(8,128)S(1)}) custom-call(s32[16]{0:T(128)} %lengths_hbm.1, f32[2]{0:T(128)} %bias_hbm.1, bf16[16,2048]{1,0:T(8,128)(2,1)} %tokens_hbm.1, f32[1,2048]{1,0:T(1,128)} %bitcast.43, bf16[2048,128]{1,0:T(8,128)(2,1)} %query_hbm.1, bf16[64,2048]{1,0:T(8,128)(2,1)} %bitcast.39, ...), custom_call_target="tpu_custom_call" | custom-call | tf_op jit(solution)/shard_map/attention/pallas_call | solution.py:222
  5.5 0.6 %collective-permute-start = (bf16[8,2048]{1,0:T(8,128)(2,1)S(1)}, bf16[8,2048]{1,0:T(8,128)(2,1)S(1)}, u32[]{:S(2)}, u32[]{:S(2)}) collective-permute-start(bf16[8,2048]{1,0:T(8,128)(2,1)S(1)} %get-tuple-element.23), channel_id=1, source_target_pairs={{0,1},{1,0},{2,3},{3,2},{4,5},{5,4},{6,7},{7,6},{8,9},{9,8},{10,11... | collective-permute-start | bytes 98312 | tf_op jit(solution)/shard_map/ppermute | solution.py:36
  6.0 0.0 copy-done.2
  6.0 0.0 copy-done.3
  6.1 0.1 copy.27
  6.1 0.8 %collective-permute-done = bf16[8,2048]{1,0:T(8,128)(2,1)S(1)} collective-permute-done((bf16[8,2048]{1,0:T(8,128)(2,1)S(1)}, bf16[8,2048]{1,0:T(8,128)(2,1)S(1)}, u32[]{:S(2)}, u32[]{:S(2)}) %collective-permute-start) | collective-permute-done | bytes 32800 | tf_op jit(solution)/shard_map/ppermute | solution.py:36
  6.9 2.9 %collective-permute-start.1 = (bf16[2,4,2048]{2,1,0:T(4,128)(2,1)S(1)}, bf16[2,4,2048]{2,1,0:T(4,128)(2,1)S(1)}, u32[]{:S(2)}, u32[]{:S(2)}) collective-permute-start(bf16[2,4,2048]{2,1,0:T(4,128)(2,1)S(1)} %convert_element_type.91), channel_id=1, source_target_pairs={{0,2},{1,3},{2,0},{3,1},{4,6},{5,7},{6,4},{7,5},{8,10},{9,11},{10,... | collective-permute-start | bytes 98312 | tf_op jit(solution)/shard_map/ppermute | solution.py:36
  9.9 1.9 %collective-permute-done.1 = bf16[2,4,2048]{2,1,0:T(4,128)(2,1)S(1)} collective-permute-done((bf16[2,4,2048]{2,1,0:T(4,128)(2,1)S(1)}, bf16[2,4,2048]{2,1,0:T(4,128)(2,1)S(1)}, u32[]{:S(2)}, u32[]{:S(2)}) %collective-permute-start.1) | collective-permute-done | bytes 32800 | tf_op jit(solution)/shard_map/ppermute | solution.py:36
  11.8 0.1 multiply_reduce_fusion.1
  11.9 0.0 copy-done
  11.9 0.0 copy-done.1
  12.0 0.2 multiply_reduce_fusion
  12.2 0.1 copy.28
  12.2 0.1 reduce-precision_convert_fusion
  12.3 0.1 fusion.9.after_ref
  12.4 4.1 %collective-permute-start.4 = (bf16[1,8,2176]{2,1,0:T(8,128)(2,1)S(1)}, bf16[1,8,2176]{2,1,0:T(8,128)(2,1)S(1)}, u32[]{:S(2)}, u32[]{:S(2)}) collective-permute-start(bf16[1,8,2176]{2,1,0:T(8,128)(2,1)S(1)} %maximum_bitcast_fusion), channel_id=1, source_target_pairs={{0,24},{4,28},{8,16},{12,20},{16,8},{20,12},{24,0},{28,4},{1,25},{... | collective-permute-start | bytes 104456 | tf_op jit(solution)/shard_map/ppermute | solution.py:36
  16.5 0.0 collective-permute-start.3
  16.5 0.6 %collective-permute-start.2 = (bf16[1,8,2176]{2,1,0:T(8,128)(2,1)S(1)}, bf16[1,8,2176]{2,1,0:T(8,128)(2,1)S(1)}, u32[]{:S(2)}, u32[]{:S(2)}) collective-permute-start(bf16[1,8,2176]{2,1,0:T(8,128)(2,1)S(1)} %maximum_bitcast_fusion), channel_id=1, source_target_pairs={{0,8},{4,12},{8,0},{12,4},{16,24},{20,28},{24,16},{28,20},{1,9},{5... | collective-permute-start | bytes 104456 | tf_op jit(solution)/shard_map/ppermute | solution.py:36
  17.2 3.3 %load.1 = (bf16[1,2048,512]{2,1,0:T(8,128)(2,1)S(1)}, bf16[1,2048,512]{2,1,0:T(8,128)(2,1)S(1)}, bf16[1,512,2048]{2,1,0:T(8,128)(2,1)S(1)}, bf16[2048,256]{1,0:T(8,128)(2,1)S(1)}, bf16[128,2048]{1,0:T(8,128)(2,1)S(1)}) custom-call(bf16[8,128]{1,0:T(8,128)(2,1)S(1)} %fusion.9.after_ref, bf16[1,2048,512]{2,1,0:T(8,128)(2,1)} %refs_0_.1, ...), custom_call_target="tpu_custom_call" | custom-call | flops 4000000000 | bytes 33554432 | tf_op jit(solution)/shard_map/load/pallas_call | solution.py:285
  20.5 0.0 collective-permute-done.4
  20.5 0.9 %collective-permute-done.3 = bf16[1,8,2176]{2,1,0:T(8,128)(2,1)S(1)} collective-permute-done((bf16[1,8,2176]{2,1,0:T(8,128)(2,1)S(1)}, bf16[1,8,2176]{2,1,0:T(8,128)(2,1)S(1)}, u32[]{:S(2)}, u32[]{:S(2)}) %collective-permute-start.3) | collective-permute-done | bytes 34848 | tf_op jit(solution)/shard_map/ppermute | solution.py:36
  21.4 0.0 collective-permute-done.2
  21.4 1.6 %collective-permute-start.5 = (bf16[4,8,2176]{2,1,0:T(8,128)(2,1)S(1)}, bf16[4,8,2176]{2,1,0:T(8,128)(2,1)S(1)}, u32[]{:S(2)}, u32[]{:S(2)}) collective-permute-start(bf16[4,8,2176]{2,1,0:T(8,128)(2,1)S(1)} %pad_maximum_fusion.1), channel_id=1, source_target_pairs={{0,4},{4,0},{8,12},{12,8},{16,20},{20,16},{24,28},{28,24},{1,5},{5... | collective-permute-start | bytes 417800 | tf_op jit(solution)/shard_map/ppermute | solution.py:36
  23.0 3.6 %collective-permute-done.5 = bf16[4,8,2176]{2,1,0:T(8,128)(2,1)S(1)} collective-permute-done((bf16[4,8,2176]{2,1,0:T(8,128)(2,1)S(1)}, bf16[4,8,2176]{2,1,0:T(8,128)(2,1)S(1)}, u32[]{:S(2)}, u32[]{:S(2)}) %collective-permute-start.5) | collective-permute-done | bytes 139296 | tf_op jit(solution)/shard_map/ppermute | solution.py:36
  26.5 0.1 collective-permute-start.6
  26.6 1.5 %collective-permute-done.6 = bf16[8,8,2176]{2,1,0:T(8,128)(2,1)S(1)} collective-permute-done((bf16[8,8,2176]{2,1,0:T(8,128)(2,1)S(1)}, bf16[8,8,2176]{2,1,0:T(8,128)(2,1)S(1)}, u32[]{:S(2)}, u32[]{:S(2)}) %collective-permute-start.6) | collective-permute-done | bytes 278560 | tf_op jit(solution)/shard_map/ppermute | solution.py:36
  28.2 0.1 pad_maximum_fusion
  28.2 1.6 %ffn.1 = (f32[64,2048]{1,0:T(8,128)S(1)}, bf16[64,2048]{1,0:T(8,128)(2,1)S(1)}) custom-call(bf16[128,2176]{1,0:T(8,128)(2,1)S(1)} %bitcast.35, bf16[1,2048,512]{2,1,0:T(8,128)(2,1)S(1)} %get-tuple-element.30.gate_ref, bf16[1,2048,512]{2,1,0:T(8,128)(2,1)S(1)} %get-tuple-element.31.up_ref, bf16[1,512,2048]{2,1,0:T(8,128)(2,1)S(1)} %get-tuple-element.32.down_ref, ...), custom_call_target="tpu_custom_call" | custom-call | tf_op jit(solution)/shard_map/ffn/pallas_call | solution.py:359
  29.8 0.2 collective-permute-start.7
  30.0 1.4 %collective-permute-done.7 = bf16[64,2048]{1,0:T(8,128)(2,1)S(1)} collective-permute-done((bf16[64,2048]{1,0:T(8,128)(2,1)S(1)}, bf16[64,2048]{1,0:T(8,128)(2,1)S(1)}, u32[]{:S(2)}, u32[]{:S(2)}) %collective-permute-start.7) | collective-permute-done | bytes 262176 | tf_op jit(solution)/shard_map/ppermute | solution.py:36
  31.4 0.1 reshape_reshape.15
  31.6 0.1 slice_bitcast_fusion.3
  31.7 1.6 %collective-permute-start.8 = (bf16[4,4,2048]{2,1,0:T(4,128)(2,1)S(1)}, bf16[4,4,2048]{2,1,0:T(4,128)(2,1)S(1)}, u32[]{:S(2)}, u32[]{:S(2)}) collective-permute-start(bf16[4,4,2048]{2,1,0:T(4,128)(2,1)S(1)} %get-tuple-element.43), channel_id=1, source_target_pairs={{0,2},{1,3},{2,0},{3,1},{4,6},{5,7},{6,4},{7,5},{8,10},{9,11},{10,... | collective-permute-start | bytes 196616 | tf_op jit(solution)/shard_map/ppermute | solution.py:46
  33.3 1.4 %collective-permute-start.10 = (bf16[4,4,2048]{2,1,0:T(4,128)(2,1)S(1)}, bf16[4,4,2048]{2,1,0:T(4,128)(2,1)S(1)}, u32[]{:S(2)}, u32[]{:S(2)}) collective-permute-start(bf16[4,4,2048]{2,1,0:T(4,128)(2,1)S(1)} %get-tuple-element.44), channel_id=1, source_target_pairs={{0,6},{1,7},{2,4},{3,5},{4,2},{5,3},{6,0},{7,1},{8,14},{9,15},{10,... | collective-permute-start | bytes 196616 | tf_op jit(solution)/shard_map/ppermute | solution.py:46
  34.7 0.5 %collective-permute-start.9 = (bf16[4,4,2048]{2,1,0:T(4,128)(2,1)S(1)}, bf16[4,4,2048]{2,1,0:T(4,128)(2,1)S(1)}, u32[]{:S(2)}, u32[]{:S(2)}) collective-permute-start(bf16[4,4,2048]{2,1,0:T(4,128)(2,1)S(1)} %get-tuple-element.45), channel_id=1, source_target_pairs={{0,4},{1,5},{2,6},{3,7},{4,0},{5,1},{6,2},{7,3},{8,12},{9,13},{10,... | collective-permute-start | bytes 196616 | tf_op jit(solution)/shard_map/ppermute | solution.py:46
  35.2 0.8 %collective-permute-done.8 = bf16[4,4,2048]{2,1,0:T(4,128)(2,1)S(1)} collective-permute-done((bf16[4,4,2048]{2,1,0:T(4,128)(2,1)S(1)}, bf16[4,4,2048]{2,1,0:T(4,128)(2,1)S(1)}, u32[]{:S(2)}, u32[]{:S(2)}) %collective-permute-start.8) | collective-permute-done | bytes 65568 | tf_op jit(solution)/shard_map/ppermute | solution.py:46
  36.0 3.0 %collective-permute-done.10 = bf16[4,4,2048]{2,1,0:T(4,128)(2,1)S(1)} collective-permute-done((bf16[4,4,2048]{2,1,0:T(4,128)(2,1)S(1)}, bf16[4,4,2048]{2,1,0:T(4,128)(2,1)S(1)}, u32[]{:S(2)}, u32[]{:S(2)}) %collective-permute-start.10) | collective-permute-done | bytes 65568 | tf_op jit(solution)/shard_map/ppermute | solution.py:46
  39.0 0.0 collective-permute-done.9
  39.0 0.1 fusion.10
  39.1 3.0 %collective-permute-start.11 = (bf16[1,4,2048]{2,1,0:T(4,128)(2,1)S(1)}, bf16[1,4,2048]{2,1,0:T(4,128)(2,1)S(1)}, u32[]{:S(2)}, u32[]{:S(2)}) collective-permute-start(bf16[1,4,2048]{2,1,0:T(4,128)(2,1)S(1)} %get-tuple-element.46), channel_id=1, source_target_pairs={{0,24},{4,28},{8,16},{12,20},{16,8},{20,12},{24,0},{28,4},{1,25},{... | collective-permute-start | bytes 49160 | tf_op jit(solution)/shard_map/ppermute | solution.py:36
  42.1 0.0 collective-permute-start.13
  42.1 1.5 %collective-permute-start.12 = (bf16[1,4,2048]{2,1,0:T(4,128)(2,1)S(1)}, bf16[1,4,2048]{2,1,0:T(4,128)(2,1)S(1)}, u32[]{:S(2)}, u32[]{:S(2)}) collective-permute-start(bf16[1,4,2048]{2,1,0:T(4,128)(2,1)S(1)} %get-tuple-element.48), channel_id=1, source_target_pairs={{0,16},{4,20},{8,24},{12,28},{16,0},{20,4},{24,8},{28,12},{1,17},{... | collective-permute-start | bytes 49160 | tf_op jit(solution)/shard_map/ppermute | solution.py:36
  43.6 1.2 %collective-permute-done.11 = bf16[1,4,2048]{2,1,0:T(4,128)(2,1)S(1)} collective-permute-done((bf16[1,4,2048]{2,1,0:T(4,128)(2,1)S(1)}, bf16[1,4,2048]{2,1,0:T(4,128)(2,1)S(1)}, u32[]{:S(2)}, u32[]{:S(2)}) %collective-permute-start.11) | collective-permute-done | bytes 16416 | tf_op jit(solution)/shard_map/ppermute | solution.py:36
  44.8 1.1 %collective-permute-done.13 = bf16[1,4,2048]{2,1,0:T(4,128)(2,1)S(1)} collective-permute-done((bf16[1,4,2048]{2,1,0:T(4,128)(2,1)S(1)}, bf16[1,4,2048]{2,1,0:T(4,128)(2,1)S(1)}, u32[]{:S(2)}, u32[]{:S(2)}) %collective-permute-start.13) | collective-permute-done | bytes 16416 | tf_op jit(solution)/shard_map/ppermute | solution.py:36
  45.8 0.9 %collective-permute-done.12 = bf16[1,4,2048]{2,1,0:T(4,128)(2,1)S(1)} collective-permute-done((bf16[1,4,2048]{2,1,0:T(4,128)(2,1)S(1)}, bf16[1,4,2048]{2,1,0:T(4,128)(2,1)S(1)}, u32[]{:S(2)}, u32[]{:S(2)}) %collective-permute-start.12) | collective-permute-done | bytes 16416 | tf_op jit(solution)/shard_map/ppermute | solution.py:36
  46.7 0.6 %fusion.3 = bf16[4,2048]{1,0:T(4,128)(2,1)} fusion(f32[4,4,2048]{2,1,0:T(4,128)S(1)} %get-tuple-element.38, f32[8,2048]{1,0:T(8,128)S(1)} %get-tuple-element.42, bf16[1,4,2048]{2,1,0:T(4,128)(2,1)S(1)} %collective-permute-done.13, bf16[1,4,2048]{2,1,0:T(4,128)(2,1)S(1)} %collective-permute-done.12, bf16[1,4,2048]{2,1,0:T(4,128)(2,1)S(1)} %collective-permute-done.11), kind=kLoop, calls=%fused_computation.18 | loop fusion | flops 65536 | bytes 131072 | tf_op jit(solution)/shard_map/convert_element_type | solution.py:467
  (18 shorter events, 0.2 us)
Async XLA Ops:
  0.0 6.0 %copy-start.2 = (f32[16,4]{0,1:T(4,128)S(1)}, f32[16,4]{0,1:T(4,128)}, u32[]{:S(2)}) copy-start(f32[16,4]{0,1:T(4,128)} %param.34) | copy-start | bytes 772
  0.0 6.0 %copy-start.3 = (s32[16,4]{0,1:T(4,128)S(1)}, s32[16,4]{0,1:T(4,128)}, u32[]{:S(2)}) copy-start(s32[16,4]{0,1:T(4,128)} %param.33) | copy-start | bytes 772
  0.0 11.9 %copy-start = (f32[2048]{0:T(1024)S(1)}, f32[2048]{0:T(1024)}, u32[]{:S(2)}) copy-start(f32[2048]{0:T(1024)} %param.41) | copy-start | bytes 24580
  0.0 11.9 %copy-start.1 = (f32[2048]{0:T(1024)S(1)}, f32[2048]{0:T(1024)}, u32[]{:S(2)}) copy-start(f32[2048]{0:T(1024)} %param.32) | copy-start | bytes 24580
  5.5 1.4 %collective-permute-start = (bf16[8,2048]{1,0:T(8,128)(2,1)S(1)}, bf16[8,2048]{1,0:T(8,128)(2,1)S(1)}, u32[]{:S(2)}, u32[]{:S(2)}) collective-permute-start(bf16[8,2048]{1,0:T(8,128)(2,1)S(1)} %get-tuple-element.23), channel_id=1, source_target_pairs={{0,1},{1,0},{2,3},{3,2},{4,5},{5,4},{6,7},{7,6},{8,9},{9,8},{10,11... | collective-permute-start | bytes 98312 | tf_op jit(solution)/shard_map/ppermute | solution.py:36
  6.9 4.8 %collective-permute-start.1 = (bf16[2,4,2048]{2,1,0:T(4,128)(2,1)S(1)}, bf16[2,4,2048]{2,1,0:T(4,128)(2,1)S(1)}, u32[]{:S(2)}, u32[]{:S(2)}) collective-permute-start(bf16[2,4,2048]{2,1,0:T(4,128)(2,1)S(1)} %convert_element_type.91), channel_id=1, source_target_pairs={{0,2},{1,3},{2,0},{3,1},{4,6},{5,7},{6,4},{7,5},{8,10},{9,11},{10,... | collective-permute-start | bytes 98312 | tf_op jit(solution)/shard_map/ppermute | solution.py:36
  12.4 8.1 %collective-permute-start.4 = (bf16[1,8,2176]{2,1,0:T(8,128)(2,1)S(1)}, bf16[1,8,2176]{2,1,0:T(8,128)(2,1)S(1)}, u32[]{:S(2)}, u32[]{:S(2)}) collective-permute-start(bf16[1,8,2176]{2,1,0:T(8,128)(2,1)S(1)} %maximum_bitcast_fusion), channel_id=1, source_target_pairs={{0,24},{4,28},{8,16},{12,20},{16,8},{20,12},{24,0},{28,4},{1,25},{... | collective-permute-start | bytes 104456 | tf_op jit(solution)/shard_map/ppermute | solution.py:36
  16.5 4.8 %collective-permute-start.3 = (bf16[1,8,2176]{2,1,0:T(8,128)(2,1)S(1)}, bf16[1,8,2176]{2,1,0:T(8,128)(2,1)S(1)}, u32[]{:S(2)}, u32[]{:S(2)}) collective-permute-start(bf16[1,8,2176]{2,1,0:T(8,128)(2,1)S(1)} %maximum_bitcast_fusion), channel_id=1, source_target_pairs={{0,16},{4,20},{8,24},{12,28},{16,0},{20,4},{24,8},{28,12},{1,17},{... | collective-permute-start | bytes 104456 | tf_op jit(solution)/shard_map/ppermute | solution.py:36
  16.5 4.8 %collective-permute-start.2 = (bf16[1,8,2176]{2,1,0:T(8,128)(2,1)S(1)}, bf16[1,8,2176]{2,1,0:T(8,128)(2,1)S(1)}, u32[]{:S(2)}, u32[]{:S(2)}) collective-permute-start(bf16[1,8,2176]{2,1,0:T(8,128)(2,1)S(1)} %maximum_bitcast_fusion), channel_id=1, source_target_pairs={{0,8},{4,12},{8,0},{12,4},{16,24},{20,28},{24,16},{28,20},{1,9},{5... | collective-permute-start | bytes 104456 | tf_op jit(solution)/shard_map/ppermute | solution.py:36
  21.4 5.1 %collective-permute-start.5 = (bf16[4,8,2176]{2,1,0:T(8,128)(2,1)S(1)}, bf16[4,8,2176]{2,1,0:T(8,128)(2,1)S(1)}, u32[]{:S(2)}, u32[]{:S(2)}) collective-permute-start(bf16[4,8,2176]{2,1,0:T(8,128)(2,1)S(1)} %pad_maximum_fusion.1), channel_id=1, source_target_pairs={{0,4},{4,0},{8,12},{12,8},{16,20},{20,16},{24,28},{28,24},{1,5},{5... | collective-permute-start | bytes 417800 | tf_op jit(solution)/shard_map/ppermute | solution.py:36
  26.5 1.6 %collective-permute-start.6 = (bf16[8,8,2176]{2,1,0:T(8,128)(2,1)S(1)}, bf16[8,8,2176]{2,1,0:T(8,128)(2,1)S(1)}, u32[]{:S(2)}, u32[]{:S(2)}) collective-permute-start(bf16[8,8,2176]{2,1,0:T(8,128)(2,1)S(1)} %constant_dynamic-update-slice_fusion), channel_id=1, source_target_pairs={{0,1},{1,0},{2,3},{3,2},{4,5},{5,4},{6,7},{7,6},{8,9},{9,8},{10,11... | collective-permute-start | bytes 835592 | tf_op jit(solution)/shard_map/ppermute | solution.py:36
  29.8 1.6 %collective-permute-start.7 = (bf16[64,2048]{1,0:T(8,128)(2,1)S(1)}, bf16[64,2048]{1,0:T(8,128)(2,1)S(1)}, u32[]{:S(2)}, u32[]{:S(2)}) collective-permute-start(bf16[64,2048]{1,0:T(8,128)(2,1)S(1)} %get-tuple-element.36), channel_id=1, source_target_pairs={{0,1},{1,0},{2,3},{3,2},{4,5},{5,4},{6,7},{7,6},{8,9},{9,8},{10,11... | collective-permute-start | bytes 786440 | tf_op jit(solution)/shard_map/ppermute | solution.py:36
  31.7 4.3 %collective-permute-start.8 = (bf16[4,4,2048]{2,1,0:T(4,128)(2,1)S(1)}, bf16[4,4,2048]{2,1,0:T(4,128)(2,1)S(1)}, u32[]{:S(2)}, u32[]{:S(2)}) collective-permute-start(bf16[4,4,2048]{2,1,0:T(4,128)(2,1)S(1)} %get-tuple-element.43), channel_id=1, source_target_pairs={{0,2},{1,3},{2,0},{3,1},{4,6},{5,7},{6,4},{7,5},{8,10},{9,11},{10,... | collective-permute-start | bytes 196616 | tf_op jit(solution)/shard_map/ppermute | solution.py:46
  33.3 5.8 %collective-permute-start.10 = (bf16[4,4,2048]{2,1,0:T(4,128)(2,1)S(1)}, bf16[4,4,2048]{2,1,0:T(4,128)(2,1)S(1)}, u32[]{:S(2)}, u32[]{:S(2)}) collective-permute-start(bf16[4,4,2048]{2,1,0:T(4,128)(2,1)S(1)} %get-tuple-element.44), channel_id=1, source_target_pairs={{0,6},{1,7},{2,4},{3,5},{4,2},{5,3},{6,0},{7,1},{8,14},{9,15},{10,... | collective-permute-start | bytes 196616 | tf_op jit(solution)/shard_map/ppermute | solution.py:46
  34.7 4.3 %collective-permute-start.9 = (bf16[4,4,2048]{2,1,0:T(4,128)(2,1)S(1)}, bf16[4,4,2048]{2,1,0:T(4,128)(2,1)S(1)}, u32[]{:S(2)}, u32[]{:S(2)}) collective-permute-start(bf16[4,4,2048]{2,1,0:T(4,128)(2,1)S(1)} %get-tuple-element.45), channel_id=1, source_target_pairs={{0,4},{1,5},{2,6},{3,7},{4,0},{5,1},{6,2},{7,3},{8,12},{9,13},{10,... | collective-permute-start | bytes 196616 | tf_op jit(solution)/shard_map/ppermute | solution.py:46
  39.1 5.6 %collective-permute-start.11 = (bf16[1,4,2048]{2,1,0:T(4,128)(2,1)S(1)}, bf16[1,4,2048]{2,1,0:T(4,128)(2,1)S(1)}, u32[]{:S(2)}, u32[]{:S(2)}) collective-permute-start(bf16[1,4,2048]{2,1,0:T(4,128)(2,1)S(1)} %get-tuple-element.46), channel_id=1, source_target_pairs={{0,24},{4,28},{8,16},{12,20},{16,8},{20,12},{24,0},{28,4},{1,25},{... | collective-permute-start | bytes 49160 | tf_op jit(solution)/shard_map/ppermute | solution.py:36
  42.1 3.7 %collective-permute-start.13 = (bf16[1,4,2048]{2,1,0:T(4,128)(2,1)S(1)}, bf16[1,4,2048]{2,1,0:T(4,128)(2,1)S(1)}, u32[]{:S(2)}, u32[]{:S(2)}) collective-permute-start(bf16[1,4,2048]{2,1,0:T(4,128)(2,1)S(1)} %get-tuple-element.47), channel_id=1, source_target_pairs={{0,8},{4,12},{8,0},{12,4},{16,24},{20,28},{24,16},{28,20},{1,9},{5... | collective-permute-start | bytes 49160 | tf_op jit(solution)/shard_map/ppermute | solution.py:36
  42.1 4.6 %collective-permute-start.12 = (bf16[1,4,2048]{2,1,0:T(4,128)(2,1)S(1)}, bf16[1,4,2048]{2,1,0:T(4,128)(2,1)S(1)}, u32[]{:S(2)}, u32[]{:S(2)}) collective-permute-start(bf16[1,4,2048]{2,1,0:T(4,128)(2,1)S(1)} %get-tuple-element.48), channel_id=1, source_target_pairs={{0,16},{4,20},{8,24},{12,28},{16,0},{20,4},{24,8},{28,12},{1,17},{... | collective-permute-start | bytes 49160 | tf_op jit(solution)/shard_map/ppermute | solution.py:36

commit v4 on v3

--- a/solution.py
+++ b/solution.py
@@ -7,16 +7,18 @@
 from jax.experimental.pallas import tpu as pltpu
 from jax.sharding import PartitionSpec as P
 
+
 EPS = 1e-05
 LIMIT = 7.0
 ALPHA = 1.702
 LANES = 128
 ROW_BLOCK = 128
 COLUMN_BLOCK = 512
-FFN_VMEM = 16 * 1024 * 1024
+FFN_VMEM = 4 * 1024 * 1024
 ATTENTION_VMEM = 16 * 1024 * 1024
 LOAD_VMEM = 1024 * 1024
 SEQ_BLOCK = 8
+NORM_VMEM = 2 * 1024 * 1024
 LOAD_COST = 4 * 10**9
 BF16 = jnp.bfloat16
 F32 = jnp.float32
@@ -78,7 +80,7 @@
     tokens_buf, gain_buf, query_buf, pair_buf, forget_buf, cache_buf, gates_buf, out_buf,
     lengths_ref, bias_ref, sems, cache_sems,
 ):
-    seq_count, width = tokens_buf.shape
+    seq_count, _ = tokens_buf.shape
     cache_len, lanes = cache_buf.shape[1:]
     head_dim = lanes // 2
     rows = seq_count * heads
@@ -192,7 +194,7 @@
     attended = jnp.dot(gather, attended, preferred_element_type=F32).astype(BF16)
     copies[9].wait()
     partial = jnp.dot(attended, out_buf[...], preferred_element_type=F32)
-    keep_ref[...] = partial[: seq_count // 2]
+    keep_ref[...] = partial[: seq_count // 2].astype(BF16)
     send_ref[...] = partial[seq_count // 2 :].astype(BF16)
 
 
@@ -222,7 +224,7 @@
     return pl.pallas_call(
         functools.partial(attention_kernel, own, heads),
         out_shape=(
-            pltpu.VMEM((half, width), F32),
+            pltpu.VMEM((half, width), BF16),
             pltpu.VMEM((half, width), BF16),
             pltpu.VMEM((half, width), F32),
         ),
@@ -369,9 +371,80 @@
     )(rows, *weights)
 
 
-def two_halves(values):
-    high = lax.reduce_precision(values, 8, 7)
-    return high.astype(BF16), (values - high).astype(BF16)
+def fold_kernel(keep_ref, received_ref, stay_ref, send_ref):
+    sublane = lax.broadcasted_iota(jnp.int32, (8, keep_ref.shape[1]), 0)
+    for row in range(0, keep_ref.shape[0], 16):
+        first, second = [
+            keep_ref[at : at + 8] + received_ref[at : at + 8].astype(F32) for at in (row, row + 8)
+        ]
+        at = slice(row // 2, row // 2 + 8)
+        stay_ref[at] = jnp.where(sublane < 4, first, pltpu.roll(second, 4, 0)).astype(stay_ref.dtype)
+        send_ref[at] = jnp.where(sublane < 4, pltpu.roll(first, 4, 0), second).astype(BF16)
+
+
+def fold(keep, received, outer, own, stay_type):
+    count, width = keep.shape
+    if outer != 2 or own != 4 or count % 16:
+        total = (keep + received.astype(F32)).reshape(-1, outer, own, width)
+        parts = [total[:, t].reshape(-1, width) for t in range(outer)]
+        return [parts[0].astype(stay_type)] + [p.astype(BF16) for p in parts[1:]]
+    near = pl.BlockSpec(memory_space=pltpu.VMEM)
+    return pl.pallas_call(
+        fold_kernel,
+        out_shape=(
+            pltpu.VMEM((count // 2, width), stay_type),
+            pltpu.VMEM((count // 2, width), BF16),
+        ),
+        in_specs=[near] * 2,
+        out_specs=(near, near),
+        compiler_params=pltpu.CompilerParams(vmem_limit_bytes=NORM_VMEM),
+        name="fold",
+    )(keep, received)
+
+
+def norm_kernel(mix_lane, shifts, *refs):
+    parts, (tokens_ref, gain_ref, dense_mix_ref, side_ref, rows_ref, residual_ref) = (
+        refs[: len(shifts)],
+        refs[len(shifts) :],
+    )
+    norm_body(mix_lane, shifts, parts, tokens_ref, gain_ref, dense_mix_ref, side_ref, rows_ref, residual_ref)
+
+
+def norm_body(mix_lane, shifts, parts, tokens_ref, gain_ref, dense_mix_ref, side_ref, rows_ref, residual_ref):
+    width = tokens_ref.shape[1]
+    sums = {}
+    for shift, part in zip(shifts, parts):
+        sums[shift] = sums.get(shift, 0.0) + part[...].astype(F32)
+    total = sums.pop(0)
+    for shift, part in sums.items():
+        total = total + pltpu.roll(part, shift, 0)
+    residual = tokens_ref[...] + total.astype(BF16).astype(F32)
+    residual_ref[...] = residual
+    hidden = rms_scaled(residual, gain_ref[...]).astype(BF16)
+    rows_ref[:, :width] = hidden
+    mix = jax.nn.sigmoid(jnp.sum(hidden.astype(F32) * dense_mix_ref[...], axis=1, keepdims=True))
+    high = mix.astype(BF16).astype(F32)
+    side = side_ref[...]
+    lane = lax.broadcasted_iota(jnp.int32, side.shape, 1)
+    side = jnp.where(lane == mix_lane, high, side)
+    side = jnp.where(lane == 2 * mix_lane + 1, mix - high, side)
+    rows_ref[:, width:] = side.astype(BF16)
+
+
+def norm_rows(parts, shifts, tokens, gain, dense_mix, side, mix_lane):
+    count, width = tokens.shape
+    near = pl.BlockSpec(memory_space=pltpu.VMEM)
+    return pl.pallas_call(
+        functools.partial(norm_kernel, mix_lane, tuple(shifts)),
+        out_shape=(
+            pltpu.VMEM((count, width + side.shape[1]), BF16),
+            pltpu.VMEM((count, width), F32),
+        ),
+        in_specs=[near] * (len(parts) + 4),
+        out_specs=(near, near),
+        compiler_params=pltpu.CompilerParams(vmem_limit_bytes=NORM_VMEM),
+        name="norm",
+    )(*parts, tokens, gain.reshape(1, width), dense_mix.reshape(1, width), side)
 
 
 def on_device(
@@ -401,7 +474,6 @@
     tp_count = lax.axis_size("tp")
     ep_count = lax.axis_size("ep")
     tp_index = lax.axis_index("tp")
-    ep_index = lax.axis_index("ep")
     own = seq_count // tp_count
     outer = tp_count // 2
     experts = expert_gate.shape[0] * ep_count
@@ -418,51 +490,55 @@
     chosen = routing[:, :, None] == jnp.arange(experts, dtype=jnp.int32)[None, None, :]
     weights = jnp.sum(jnp.where(chosen, route_weight[:, :, None], 0.0), axis=1)
     weights = grouped(weights)[:, 0].reshape(outer * own, experts)
-    total = (keep + swap_with(sent, "tp", 1).astype(F32)).reshape(outer, own, width)
-    for (offset,) in [[1 << b] for b in range((outer - 1).bit_length())]:
-        rounded = total.astype(BF16)
-        received = swap_with(rounded, "tp", 2 * offset)
-        received = received.reshape((outer // (2 * offset), 2, offset, own, width))[:, ::-1]
-        total = rounded.astype(F32) + received.reshape(total.shape).astype(F32)
-    residual = tokens_near + total.astype(BF16).astype(F32).reshape(outer * own, width)
-    hidden_f32 = rms_scaled(residual, norm2_gain)
-    hidden = hidden_f32.astype(BF16)
-    mix_gate = jax.nn.sigmoid(jnp.sum(hidden.astype(F32) * dense_mix, axis=-1, keepdims=True))
-    scales = jnp.concatenate([weights, mix_gate], axis=1)
-    side = jnp.concatenate(two_halves(scales), axis=1)
-    side_width = -(-side.shape[1] // LANES) * LANES
-    side = jnp.pad(side, ((0, 0), (0, side_width - side.shape[1])))
-    rows = jnp.concatenate([hidden, side], axis=1)[None]
+    parts, shifts = [keep], [0]
+    for k in range(1, tp_count):
+        part = swap_with(sent if k & 1 else keep, "tp", k)
+        turn = k >> 1
+        if outer == 2:
+            shifts.append(turn * own)
+        else:
+            blocks = part.reshape(outer, own, width)
+            part = jnp.stack([blocks[j ^ turn] for j in range(outer)]).reshape(part.shape)
+            shifts.append(0)
+        parts.append(part)
+    high = lax.reduce_precision(weights, 8, 7)
+    none = jnp.zeros((outer * own, 1), F32)
+    side = jnp.concatenate([high, none, weights - high, none], axis=1)
+    side = jnp.pad(side, ((0, 0), (0, -side.shape[1] % LANES)))
+    rows, residual = norm_rows(
+        parts, shifts, tokens_near, norm2_gain, dense_mix, side, experts
+    )
     units = dense_gate.shape[1] // tp_count
     weights_near = load_weights(
-        side, [expert_gate, expert_up, expert_down], [dense_gate, dense_up, dense_down], units
-    )
-
-    for step, offsets in enumerate(stages_of(ep_count)[::-1]):
-        if step == 1:
-            rows, *weights_near = lax.optimization_barrier((rows, *weights_near))
-        rows = jnp.concatenate([rows] + [swap_with(rows, "ep", k) for k in offsets], axis=0)
-    rows = jnp.stack([rows, swap_with(rows, "tp", 1)])
-    total_rows = rows.size // rows.shape[-1]
-    rows = rows.reshape(total_rows, width + side_width)
-
+        rows, [expert_gate, expert_up, expert_down], [dense_gate, dense_up, dense_down], units
+    )
+
+    stages = stages_of(ep_count)
+    for offsets in stages[:0:-1]:
+        others = []
+        for k in offsets:
+            others.append(swap_with(rows, "ep", k))
+        rows = jnp.concatenate([rows] + others, axis=0)
+    rows, *weights_near = lax.optimization_barrier((rows, *weights_near))
+
+    rows = jnp.concatenate([rows, swap_with(rows, "ep", 1)], axis=0)
+    rows = jnp.concatenate([rows, swap_with(rows, "tp", 1)], axis=0)
     keep, sent = ffn(rows, weights_near, experts, units)
-
-    mixed = (keep + swap_with(sent, "tp", 1).astype(F32)).reshape(ep_count, outer, own, width)
-    stages = stages_of(ep_count)
-    mixed = mixed.reshape(2, ep_count // 2, outer, own, width)
-    pieces = [
-        swap_both(mixed[e, :, t].astype(BF16), e, 2 * t)
-        for e in range(2)
-        for t in range(outer)
-        if e or t
-    ]
-    mixed = mixed[0, :, 0] + sum(p.astype(F32) for p in pieces)
+    parts = fold(keep, swap_with(sent, "tp", 1), outer, own, F32)
+    half = parts[0].shape[0] // 2
+    mixed = parts[0][:half]
+    pieces = []
+    for e in range(2):
+        for t in range(outer):
+            if e or t:
+                part = parts[t][e * half : (e + 1) * half].astype(BF16)
+                pieces.append(swap_both(part, e, 2 * t))
+    mixed = (mixed + sum(p.astype(F32) for p in pieces)).reshape(ep_count // 2, own, width)
     for offsets in stages[1:]:
         mixed = mixed.reshape((len(offsets) + 1, -1) + mixed.shape[1:])
-        pieces = [
-            swap_with(mixed[i + 1].astype(BF16), "ep", k) for i, k in reversed(list(enumerate(offsets)))
-        ]
+        pieces = []
+        for i, k in enumerate(offsets):
+            pieces.append(swap_with(mixed[i + 1].astype(BF16), "ep", k))
         mixed = mixed[0] + sum(p.astype(F32) for p in pieces)
     return (residual[:own] + mixed[0]).astype(BF16)
 

time: 47.5 us -> 47.8 us (level)
  waiting for transfers between devices: 17 us -> 19.4 us
  starting transfers between devices: 18.1 us -> 16.6 us
  other arithmetic: 1.39 us -> 0.85 us
    ppermute x11 -> x12, waiting for transfers between devices: 13.2 us -> 15.7 us  [swap_with(): return lax.ppermute(values, axis, [(i, i ^ offset) for i in range(count)])]
    ppermute x11 -> x12, starting transfers between devices: 14.5 us -> 13 us  [swap_with(): return lax.ppermute(values, axis, [(i, i ^ offset) for i in range(count)])]
  transfers between devices with their start and end apart: 14 -> 15, of which waited for: 11 -> 11; matrix products, arithmetic and copies ran while one was open for 0% -> 0% of each run, Pallas kernels for 7% -> 7%
where the time goes in v4:
time: 47.8 us; the launch traced here: 47.6 us
  waiting for transfers between devices  19.4 us (41%)
  starting transfers between devices  16.6 us (35%)
  Pallas kernels  10.6 us (22%)
  other arithmetic  0.85 us (2%)
    ppermute x12, waiting for transfers between devices, swap_with(): return lax.ppermute(values, axis, [(i, i ^ offset) for i in range(count)])  15.7 us
    ppermute x12, starting transfers between devices, swap_with(): return lax.ppermute(values, axis, [(i, i ^ offset) for i in range(count)])  13 us
    pallas_call x1, Pallas kernels, attention(): pl.pallas_call(functools.partial(attention_kernel, own, heads), out_shape...  5.47 us
    ppermute x3, waiting for transfers between devices, swap_both(): return lax.ppermute(values, ('ep', 'tp'), pairs)  3.68 us
    ppermute x3, starting transfers between devices, swap_both(): return lax.ppermute(values, ('ep', 'tp'), pairs)  3.55 us
    pallas_call x1, Pallas kernels, load_weights(): pl.pallas_call(functools.partial(load_kernel, count, units), out_shape=tu...  3.29 us
    pallas_call x1, Pallas kernels, ffn(): pl.pallas_call(functools.partial(ffn_kernel, experts, part), out_shape=(j...  1.55 us
  transfers between devices with their start and end apart: 15, of which 11 were waited for; matrix products, arithmetic and copies ran while one was open for 0% of the time, Pallas kernels for 7%

profile of v4, /device:TPU:0, one launch (start us, length us, event | category | flops | bytes accessed | tf_op | source)
XLA Modules:
  0.0 47.6 jit_solution(13345844671688916766)
XLA Ops:
  0.0 0.0 copy-start.2
  0.0 0.0 copy-start.3
  0.0 0.0 copy-start
  0.0 0.0 copy-start.1
  0.0 5.5 %attention.1 = (bf16[8,2048]{1,0:T(8,128)(2,1)S(1)}, bf16[8,2048]{1,0:T(8,128)(2,1)S(1)}, f32[8,2048]{1,0:T(8,128)S(1)}) custom-call(s32[16]{0:T(128)} %lengths_hbm.1, f32[2]{0:T(128)} %bias_hbm.1, bf16[16,2048]{1,0:T(8,128)(2,1)} %tokens_hbm.1, f32[1,2048]{1,0:T(1,128)} %bitcast.42, bf16[2048,128]{1,0:T(8,128)(2,1)} %query_hbm.1, ...), custom_call_target="tpu_custom_call" | custom-call | tf_op jit(solution)/shard_map/attention/pallas_call | solution.py:224
  5.5 2.5 %collective-permute-start.2 = (bf16[8,2048]{1,0:T(8,128)(2,1)S(1)}, bf16[8,2048]{1,0:T(8,128)(2,1)S(1)}, u32[]{:S(2)}, u32[]{:S(2)}) collective-permute-start(bf16[8,2048]{1,0:T(8,128)(2,1)S(1)} %get-tuple-element.26), channel_id=1, source_target_pairs={{0,3},{1,2},{2,1},{3,0},{4,7},{5,6},{6,5},{7,4},{8,11},{9,10},{10,... | collective-permute-start | bytes 98312 | tf_op jit(solution)/shard_map/ppermute | solution.py:38
  8.0 0.7 %collective-permute-start = (bf16[8,2048]{1,0:T(8,128)(2,1)S(1)}, bf16[8,2048]{1,0:T(8,128)(2,1)S(1)}, u32[]{:S(2)}, u32[]{:S(2)}) collective-permute-start(bf16[8,2048]{1,0:T(8,128)(2,1)S(1)} %get-tuple-element.26), channel_id=1, source_target_pairs={{0,1},{1,0},{2,3},{3,2},{4,5},{5,4},{6,7},{7,6},{8,9},{9,8},{10,11... | collective-permute-start | bytes 98312 | tf_op jit(solution)/shard_map/ppermute | solution.py:38
  8.7 0.0 collective-permute-start.1
  8.7 0.0 copy-done.2
  8.7 0.0 copy-done.3
  8.7 0.1 copy.24
  8.8 0.1 select_maximum_fusion.refs_7_
  8.9 3.7 %collective-permute-done.1.refs_2_ = bf16[8,2048]{1,0:T(8,128)(2,1)S(1)} collective-permute-done((bf16[8,2048]{1,0:T(8,128)(2,1)S(1)}, bf16[8,2048]{1,0:T(8,128)(2,1)S(1)}, u32[]{:S(2)}, u32[]{:S(2)}) %collective-permute-start.1) | collective-permute-done | bytes 32800 | tf_op jit(solution)/shard_map/ppermute | solution.py:38
  12.6 0.0 collective-permute-done.2.refs_3_
  12.6 0.0 collective-permute-done.refs_1_
  12.6 0.0 copy-done
  12.6 0.0 copy-done.1
  12.6 0.2 norm.1
  12.8 3.6 %collective-permute-start.5 = (bf16[8,2176]{1,0:T(8,128)(2,1)S(1)}, bf16[8,2176]{1,0:T(8,128)(2,1)S(1)}, u32[]{:S(2)}, u32[]{:S(2)}) collective-permute-start(bf16[8,2176]{1,0:T(8,128)(2,1)S(1)} %get-tuple-element.29.after_ref), channel_id=1, source_target_pairs={{0,24},{4,28},{8,16},{12,20},{16,8},{20,12},{24,0},{28,4},{1,25},{... | collective-permute-start | bytes 104456 | tf_op jit(solution)/shard_map/ppermute | solution.py:38
  16.4 0.0 collective-permute-start.4
  16.4 0.8 %collective-permute-start.3 = (bf16[8,2176]{1,0:T(8,128)(2,1)S(1)}, bf16[8,2176]{1,0:T(8,128)(2,1)S(1)}, u32[]{:S(2)}, u32[]{:S(2)}) collective-permute-start(bf16[8,2176]{1,0:T(8,128)(2,1)S(1)} %get-tuple-element.29.after_ref), channel_id=1, source_target_pairs={{0,8},{4,12},{8,0},{12,4},{16,24},{20,28},{24,16},{28,20},{1,9},{5... | collective-permute-start | bytes 104456 | tf_op jit(solution)/shard_map/ppermute | solution.py:38
  17.2 3.3 %load.1 = (bf16[1,2048,512]{2,1,0:T(8,128)(2,1)S(1)}, bf16[1,2048,512]{2,1,0:T(8,128)(2,1)S(1)}, bf16[1,512,2048]{2,1,0:T(8,128)(2,1)S(1)}, bf16[2048,256]{1,0:T(8,128)(2,1)S(1)}, bf16[128,2048]{1,0:T(8,128)(2,1)S(1)}) custom-call(bf16[8,2176]{1,0:T(8,128)(2,1)S(1)} %get-tuple-element.29.after_ref, bf16[1,2048,512]{2,1,0:T(8,128)(2,1)} %refs_0_.1, ...), custom_call_target="tpu_custom_call" | custom-call | flops 4000000000 | bytes 33554432 | tf_op jit(solution)/shard_map/load/pallas_call | solution.py:287
  20.5 0.0 collective-permute-done.5
  20.5 0.7 %collective-permute-done.4 = bf16[8,2176]{1,0:T(8,128)(2,1)S(1)} collective-permute-done((bf16[8,2176]{1,0:T(8,128)(2,1)S(1)}, bf16[8,2176]{1,0:T(8,128)(2,1)S(1)}, u32[]{:S(2)}, u32[]{:S(2)}) %collective-permute-start.4) | collective-permute-done | bytes 34848 | tf_op jit(solution)/shard_map/ppermute | solution.py:38
  21.3 0.0 collective-permute-done.3
  21.3 1.6 %collective-permute-start.6 = (bf16[32,2176]{1,0:T(8,128)(2,1)S(1)}, bf16[32,2176]{1,0:T(8,128)(2,1)S(1)}, u32[]{:S(2)}, u32[]{:S(2)}) collective-permute-start(bf16[32,2176]{1,0:T(8,128)(2,1)S(1)} %pad_maximum_fusion.2), channel_id=1, source_target_pairs={{0,4},{4,0},{8,12},{12,8},{16,20},{20,16},{24,28},{28,24},{1,5},{5... | collective-permute-start | bytes 417800 | tf_op jit(solution)/shard_map/ppermute | solution.py:38
  22.9 3.6 %collective-permute-done.6 = bf16[32,2176]{1,0:T(8,128)(2,1)S(1)} collective-permute-done((bf16[32,2176]{1,0:T(8,128)(2,1)S(1)}, bf16[32,2176]{1,0:T(8,128)(2,1)S(1)}, u32[]{:S(2)}, u32[]{:S(2)}) %collective-permute-start.6) | collective-permute-done | bytes 139296 | tf_op jit(solution)/shard_map/ppermute | solution.py:38
  26.4 0.1 collective-permute-start.7
  26.5 1.5 %collective-permute-done.7 = bf16[64,2176]{1,0:T(8,128)(2,1)S(1)} collective-permute-done((bf16[64,2176]{1,0:T(8,128)(2,1)S(1)}, bf16[64,2176]{1,0:T(8,128)(2,1)S(1)}, u32[]{:S(2)}, u32[]{:S(2)}) %collective-permute-start.7) | collective-permute-done | bytes 278560 | tf_op jit(solution)/shard_map/ppermute | solution.py:38
  28.1 1.5 %ffn.1 = (f32[64,2048]{1,0:T(8,128)S(1)}, bf16[64,2048]{1,0:T(8,128)(2,1)S(1)}) custom-call(bf16[128,2176]{1,0:T(8,128)(2,1)S(1)} %pad_maximum_fusion.rows_ref, bf16[1,2048,512]{2,1,0:T(8,128)(2,1)S(1)} %get-tuple-element.36.gate_ref, bf16[1,2048,512]{2,1,0:T(8,128)(2,1)S(1)} %get-tuple-element.37.up_ref, ...), custom_call_target="tpu_custom_call" | custom-call | tf_op jit(solution)/shard_map/ffn/pallas_call | solution.py:361
  29.7 0.2 collective-permute-start.8
  29.9 1.4 %collective-permute-done.8.received_ref = bf16[64,2048]{1,0:T(8,128)(2,1)S(1)} collective-permute-done((bf16[64,2048]{1,0:T(8,128)(2,1)S(1)}, bf16[64,2048]{1,0:T(8,128)(2,1)S(1)}, u32[]{:S(2)}, u32[]{:S(2)}) %collective-permute-start.8) | collective-permute-done | bytes 262176 | tf_op jit(solution)/shard_map/ppermute | solution.py:38
  31.3 0.1 fold.1
  31.4 1.6 %collective-permute-start.10 = (bf16[16,2048]{1,0:T(8,128)(2,1)S(1)}, bf16[16,2048]{1,0:T(8,128)(2,1)S(1)}, u32[]{:S(2)}, u32[]{:S(2)}) collective-permute-start(bf16[16,2048]{1,0:T(8,128)(2,1)S(1)} %slice.69), channel_id=1, source_target_pairs={{0,4},{1,5},{2,6},{3,7},{4,0},{5,1},{6,2},{7,3},{8,12},{9,13},{10,... | collective-permute-start | bytes 196616 | tf_op jit(solution)/shard_map/ppermute | solution.py:48
  32.9 0.5 %collective-permute-start.9 = (bf16[16,2048]{1,0:T(8,128)(2,1)S(1)}, bf16[16,2048]{1,0:T(8,128)(2,1)S(1)}, u32[]{:S(2)}, u32[]{:S(2)}) collective-permute-start(bf16[16,2048]{1,0:T(8,128)(2,1)S(1)} %get-tuple-element.47), channel_id=1, source_target_pairs={{0,2},{1,3},{2,0},{3,1},{4,6},{5,7},{6,4},{7,5},{8,10},{9,11},{10,... | collective-permute-start | bytes 196616 | tf_op jit(solution)/shard_map/ppermute | solution.py:48
  33.4 1.5 %collective-permute-start.11 = (bf16[16,2048]{1,0:T(8,128)(2,1)S(1)}, bf16[16,2048]{1,0:T(8,128)(2,1)S(1)}, u32[]{:S(2)}, u32[]{:S(2)}) collective-permute-start(bf16[16,2048]{1,0:T(8,128)(2,1)S(1)} %get-tuple-element.48), channel_id=1, source_target_pairs={{0,6},{1,7},{2,4},{3,5},{4,2},{5,3},{6,0},{7,1},{8,14},{9,15},{10,... | collective-permute-start | bytes 196616 | tf_op jit(solution)/shard_map/ppermute | solution.py:48
  34.9 0.8 %collective-permute-done.10 = bf16[16,2048]{1,0:T(8,128)(2,1)S(1)} collective-permute-done((bf16[16,2048]{1,0:T(8,128)(2,1)S(1)}, bf16[16,2048]{1,0:T(8,128)(2,1)S(1)}, u32[]{:S(2)}, u32[]{:S(2)}) %collective-permute-start.10) | collective-permute-done | bytes 65568 | tf_op jit(solution)/shard_map/ppermute | solution.py:48
  35.7 2.2 %collective-permute-done.9 = bf16[16,2048]{1,0:T(8,128)(2,1)S(1)} collective-permute-done((bf16[16,2048]{1,0:T(8,128)(2,1)S(1)}, bf16[16,2048]{1,0:T(8,128)(2,1)S(1)}, u32[]{:S(2)}, u32[]{:S(2)}) %collective-permute-start.9) | collective-permute-done | bytes 65568 | tf_op jit(solution)/shard_map/ppermute | solution.py:48
  37.9 0.7 %collective-permute-done.11 = bf16[16,2048]{1,0:T(8,128)(2,1)S(1)} collective-permute-done((bf16[16,2048]{1,0:T(8,128)(2,1)S(1)}, bf16[16,2048]{1,0:T(8,128)(2,1)S(1)}, u32[]{:S(2)}, u32[]{:S(2)}) %collective-permute-start.11) | collective-permute-done | bytes 65568 | tf_op jit(solution)/shard_map/ppermute | solution.py:48
  38.7 0.6 %collective-permute-start.12 = (bf16[1,4,2048]{2,1,0:T(4,128)(2,1)S(1)}, bf16[1,4,2048]{2,1,0:T(4,128)(2,1)S(1)}, u32[]{:S(2)}, u32[]{:S(2)}) collective-permute-start(bf16[1,4,2048]{2,1,0:T(4,128)(2,1)S(1)} %get-tuple-element.49), channel_id=1, source_target_pairs={{0,8},{4,12},{8,0},{12,4},{16,24},{20,28},{24,16},{28,20},{1,9},{5... | collective-permute-start | bytes 49160 | tf_op jit(solution)/shard_map/ppermute | solution.py:38
  39.3 3.0 %collective-permute-start.14 = (bf16[1,4,2048]{2,1,0:T(4,128)(2,1)S(1)}, bf16[1,4,2048]{2,1,0:T(4,128)(2,1)S(1)}, u32[]{:S(2)}, u32[]{:S(2)}) collective-permute-start(bf16[1,4,2048]{2,1,0:T(4,128)(2,1)S(1)} %get-tuple-element.50), channel_id=1, source_target_pairs={{0,24},{4,28},{8,16},{12,20},{16,8},{20,12},{24,0},{28,4},{1,25},{... | collective-permute-start | bytes 49160 | tf_op jit(solution)/shard_map/ppermute | solution.py:38
  42.2 0.0 collective-permute-start.13
  42.2 0.2 collective-permute-done.12
  42.5 2.3 %collective-permute-done.14 = bf16[1,4,2048]{2,1,0:T(4,128)(2,1)S(1)} collective-permute-done((bf16[1,4,2048]{2,1,0:T(4,128)(2,1)S(1)}, bf16[1,4,2048]{2,1,0:T(4,128)(2,1)S(1)}, u32[]{:S(2)}, u32[]{:S(2)}) %collective-permute-start.14) | collective-permute-done | bytes 16416 | tf_op jit(solution)/shard_map/ppermute | solution.py:38
  44.8 2.2 %collective-permute-done.13 = bf16[1,4,2048]{2,1,0:T(4,128)(2,1)S(1)} collective-permute-done((bf16[1,4,2048]{2,1,0:T(4,128)(2,1)S(1)}, bf16[1,4,2048]{2,1,0:T(4,128)(2,1)S(1)}, u32[]{:S(2)}, u32[]{:S(2)}) %collective-permute-start.13) | collective-permute-done | bytes 16416 | tf_op jit(solution)/shard_map/ppermute | solution.py:38
  47.0 0.6 %fusion.3 = bf16[4,2048]{1,0:T(4,128)(2,1)} fusion(f32[16,2048]{1,0:T(8,128)S(1)} %get-tuple-element.46, bf16[1,4,2048]{2,1,0:T(4,128)(2,1)S(1)} %collective-permute-done.14, bf16[1,4,2048]{2,1,0:T(4,128)(2,1)S(1)} %collective-permute-done.13, bf16[1,4,2048]{2,1,0:T(4,128)(2,1)S(1)} %collective-permute-done.12, f32[8,2048]{1,0:T(8,128)S(1)} %get-tuple-element.28), kind=kLoop, calls=%fused_computation.9 | loop fusion | flops 65536 | bytes 131072 | tf_op jit(solution)/shard_map/convert_element_type | solution.py:543
  (13 shorter events, 0.2 us)
Async XLA Ops:
  0.0 8.7 %copy-start.2 = (f32[16,4]{0,1:T(4,128)S(1)}, f32[16,4]{0,1:T(4,128)}, u32[]{:S(2)}) copy-start(f32[16,4]{0,1:T(4,128)} %param.34) | copy-start | bytes 772
  0.0 8.7 %copy-start.3 = (s32[16,4]{0,1:T(4,128)S(1)}, s32[16,4]{0,1:T(4,128)}, u32[]{:S(2)}) copy-start(s32[16,4]{0,1:T(4,128)} %param.33) | copy-start | bytes 772
  0.0 12.6 %copy-start = (f32[2048]{0:T(1024)S(1)}, f32[2048]{0:T(1024)}, u32[]{:S(2)}) copy-start(f32[2048]{0:T(1024)} %param.32) | copy-start | bytes 24580
  0.0 12.6 %copy-start.1 = (f32[2048]{0:T(1024)S(1)}, f32[2048]{0:T(1024)}, u32[]{:S(2)}) copy-start(f32[2048]{0:T(1024)} %param.41) | copy-start | bytes 24580
  5.5 7.1 %collective-permute-start.2 = (bf16[8,2048]{1,0:T(8,128)(2,1)S(1)}, bf16[8,2048]{1,0:T(8,128)(2,1)S(1)}, u32[]{:S(2)}, u32[]{:S(2)}) collective-permute-start(bf16[8,2048]{1,0:T(8,128)(2,1)S(1)} %get-tuple-element.26), channel_id=1, source_target_pairs={{0,3},{1,2},{2,1},{3,0},{4,7},{5,6},{6,5},{7,4},{8,11},{9,10},{10,... | collective-permute-start | bytes 98312 | tf_op jit(solution)/shard_map/ppermute | solution.py:38
  8.0 4.6 %collective-permute-start = (bf16[8,2048]{1,0:T(8,128)(2,1)S(1)}, bf16[8,2048]{1,0:T(8,128)(2,1)S(1)}, u32[]{:S(2)}, u32[]{:S(2)}) collective-permute-start(bf16[8,2048]{1,0:T(8,128)(2,1)S(1)} %get-tuple-element.26), channel_id=1, source_target_pairs={{0,1},{1,0},{2,3},{3,2},{4,5},{5,4},{6,7},{7,6},{8,9},{9,8},{10,11... | collective-permute-start | bytes 98312 | tf_op jit(solution)/shard_map/ppermute | solution.py:38
  8.7 3.9 %collective-permute-start.1 = (bf16[8,2048]{1,0:T(8,128)(2,1)S(1)}, bf16[8,2048]{1,0:T(8,128)(2,1)S(1)}, u32[]{:S(2)}, u32[]{:S(2)}) collective-permute-start(bf16[8,2048]{1,0:T(8,128)(2,1)S(1)} %get-tuple-element.25.refs_0_), channel_id=1, source_target_pairs={{0,2},{1,3},{2,0},{3,1},{4,6},{5,7},{6,4},{7,5},{8,10},{9,11},{10,... | collective-permute-start | bytes 98312 | tf_op jit(solution)/shard_map/ppermute | solution.py:38
  12.8 7.7 %collective-permute-start.5 = (bf16[8,2176]{1,0:T(8,128)(2,1)S(1)}, bf16[8,2176]{1,0:T(8,128)(2,1)S(1)}, u32[]{:S(2)}, u32[]{:S(2)}) collective-permute-start(bf16[8,2176]{1,0:T(8,128)(2,1)S(1)} %get-tuple-element.29.after_ref), channel_id=1, source_target_pairs={{0,24},{4,28},{8,16},{12,20},{16,8},{20,12},{24,0},{28,4},{1,25},{... | collective-permute-start | bytes 104456 | tf_op jit(solution)/shard_map/ppermute | solution.py:38
  16.4 4.8 %collective-permute-start.4 = (bf16[8,2176]{1,0:T(8,128)(2,1)S(1)}, bf16[8,2176]{1,0:T(8,128)(2,1)S(1)}, u32[]{:S(2)}, u32[]{:S(2)}) collective-permute-start(bf16[8,2176]{1,0:T(8,128)(2,1)S(1)} %get-tuple-element.29.after_ref), channel_id=1, source_target_pairs={{0,16},{4,20},{8,24},{12,28},{16,0},{20,4},{24,8},{28,12},{1,17},{... | collective-permute-start | bytes 104456 | tf_op jit(solution)/shard_map/ppermute | solution.py:38
  16.4 4.8 %collective-permute-start.3 = (bf16[8,2176]{1,0:T(8,128)(2,1)S(1)}, bf16[8,2176]{1,0:T(8,128)(2,1)S(1)}, u32[]{:S(2)}, u32[]{:S(2)}) collective-permute-start(bf16[8,2176]{1,0:T(8,128)(2,1)S(1)} %get-tuple-element.29.after_ref), channel_id=1, source_target_pairs={{0,8},{4,12},{8,0},{12,4},{16,24},{20,28},{24,16},{28,20},{1,9},{5... | collective-permute-start | bytes 104456 | tf_op jit(solution)/shard_map/ppermute | solution.py:38
  21.3 5.1 %collective-permute-start.6 = (bf16[32,2176]{1,0:T(8,128)(2,1)S(1)}, bf16[32,2176]{1,0:T(8,128)(2,1)S(1)}, u32[]{:S(2)}, u32[]{:S(2)}) collective-permute-start(bf16[32,2176]{1,0:T(8,128)(2,1)S(1)} %pad_maximum_fusion.2), channel_id=1, source_target_pairs={{0,4},{4,0},{8,12},{12,8},{16,20},{20,16},{24,28},{28,24},{1,5},{5... | collective-permute-start | bytes 417800 | tf_op jit(solution)/shard_map/ppermute | solution.py:38
  26.4 1.6 %collective-permute-start.7 = (bf16[64,2176]{1,0:T(8,128)(2,1)S(1)}, bf16[64,2176]{1,0:T(8,128)(2,1)S(1)}, u32[]{:S(2)}, u32[]{:S(2)}) collective-permute-start(bf16[64,2176]{1,0:T(8,128)(2,1)S(1)} %pad_maximum_fusion.1), channel_id=1, source_target_pairs={{0,1},{1,0},{2,3},{3,2},{4,5},{5,4},{6,7},{7,6},{8,9},{9,8},{10,11... | collective-permute-start | bytes 835592 | tf_op jit(solution)/shard_map/ppermute | solution.py:38
  29.7 1.6 %collective-permute-start.8 = (bf16[64,2048]{1,0:T(8,128)(2,1)S(1)}, bf16[64,2048]{1,0:T(8,128)(2,1)S(1)}, u32[]{:S(2)}, u32[]{:S(2)}) collective-permute-start(bf16[64,2048]{1,0:T(8,128)(2,1)S(1)} %get-tuple-element.42), channel_id=1, source_target_pairs={{0,1},{1,0},{2,3},{3,2},{4,5},{5,4},{6,7},{7,6},{8,9},{9,8},{10,11... | collective-permute-start | bytes 786440 | tf_op jit(solution)/shard_map/ppermute | solution.py:38
  31.4 4.3 %collective-permute-start.10 = (bf16[16,2048]{1,0:T(8,128)(2,1)S(1)}, bf16[16,2048]{1,0:T(8,128)(2,1)S(1)}, u32[]{:S(2)}, u32[]{:S(2)}) collective-permute-start(bf16[16,2048]{1,0:T(8,128)(2,1)S(1)} %slice.69), channel_id=1, source_target_pairs={{0,4},{1,5},{2,6},{3,7},{4,0},{5,1},{6,2},{7,3},{8,12},{9,13},{10,... | collective-permute-start | bytes 196616 | tf_op jit(solution)/shard_map/ppermute | solution.py:48
  32.9 5.0 %collective-permute-start.9 = (bf16[16,2048]{1,0:T(8,128)(2,1)S(1)}, bf16[16,2048]{1,0:T(8,128)(2,1)S(1)}, u32[]{:S(2)}, u32[]{:S(2)}) collective-permute-start(bf16[16,2048]{1,0:T(8,128)(2,1)S(1)} %get-tuple-element.47), channel_id=1, source_target_pairs={{0,2},{1,3},{2,0},{3,1},{4,6},{5,7},{6,4},{7,5},{8,10},{9,11},{10,... | collective-permute-start | bytes 196616 | tf_op jit(solution)/shard_map/ppermute | solution.py:48
  33.4 5.2 %collective-permute-start.11 = (bf16[16,2048]{1,0:T(8,128)(2,1)S(1)}, bf16[16,2048]{1,0:T(8,128)(2,1)S(1)}, u32[]{:S(2)}, u32[]{:S(2)}) collective-permute-start(bf16[16,2048]{1,0:T(8,128)(2,1)S(1)} %get-tuple-element.48), channel_id=1, source_target_pairs={{0,6},{1,7},{2,4},{3,5},{4,2},{5,3},{6,0},{7,1},{8,14},{9,15},{10,... | collective-permute-start | bytes 196616 | tf_op jit(solution)/shard_map/ppermute | solution.py:48
  38.7 3.8 %collective-permute-start.12 = (bf16[1,4,2048]{2,1,0:T(4,128)(2,1)S(1)}, bf16[1,4,2048]{2,1,0:T(4,128)(2,1)S(1)}, u32[]{:S(2)}, u32[]{:S(2)}) collective-permute-start(bf16[1,4,2048]{2,1,0:T(4,128)(2,1)S(1)} %get-tuple-element.49), channel_id=1, source_target_pairs={{0,8},{4,12},{8,0},{12,4},{16,24},{20,28},{24,16},{28,20},{1,9},{5... | collective-permute-start | bytes 49160 | tf_op jit(solution)/shard_map/ppermute | solution.py:38
  39.3 5.5 %collective-permute-start.14 = (bf16[1,4,2048]{2,1,0:T(4,128)(2,1)S(1)}, bf16[1,4,2048]{2,1,0:T(4,128)(2,1)S(1)}, u32[]{:S(2)}, u32[]{:S(2)}) collective-permute-start(bf16[1,4,2048]{2,1,0:T(4,128)(2,1)S(1)} %get-tuple-element.50), channel_id=1, source_target_pairs={{0,24},{4,28},{8,16},{12,20},{16,8},{20,12},{24,0},{28,4},{1,25},{... | collective-permute-start | bytes 49160 | tf_op jit(solution)/shard_map/ppermute | solution.py:38
  42.2 4.8 %collective-permute-start.13 = (bf16[1,4,2048]{2,1,0:T(4,128)(2,1)S(1)}, bf16[1,4,2048]{2,1,0:T(4,128)(2,1)S(1)}, u32[]{:S(2)}, u32[]{:S(2)}) collective-permute-start(bf16[1,4,2048]{2,1,0:T(4,128)(2,1)S(1)} %get-tuple-element.51), channel_id=1, source_target_pairs={{0,16},{4,20},{8,24},{12,28},{16,0},{20,4},{24,8},{28,12},{1,17},{... | collective-permute-start | bytes 49160 | tf_op jit(solution)/shard_map/ppermute | solution.py:38

commit v5 on v4

--- a/solution.py
+++ b/solution.py
@@ -303,7 +303,7 @@
 
 
 def ffn_kernel(
-    experts, part, rows_ref, gate_ref, up_ref, down_ref, both_ref, dense_down_ref, keep_ref, send_ref
+    experts, part, rows_ref, gate_ref, up_ref, down_ref, both_ref, dense_down_ref, *out_refs
 ):
     local, width = gate_ref.shape[:2]
     units = dense_down_ref.shape[0]
@@ -338,20 +338,20 @@
                 mixed = mixed + jnp.dot(acts[1 + j], down_ref[j, :, cols], preferred_element_type=F32)
             yield cols, mixed
 
+    quarter = half // 2
     if 2 * half <= ROW_BLOCK:
         for cols, mixed in products(slice(0, 2 * half)):
-            keep_ref[:, cols] = mixed[:half]
-            send_ref[:, cols] = mixed[half:].astype(BF16)
+            for i, ref in enumerate(out_refs):
+                ref[:, cols] = mixed[i * quarter : (i + 1) * quarter].astype(ref.dtype)
         return
-    block = min(half, ROW_BLOCK)
-
-    @pl.loop(0, half // block)
+    block = min(quarter, ROW_BLOCK)
+
+    @pl.loop(0, quarter // block)
     def _(index):
         at = pl.ds(pl.multiple_of(index * block, block), block)
-        for cols, mixed in products(at):
-            keep_ref[at, cols] = mixed
-        for cols, mixed in products(pl.ds(pl.multiple_of(index * block + half, block), block)):
-            send_ref[at, cols] = mixed.astype(BF16)
+        for i, ref in enumerate(out_refs):
+            for cols, mixed in products(pl.ds(pl.multiple_of(index * block + i * quarter, block), block)):
+                ref[at, cols] = mixed.astype(ref.dtype)
 
 
 def ffn(rows, weights, experts, part):
@@ -360,12 +360,9 @@
     near = pl.BlockSpec(memory_space=pltpu.VMEM)
     return pl.pallas_call(
         functools.partial(ffn_kernel, experts, part),
-        out_shape=(
-            jax.ShapeDtypeStruct((total // 2, width), F32),
-            jax.ShapeDtypeStruct((total // 2, width), BF16),
-        ),
+        out_shape=tuple(pltpu.VMEM((total // 4, width), kind) for kind in (F32, F32, BF16, BF16)),
         in_specs=[near] * 6,
-        out_specs=(near, near),
+        out_specs=(near,) * 4,
         compiler_params=pltpu.CompilerParams(vmem_limit_bytes=FFN_VMEM),
         name="ffn",
     )(rows, *weights)
@@ -521,18 +518,20 @@
         rows = jnp.concatenate([rows] + others, axis=0)
     rows, *weights_near = lax.optimization_barrier((rows, *weights_near))
 
-    rows = jnp.concatenate([rows, swap_with(rows, "ep", 1)], axis=0)
-    rows = jnp.concatenate([rows, swap_with(rows, "tp", 1)], axis=0)
-    keep, sent = ffn(rows, weights_near, experts, units)
-    parts = fold(keep, swap_with(sent, "tp", 1), outer, own, F32)
-    half = parts[0].shape[0] // 2
-    mixed = parts[0][:half]
+    near_other = swap_with(rows, "tp", 1)
+    far = swap_with(rows, "ep", 1)
+    rows = jnp.concatenate([rows, far, near_other, swap_with(far, "tp", 1)], axis=0)
+    keep_near, keep_far, sent_near, sent_far = ffn(rows, weights_near, experts, units)
+    received_far = swap_with(sent_far, "tp", 1)
+    received_near = swap_with(sent_near, "tp", 1)
+    parts = [None, fold(keep_far, received_far, outer, own, BF16)]
+    parts[0] = fold(keep_near, received_near, outer, own, F32)
+    mixed = parts[0][0]
     pieces = []
     for e in range(2):
         for t in range(outer):
             if e or t:
-                part = parts[t][e * half : (e + 1) * half].astype(BF16)
-                pieces.append(swap_both(part, e, 2 * t))
+                pieces.append(swap_both(parts[e][t], e, 2 * t))
     mixed = (mixed + sum(p.astype(F32) for p in pieces)).reshape(ep_count // 2, own, width)
     for offsets in stages[1:]:
         mixed = mixed.reshape((len(offsets) + 1, -1) + mixed.shape[1:])

time: 47.8 us -> 47.3 us (0.990)
  waiting for transfers between devices: 19.4 us -> 18.6 us
    ppermute x12 -> x14, waiting for transfers between devices: 15.7 us -> 14.9 us  [swap_with(): return lax.ppermute(values, axis, [(i, i ^ offset) for i in range(count)])]
    ppermute x12 -> x14, starting transfers between devices: 13 us -> 13.3 us  [swap_with(): return lax.ppermute(values, axis, [(i, i ^ offset) for i in range(count)])]
  transfers between devices with their start and end apart: 15 -> 17, of which waited for: 11 -> 11; matrix products, arithmetic and copies ran while one was open for 0% -> 0% of each run, Pallas kernels for 7% -> 7%
where the time goes in v5:
time: 47.3 us; the launch traced here: 47.2 us
  waiting for transfers between devices  18.6 us (39%)
  starting transfers between devices  16.9 us (36%)
  Pallas kernels  10.6 us (22%)
  other arithmetic  0.83 us (2%)
    ppermute x14, waiting for transfers between devices, swap_with(): return lax.ppermute(values, axis, [(i, i ^ offset) for i in range(count)])  14.9 us
    ppermute x14, starting transfers between devices, swap_with(): return lax.ppermute(values, axis, [(i, i ^ offset) for i in range(count)])  13.3 us
    pallas_call x1, Pallas kernels, attention(): pl.pallas_call(functools.partial(attention_kernel, own, heads), out_shape...  5.47 us
    ppermute x3, waiting for transfers between devices, swap_both(): return lax.ppermute(values, ('ep', 'tp'), pairs)  3.67 us
    ppermute x3, starting transfers between devices, swap_both(): return lax.ppermute(values, ('ep', 'tp'), pairs)  3.62 us
    pallas_call x1, Pallas kernels, load_weights(): pl.pallas_call(functools.partial(load_kernel, count, units), out_shape=tu...  3.29 us
    pallas_call x1, Pallas kernels, ffn(): pl.pallas_call(functools.partial(ffn_kernel, experts, part), out_shape=tu...  1.55 us
  transfers between devices with their start and end apart: 17, of which 11 were waited for; matrix products, arithmetic and copies ran while one was open for 0% of the time, Pallas kernels for 7%

profile of v5, /device:TPU:0, one launch (start us, length us, event | category | flops | bytes accessed | tf_op | source)
XLA Modules:
  0.0 47.2 jit_solution(15105816875278286885)
XLA Ops:
  0.0 0.0 copy-start.2
  0.0 0.0 copy-start.3
  0.0 0.0 copy-start
  0.0 5.5 %attention.1 = (bf16[8,2048]{1,0:T(8,128)(2,1)S(1)}, bf16[8,2048]{1,0:T(8,128)(2,1)S(1)}, f32[8,2048]{1,0:T(8,128)S(1)}) custom-call(s32[16]{0:T(128)} %lengths_hbm.1, f32[2]{0:T(128)} %bias_hbm.1, bf16[16,2048]{1,0:T(8,128)(2,1)} %tokens_hbm.1, f32[1,2048]{1,0:T(1,128)} %bitcast.42, bf16[2048,128]{1,0:T(8,128)(2,1)} %query_hbm.1, ...), custom_call_target="tpu_custom_call" | custom-call | tf_op jit(solution)/shard_map/attention/pallas_call | solution.py:224
  5.5 2.5 %collective-permute-start.2 = (bf16[8,2048]{1,0:T(8,128)(2,1)S(1)}, bf16[8,2048]{1,0:T(8,128)(2,1)S(1)}, u32[]{:S(2)}, u32[]{:S(2)}) collective-permute-start(bf16[8,2048]{1,0:T(8,128)(2,1)S(1)} %get-tuple-element.30), channel_id=1, source_target_pairs={{0,3},{1,2},{2,1},{3,0},{4,7},{5,6},{6,5},{7,4},{8,11},{9,10},{10,... | collective-permute-start | bytes 98312 | tf_op jit(solution)/shard_map/ppermute | solution.py:38
  8.0 0.7 %collective-permute-start = (bf16[8,2048]{1,0:T(8,128)(2,1)S(1)}, bf16[8,2048]{1,0:T(8,128)(2,1)S(1)}, u32[]{:S(2)}, u32[]{:S(2)}) collective-permute-start(bf16[8,2048]{1,0:T(8,128)(2,1)S(1)} %get-tuple-element.30), channel_id=1, source_target_pairs={{0,1},{1,0},{2,3},{3,2},{4,5},{5,4},{6,7},{7,6},{8,9},{9,8},{10,11... | collective-permute-start | bytes 98312 | tf_op jit(solution)/shard_map/ppermute | solution.py:38
  8.7 0.0 collective-permute-start.1
  8.7 0.0 copy-done.2
  8.7 0.0 copy-done.3
  8.7 0.1 copy.24
  8.8 0.1 select_maximum_fusion.refs_7_
  8.9 3.7 %collective-permute-done.1.refs_2_ = bf16[8,2048]{1,0:T(8,128)(2,1)S(1)} collective-permute-done((bf16[8,2048]{1,0:T(8,128)(2,1)S(1)}, bf16[8,2048]{1,0:T(8,128)(2,1)S(1)}, u32[]{:S(2)}, u32[]{:S(2)}) %collective-permute-start.1) | collective-permute-done | bytes 32800 | tf_op jit(solution)/shard_map/ppermute | solution.py:38
  12.6 0.0 collective-permute-done.2.refs_3_
  12.6 0.0 collective-permute-done.refs_1_
  12.6 0.0 copy-done
  12.6 0.0 copy-done.1
  12.6 0.2 norm.1
  12.8 3.6 %collective-permute-start.5 = (bf16[8,2176]{1,0:T(8,128)(2,1)S(1)}, bf16[8,2176]{1,0:T(8,128)(2,1)S(1)}, u32[]{:S(2)}, u32[]{:S(2)}) collective-permute-start(bf16[8,2176]{1,0:T(8,128)(2,1)S(1)} %get-tuple-element.33.after_ref), channel_id=1, source_target_pairs={{0,24},{4,28},{8,16},{12,20},{16,8},{20,12},{24,0},{28,4},{1,25},{... | collective-permute-start | bytes 104456 | tf_op jit(solution)/shard_map/ppermute | solution.py:38
  16.4 0.0 collective-permute-start.4
  16.4 0.8 %collective-permute-start.3 = (bf16[8,2176]{1,0:T(8,128)(2,1)S(1)}, bf16[8,2176]{1,0:T(8,128)(2,1)S(1)}, u32[]{:S(2)}, u32[]{:S(2)}) collective-permute-start(bf16[8,2176]{1,0:T(8,128)(2,1)S(1)} %get-tuple-element.33.after_ref), channel_id=1, source_target_pairs={{0,8},{4,12},{8,0},{12,4},{16,24},{20,28},{24,16},{28,20},{1,9},{5... | collective-permute-start | bytes 104456 | tf_op jit(solution)/shard_map/ppermute | solution.py:38
  17.2 3.3 %load.1 = (bf16[1,2048,512]{2,1,0:T(8,128)(2,1)S(1)}, bf16[1,2048,512]{2,1,0:T(8,128)(2,1)S(1)}, bf16[1,512,2048]{2,1,0:T(8,128)(2,1)S(1)}, bf16[2048,256]{1,0:T(8,128)(2,1)S(1)}, bf16[128,2048]{1,0:T(8,128)(2,1)S(1)}) custom-call(bf16[8,2176]{1,0:T(8,128)(2,1)S(1)} %get-tuple-element.33.after_ref, bf16[1,2048,512]{2,1,0:T(8,128)(2,1)} %refs_0_.1, ...), custom_call_target="tpu_custom_call" | custom-call | flops 4000000000 | bytes 33554432 | tf_op jit(solution)/shard_map/load/pallas_call | solution.py:287
  20.5 0.0 collective-permute-done.5
  20.5 0.7 %collective-permute-done.4 = bf16[8,2176]{1,0:T(8,128)(2,1)S(1)} collective-permute-done((bf16[8,2176]{1,0:T(8,128)(2,1)S(1)}, bf16[8,2176]{1,0:T(8,128)(2,1)S(1)}, u32[]{:S(2)}, u32[]{:S(2)}) %collective-permute-start.4) | collective-permute-done | bytes 34848 | tf_op jit(solution)/shard_map/ppermute | solution.py:38
  21.3 0.0 collective-permute-done.3
  21.3 1.6 %collective-permute-start.6 = (bf16[32,2176]{1,0:T(8,128)(2,1)S(1)}, bf16[32,2176]{1,0:T(8,128)(2,1)S(1)}, u32[]{:S(2)}, u32[]{:S(2)}) collective-permute-start(bf16[32,2176]{1,0:T(8,128)(2,1)S(1)} %pad_maximum_fusion.1), channel_id=1, source_target_pairs={{0,4},{4,0},{8,12},{12,8},{16,20},{20,16},{24,28},{28,24},{1,5},{5... | collective-permute-start | bytes 417800 | tf_op jit(solution)/shard_map/ppermute | solution.py:38
  22.9 0.0 collective-permute-start.7
  22.9 3.6 %collective-permute-done.6 = bf16[32,2176]{1,0:T(8,128)(2,1)S(1)} collective-permute-done((bf16[32,2176]{1,0:T(8,128)(2,1)S(1)}, bf16[32,2176]{1,0:T(8,128)(2,1)S(1)}, u32[]{:S(2)}, u32[]{:S(2)}) %collective-permute-start.6) | collective-permute-done | bytes 139296 | tf_op jit(solution)/shard_map/ppermute | solution.py:38
  26.4 0.0 collective-permute-start.8
  26.4 0.0 collective-permute-done.7
  26.4 1.4 %collective-permute-done.8 = bf16[32,2176]{1,0:T(8,128)(2,1)S(1)} collective-permute-done((bf16[32,2176]{1,0:T(8,128)(2,1)S(1)}, bf16[32,2176]{1,0:T(8,128)(2,1)S(1)}, u32[]{:S(2)}, u32[]{:S(2)}) %collective-permute-start.8) | collective-permute-done | bytes 139296 | tf_op jit(solution)/shard_map/ppermute | solution.py:38
  27.8 1.5 %ffn.1 = (f32[32,2048]{1,0:T(8,128)S(1)}, f32[32,2048]{1,0:T(8,128)S(1)}, bf16[32,2048]{1,0:T(8,128)(2,1)S(1)}, bf16[32,2048]{1,0:T(8,128)(2,1)S(1)}) custom-call(bf16[128,2176]{1,0:T(8,128)(2,1)S(1)} %pad_maximum_fusion.rows_ref, bf16[1,2048,512]{2,1,0:T(8,128)(2,1)S(1)} %get-tuple-element.40.gate_ref, bf16[1,2048,512]{2,1,0:T(8,128)(2,1)S(1)} %get-tuple-element.41.up_ref, ...), custom_call_target="tpu_custom_call" | custom-call | tf_op jit(solution)/shard_map/ffn/pallas_call | solution.py:361
  29.4 0.2 collective-permute-start.9
  29.6 0.4 collective-permute-start.11
  30.0 0.8 %collective-permute-done.9.received_ref = bf16[32,2048]{1,0:T(8,128)(2,1)S(1)} collective-permute-done((bf16[32,2048]{1,0:T(8,128)(2,1)S(1)}, bf16[32,2048]{1,0:T(8,128)(2,1)S(1)}, u32[]{:S(2)}, u32[]{:S(2)}) %collective-permute-start.9) | collective-permute-done | bytes 131104 | tf_op jit(solution)/shard_map/ppermute | solution.py:38
  30.8 0.6 %collective-permute-start.10 = (bf16[16,2048]{1,0:T(8,128)(2,1)S(1)}, bf16[16,2048]{1,0:T(8,128)(2,1)S(1)}, u32[]{:S(2)}, u32[]{:S(2)}) collective-permute-start(bf16[16,2048]{1,0:T(8,128)(2,1)S(1)} %get-tuple-element.48), channel_id=1, source_target_pairs={{0,2},{1,3},{2,0},{3,1},{4,6},{5,7},{6,4},{7,5},{8,10},{9,11},{10,... | collective-permute-start | bytes 196616 | tf_op jit(solution)/shard_map/ppermute | solution.py:48
  31.4 0.0 collective-permute-done.11.received_ref
  31.5 1.6 %collective-permute-start.12 = (bf16[16,2048]{1,0:T(8,128)(2,1)S(1)}, bf16[16,2048]{1,0:T(8,128)(2,1)S(1)}, u32[]{:S(2)}, u32[]{:S(2)}) collective-permute-start(bf16[16,2048]{1,0:T(8,128)(2,1)S(1)} %get-tuple-element.51), channel_id=1, source_target_pairs={{0,4},{1,5},{2,6},{3,7},{4,0},{5,1},{6,2},{7,3},{8,12},{9,13},{10,... | collective-permute-start | bytes 196616 | tf_op jit(solution)/shard_map/ppermute | solution.py:48
  33.0 1.5 %collective-permute-start.13 = (bf16[16,2048]{1,0:T(8,128)(2,1)S(1)}, bf16[16,2048]{1,0:T(8,128)(2,1)S(1)}, u32[]{:S(2)}, u32[]{:S(2)}) collective-permute-start(bf16[16,2048]{1,0:T(8,128)(2,1)S(1)} %get-tuple-element.52), channel_id=1, source_target_pairs={{0,6},{1,7},{2,4},{3,5},{4,2},{5,3},{6,0},{7,1},{8,14},{9,15},{10,... | collective-permute-start | bytes 196616 | tf_op jit(solution)/shard_map/ppermute | solution.py:48
  34.5 0.7 %collective-permute-done.10 = bf16[16,2048]{1,0:T(8,128)(2,1)S(1)} collective-permute-done((bf16[16,2048]{1,0:T(8,128)(2,1)S(1)}, bf16[16,2048]{1,0:T(8,128)(2,1)S(1)}, u32[]{:S(2)}, u32[]{:S(2)}) %collective-permute-start.10) | collective-permute-done | bytes 65568 | tf_op jit(solution)/shard_map/ppermute | solution.py:48
  35.2 0.6 %collective-permute-done.12 = bf16[16,2048]{1,0:T(8,128)(2,1)S(1)} collective-permute-done((bf16[16,2048]{1,0:T(8,128)(2,1)S(1)}, bf16[16,2048]{1,0:T(8,128)(2,1)S(1)}, u32[]{:S(2)}, u32[]{:S(2)}) %collective-permute-start.12) | collective-permute-done | bytes 65568 | tf_op jit(solution)/shard_map/ppermute | solution.py:48
  35.8 2.4 %collective-permute-done.13 = bf16[16,2048]{1,0:T(8,128)(2,1)S(1)} collective-permute-done((bf16[16,2048]{1,0:T(8,128)(2,1)S(1)}, bf16[16,2048]{1,0:T(8,128)(2,1)S(1)}, u32[]{:S(2)}, u32[]{:S(2)}) %collective-permute-start.13) | collective-permute-done | bytes 65568 | tf_op jit(solution)/shard_map/ppermute | solution.py:48
  38.2 0.6 %collective-permute-start.14 = (bf16[1,4,2048]{2,1,0:T(4,128)(2,1)S(1)}, bf16[1,4,2048]{2,1,0:T(4,128)(2,1)S(1)}, u32[]{:S(2)}, u32[]{:S(2)}) collective-permute-start(bf16[1,4,2048]{2,1,0:T(4,128)(2,1)S(1)} %get-tuple-element.55), channel_id=1, source_target_pairs={{0,8},{4,12},{8,0},{12,4},{16,24},{20,28},{24,16},{28,20},{1,9},{5... | collective-permute-start | bytes 49160 | tf_op jit(solution)/shard_map/ppermute | solution.py:38
  38.8 3.0 %collective-permute-start.16 = (bf16[1,4,2048]{2,1,0:T(4,128)(2,1)S(1)}, bf16[1,4,2048]{2,1,0:T(4,128)(2,1)S(1)}, u32[]{:S(2)}, u32[]{:S(2)}) collective-permute-start(bf16[1,4,2048]{2,1,0:T(4,128)(2,1)S(1)} %get-tuple-element.56), channel_id=1, source_target_pairs={{0,24},{4,28},{8,16},{12,20},{16,8},{20,12},{24,0},{28,4},{1,25},{... | collective-permute-start | bytes 49160 | tf_op jit(solution)/shard_map/ppermute | solution.py:38
  41.8 0.0 collective-permute-start.15
  41.8 0.3 collective-permute-done.14
  42.1 2.3 %collective-permute-done.16 = bf16[1,4,2048]{2,1,0:T(4,128)(2,1)S(1)} collective-permute-done((bf16[1,4,2048]{2,1,0:T(4,128)(2,1)S(1)}, bf16[1,4,2048]{2,1,0:T(4,128)(2,1)S(1)}, u32[]{:S(2)}, u32[]{:S(2)}) %collective-permute-start.16) | collective-permute-done | bytes 16416 | tf_op jit(solution)/shard_map/ppermute | solution.py:38
  44.4 2.2 %collective-permute-done.15 = bf16[1,4,2048]{2,1,0:T(4,128)(2,1)S(1)} collective-permute-done((bf16[1,4,2048]{2,1,0:T(4,128)(2,1)S(1)}, bf16[1,4,2048]{2,1,0:T(4,128)(2,1)S(1)}, u32[]{:S(2)}, u32[]{:S(2)}) %collective-permute-start.15) | collective-permute-done | bytes 16416 | tf_op jit(solution)/shard_map/ppermute | solution.py:38
  46.6 0.6 %fusion.3 = bf16[4,2048]{1,0:T(4,128)(2,1)} fusion(f32[16,2048]{1,0:T(8,128)S(1)} %get-tuple-element.54, bf16[1,4,2048]{2,1,0:T(4,128)(2,1)S(1)} %collective-permute-done.16, bf16[1,4,2048]{2,1,0:T(4,128)(2,1)S(1)} %collective-permute-done.15, bf16[1,4,2048]{2,1,0:T(4,128)(2,1)S(1)} %collective-permute-done.14, f32[8,2048]{1,0:T(8,128)S(1)} %get-tuple-element.32), kind=kLoop, calls=%fused_computation.7 | loop fusion | flops 65536 | bytes 131072 | tf_op jit(solution)/shard_map/convert_element_type | solution.py:542
  (13 shorter events, 0.2 us)
Async XLA Ops:
  0.0 8.7 %copy-start.2 = (f32[16,4]{0,1:T(4,128)S(1)}, f32[16,4]{0,1:T(4,128)}, u32[]{:S(2)}) copy-start(f32[16,4]{0,1:T(4,128)} %param.34) | copy-start | bytes 772
  0.0 8.7 %copy-start.3 = (s32[16,4]{0,1:T(4,128)S(1)}, s32[16,4]{0,1:T(4,128)}, u32[]{:S(2)}) copy-start(s32[16,4]{0,1:T(4,128)} %param.33) | copy-start | bytes 772
  0.0 12.6 %copy-start = (f32[2048]{0:T(1024)S(1)}, f32[2048]{0:T(1024)}, u32[]{:S(2)}) copy-start(f32[2048]{0:T(1024)} %param.32) | copy-start | bytes 24580
  0.0 12.6 %copy-start.1 = (f32[2048]{0:T(1024)S(1)}, f32[2048]{0:T(1024)}, u32[]{:S(2)}) copy-start(f32[2048]{0:T(1024)} %param.41) | copy-start | bytes 24580
  5.5 7.1 %collective-permute-start.2 = (bf16[8,2048]{1,0:T(8,128)(2,1)S(1)}, bf16[8,2048]{1,0:T(8,128)(2,1)S(1)}, u32[]{:S(2)}, u32[]{:S(2)}) collective-permute-start(bf16[8,2048]{1,0:T(8,128)(2,1)S(1)} %get-tuple-element.30), channel_id=1, source_target_pairs={{0,3},{1,2},{2,1},{3,0},{4,7},{5,6},{6,5},{7,4},{8,11},{9,10},{10,... | collective-permute-start | bytes 98312 | tf_op jit(solution)/shard_map/ppermute | solution.py:38
  8.0 4.6 %collective-permute-start = (bf16[8,2048]{1,0:T(8,128)(2,1)S(1)}, bf16[8,2048]{1,0:T(8,128)(2,1)S(1)}, u32[]{:S(2)}, u32[]{:S(2)}) collective-permute-start(bf16[8,2048]{1,0:T(8,128)(2,1)S(1)} %get-tuple-element.30), channel_id=1, source_target_pairs={{0,1},{1,0},{2,3},{3,2},{4,5},{5,4},{6,7},{7,6},{8,9},{9,8},{10,11... | collective-permute-start | bytes 98312 | tf_op jit(solution)/shard_map/ppermute | solution.py:38
  8.7 3.9 %collective-permute-start.1 = (bf16[8,2048]{1,0:T(8,128)(2,1)S(1)}, bf16[8,2048]{1,0:T(8,128)(2,1)S(1)}, u32[]{:S(2)}, u32[]{:S(2)}) collective-permute-start(bf16[8,2048]{1,0:T(8,128)(2,1)S(1)} %get-tuple-element.29.refs_0_), channel_id=1, source_target_pairs={{0,2},{1,3},{2,0},{3,1},{4,6},{5,7},{6,4},{7,5},{8,10},{9,11},{10,... | collective-permute-start | bytes 98312 | tf_op jit(solution)/shard_map/ppermute | solution.py:38
  12.8 7.7 %collective-permute-start.5 = (bf16[8,2176]{1,0:T(8,128)(2,1)S(1)}, bf16[8,2176]{1,0:T(8,128)(2,1)S(1)}, u32[]{:S(2)}, u32[]{:S(2)}) collective-permute-start(bf16[8,2176]{1,0:T(8,128)(2,1)S(1)} %get-tuple-element.33.after_ref), channel_id=1, source_target_pairs={{0,24},{4,28},{8,16},{12,20},{16,8},{20,12},{24,0},{28,4},{1,25},{... | collective-permute-start | bytes 104456 | tf_op jit(solution)/shard_map/ppermute | solution.py:38
  16.4 4.8 %collective-permute-start.4 = (bf16[8,2176]{1,0:T(8,128)(2,1)S(1)}, bf16[8,2176]{1,0:T(8,128)(2,1)S(1)}, u32[]{:S(2)}, u32[]{:S(2)}) collective-permute-start(bf16[8,2176]{1,0:T(8,128)(2,1)S(1)} %get-tuple-element.33.after_ref), channel_id=1, source_target_pairs={{0,16},{4,20},{8,24},{12,28},{16,0},{20,4},{24,8},{28,12},{1,17},{... | collective-permute-start | bytes 104456 | tf_op jit(solution)/shard_map/ppermute | solution.py:38
  16.4 4.8 %collective-permute-start.3 = (bf16[8,2176]{1,0:T(8,128)(2,1)S(1)}, bf16[8,2176]{1,0:T(8,128)(2,1)S(1)}, u32[]{:S(2)}, u32[]{:S(2)}) collective-permute-start(bf16[8,2176]{1,0:T(8,128)(2,1)S(1)} %get-tuple-element.33.after_ref), channel_id=1, source_target_pairs={{0,8},{4,12},{8,0},{12,4},{16,24},{20,28},{24,16},{28,20},{1,9},{5... | collective-permute-start | bytes 104456 | tf_op jit(solution)/shard_map/ppermute | solution.py:38
  21.3 5.1 %collective-permute-start.6 = (bf16[32,2176]{1,0:T(8,128)(2,1)S(1)}, bf16[32,2176]{1,0:T(8,128)(2,1)S(1)}, u32[]{:S(2)}, u32[]{:S(2)}) collective-permute-start(bf16[32,2176]{1,0:T(8,128)(2,1)S(1)} %pad_maximum_fusion.1), channel_id=1, source_target_pairs={{0,4},{4,0},{8,12},{12,8},{16,20},{20,16},{24,28},{28,24},{1,5},{5... | collective-permute-start | bytes 417800 | tf_op jit(solution)/shard_map/ppermute | solution.py:38
  22.9 3.6 %collective-permute-start.7 = (bf16[32,2176]{1,0:T(8,128)(2,1)S(1)}, bf16[32,2176]{1,0:T(8,128)(2,1)S(1)}, u32[]{:S(2)}, u32[]{:S(2)}) collective-permute-start(bf16[32,2176]{1,0:T(8,128)(2,1)S(1)} %pad_maximum_fusion.1), channel_id=1, source_target_pairs={{0,1},{1,0},{2,3},{3,2},{4,5},{5,4},{6,7},{7,6},{8,9},{9,8},{10,11... | collective-permute-start | bytes 417800 | tf_op jit(solution)/shard_map/ppermute | solution.py:38
  26.4 1.4 %collective-permute-start.8 = (bf16[32,2176]{1,0:T(8,128)(2,1)S(1)}, bf16[32,2176]{1,0:T(8,128)(2,1)S(1)}, u32[]{:S(2)}, u32[]{:S(2)}) collective-permute-start(bf16[32,2176]{1,0:T(8,128)(2,1)S(1)} %collective-permute-done.6), channel_id=1, source_target_pairs={{0,1},{1,0},{2,3},{3,2},{4,5},{5,4},{6,7},{7,6},{8,9},{9,8},{10,11... | collective-permute-start | bytes 417800 | tf_op jit(solution)/shard_map/ppermute | solution.py:38
  29.4 1.4 %collective-permute-start.9 = (bf16[32,2048]{1,0:T(8,128)(2,1)S(1)}, bf16[32,2048]{1,0:T(8,128)(2,1)S(1)}, u32[]{:S(2)}, u32[]{:S(2)}) collective-permute-start(bf16[32,2048]{1,0:T(8,128)(2,1)S(1)} %get-tuple-element.46), channel_id=1, source_target_pairs={{0,1},{1,0},{2,3},{3,2},{4,5},{5,4},{6,7},{7,6},{8,9},{9,8},{10,11... | collective-permute-start | bytes 393224 | tf_op jit(solution)/shard_map/ppermute | solution.py:38
  29.6 1.8 %collective-permute-start.11 = (bf16[32,2048]{1,0:T(8,128)(2,1)S(1)}, bf16[32,2048]{1,0:T(8,128)(2,1)S(1)}, u32[]{:S(2)}, u32[]{:S(2)}) collective-permute-start(bf16[32,2048]{1,0:T(8,128)(2,1)S(1)} %get-tuple-element.50), channel_id=1, source_target_pairs={{0,1},{1,0},{2,3},{3,2},{4,5},{5,4},{6,7},{7,6},{8,9},{9,8},{10,11... | collective-permute-start | bytes 393224 | tf_op jit(solution)/shard_map/ppermute | solution.py:38
  30.8 4.3 %collective-permute-start.10 = (bf16[16,2048]{1,0:T(8,128)(2,1)S(1)}, bf16[16,2048]{1,0:T(8,128)(2,1)S(1)}, u32[]{:S(2)}, u32[]{:S(2)}) collective-permute-start(bf16[16,2048]{1,0:T(8,128)(2,1)S(1)} %get-tuple-element.48), channel_id=1, source_target_pairs={{0,2},{1,3},{2,0},{3,1},{4,6},{5,7},{6,4},{7,5},{8,10},{9,11},{10,... | collective-permute-start | bytes 196616 | tf_op jit(solution)/shard_map/ppermute | solution.py:48
  31.5 4.3 %collective-permute-start.12 = (bf16[16,2048]{1,0:T(8,128)(2,1)S(1)}, bf16[16,2048]{1,0:T(8,128)(2,1)S(1)}, u32[]{:S(2)}, u32[]{:S(2)}) collective-permute-start(bf16[16,2048]{1,0:T(8,128)(2,1)S(1)} %get-tuple-element.51), channel_id=1, source_target_pairs={{0,4},{1,5},{2,6},{3,7},{4,0},{5,1},{6,2},{7,3},{8,12},{9,13},{10,... | collective-permute-start | bytes 196616 | tf_op jit(solution)/shard_map/ppermute | solution.py:48
  33.0 5.2 %collective-permute-start.13 = (bf16[16,2048]{1,0:T(8,128)(2,1)S(1)}, bf16[16,2048]{1,0:T(8,128)(2,1)S(1)}, u32[]{:S(2)}, u32[]{:S(2)}) collective-permute-start(bf16[16,2048]{1,0:T(8,128)(2,1)S(1)} %get-tuple-element.52), channel_id=1, source_target_pairs={{0,6},{1,7},{2,4},{3,5},{4,2},{5,3},{6,0},{7,1},{8,14},{9,15},{10,... | collective-permute-start | bytes 196616 | tf_op jit(solution)/shard_map/ppermute | solution.py:48
  38.2 3.8 %collective-permute-start.14 = (bf16[1,4,2048]{2,1,0:T(4,128)(2,1)S(1)}, bf16[1,4,2048]{2,1,0:T(4,128)(2,1)S(1)}, u32[]{:S(2)}, u32[]{:S(2)}) collective-permute-start(bf16[1,4,2048]{2,1,0:T(4,128)(2,1)S(1)} %get-tuple-element.55), channel_id=1, source_target_pairs={{0,8},{4,12},{8,0},{12,4},{16,24},{20,28},{24,16},{28,20},{1,9},{5... | collective-permute-start | bytes 49160 | tf_op jit(solution)/shard_map/ppermute | solution.py:38
  38.8 5.5 %collective-permute-start.16 = (bf16[1,4,2048]{2,1,0:T(4,128)(2,1)S(1)}, bf16[1,4,2048]{2,1,0:T(4,128)(2,1)S(1)}, u32[]{:S(2)}, u32[]{:S(2)}) collective-permute-start(bf16[1,4,2048]{2,1,0:T(4,128)(2,1)S(1)} %get-tuple-element.56), channel_id=1, source_target_pairs={{0,24},{4,28},{8,16},{12,20},{16,8},{20,12},{24,0},{28,4},{1,25},{... | collective-permute-start | bytes 49160 | tf_op jit(solution)/shard_map/ppermute | solution.py:38
  41.8 4.8 %collective-permute-start.15 = (bf16[1,4,2048]{2,1,0:T(4,128)(2,1)S(1)}, bf16[1,4,2048]{2,1,0:T(4,128)(2,1)S(1)}, u32[]{:S(2)}, u32[]{:S(2)}) collective-permute-start(bf16[1,4,2048]{2,1,0:T(4,128)(2,1)S(1)} %get-tuple-element.57), channel_id=1, source_target_pairs={{0,16},{4,20},{8,24},{12,28},{16,0},{20,4},{24,8},{28,12},{1,17},{... | collective-permute-start | bytes 49160 | tf_op jit(solution)/shard_map/ppermute | solution.py:38

commit v6 on v5

--- a/solution.py
+++ b/solution.py
@@ -127,15 +127,11 @@
     near_ref[...] = jnp.dot(order, tokens_buf[...], preferred_element_type=F32)[: seq_count // 2]
 
     transposed = (((1,), (1,)), ((), ()))
-    copies[2].wait()
+    for copy in copies[2:9]:
+        copy.wait()
     queries = jnp.dot(normed, query_buf[...], preferred_element_type=F32).astype(BF16).astype(F32)
-    copies[3].wait()
-    copies[4].wait()
     own_pair = lax.dot_general(normed, pair_buf[...], transposed, preferred_element_type=F32)
     own_pair = own_pair.astype(BF16).astype(F32)
-    copies[5].wait()
-    copies[7].wait()
-    copies[8].wait()
     forget = lax.dot_general(normed, forget_buf[...], transposed, preferred_element_type=F32)
 
     lane = lax.broadcasted_iota(jnp.int32, (rows, lanes), 1)
@@ -157,7 +153,6 @@
     scale = head_dim ** (-0.5)
     sequence = lax.broadcasted_iota(jnp.int32, (span, 1), 0) // heads
     place = lax.broadcasted_iota(jnp.int32, (span, cache_len), 1)
-    copies[6].wait()
     outputs = []
     for first in range(0, seq_count, group):
         at = slice(first * heads, first * heads + span)
@@ -180,9 +175,11 @@
         probs = (cached / denominator).astype(BF16)
         probs_own = (own_exp / denominator).astype(BF16).astype(F32)
         mixed = jnp.zeros((span, lanes), F32)
-        for i in range(group):
-            found = jnp.dot(probs, cache_buf[first + i], preferred_element_type=F32)
-            mixed = jnp.where(sequence == i, found, mixed)
+        for i in range(0, group, 2):
+            both = jnp.concatenate([cache_buf[first + i], cache_buf[first + i + 1]], axis=1)
+            found = jnp.dot(probs, both, preferred_element_type=F32)
+            mixed = jnp.where(sequence == i, found[:, :lanes], mixed)
+            mixed = jnp.where(sequence == i + 1, found[:, lanes:], mixed)
         outputs.append(mixed + probs_own * own_pair[at])
     attended = jnp.concatenate(outputs, axis=0)
     attended = jnp.where(head == 0, pltpu.roll(attended, head_dim, 1), attended)

time: 47.3 us -> 47.3 us (level)
  no operation moved by 1% of the time
where the time goes in v6:
time: 47.3 us; the launch traced here: 47.2 us
  waiting for transfers between devices  18.6 us (39%)
  starting transfers between devices  16.9 us (36%)
  Pallas kernels  10.6 us (22%)
  other arithmetic  0.83 us (2%)
    ppermute x14, waiting for transfers between devices, swap_with(): return lax.ppermute(values, axis, [(i, i ^ offset) for i in range(count)])  14.9 us
    ppermute x14, starting transfers between devices, swap_with(): return lax.ppermute(values, axis, [(i, i ^ offset) for i in range(count)])  13.3 us
    pallas_call x1, Pallas kernels, attention(): pl.pallas_call(functools.partial(attention_kernel, own, heads), out_shape...  5.43 us
    ppermute x3, waiting for transfers between devices, swap_both(): return lax.ppermute(values, ('ep', 'tp'), pairs)  3.67 us
    ppermute x3, starting transfers between devices, swap_both(): return lax.ppermute(values, ('ep', 'tp'), pairs)  3.62 us
    pallas_call x1, Pallas kernels, load_weights(): pl.pallas_call(functools.partial(load_kernel, count, units), out_shape=tu...  3.29 us
    pallas_call x1, Pallas kernels, ffn(): pl.pallas_call(functools.partial(ffn_kernel, experts, part), out_shape=tu...  1.55 us
  transfers between devices with their start and end apart: 17, of which 11 were waited for; matrix products, arithmetic and copies ran while one was open for 0% of the time, Pallas kernels for 7%

profile of v6, /device:TPU:0, one launch (start us, length us, event | category | flops | bytes accessed | tf_op | source)
XLA Modules:
  0.0 47.2 jit_solution(4145778026481848910)
XLA Ops:
  0.0 0.0 copy-start.2
  0.0 0.0 copy-start.3
  0.0 0.0 copy-start
  0.0 5.4 %attention.1 = (bf16[8,2048]{1,0:T(8,128)(2,1)S(1)}, bf16[8,2048]{1,0:T(8,128)(2,1)S(1)}, f32[8,2048]{1,0:T(8,128)S(1)}) custom-call(s32[16]{0:T(128)} %lengths_hbm.1, f32[2]{0:T(128)} %bias_hbm.1, bf16[16,2048]{1,0:T(8,128)(2,1)} %tokens_hbm.1, f32[1,2048]{1,0:T(1,128)} %bitcast.42, bf16[2048,128]{1,0:T(8,128)(2,1)} %query_hbm.1, ...), custom_call_target="tpu_custom_call" | custom-call | tf_op jit(solution)/shard_map/attention/pallas_call | solution.py:221
  5.4 2.5 %collective-permute-start.2 = (bf16[8,2048]{1,0:T(8,128)(2,1)S(1)}, bf16[8,2048]{1,0:T(8,128)(2,1)S(1)}, u32[]{:S(2)}, u32[]{:S(2)}) collective-permute-start(bf16[8,2048]{1,0:T(8,128)(2,1)S(1)} %get-tuple-element.30), channel_id=1, source_target_pairs={{0,3},{1,2},{2,1},{3,0},{4,7},{5,6},{6,5},{7,4},{8,11},{9,10},{10,... | collective-permute-start | bytes 98312 | tf_op jit(solution)/shard_map/ppermute | solution.py:38
  7.9 0.7 %collective-permute-start = (bf16[8,2048]{1,0:T(8,128)(2,1)S(1)}, bf16[8,2048]{1,0:T(8,128)(2,1)S(1)}, u32[]{:S(2)}, u32[]{:S(2)}) collective-permute-start(bf16[8,2048]{1,0:T(8,128)(2,1)S(1)} %get-tuple-element.30), channel_id=1, source_target_pairs={{0,1},{1,0},{2,3},{3,2},{4,5},{5,4},{6,7},{7,6},{8,9},{9,8},{10,11... | collective-permute-start | bytes 98312 | tf_op jit(solution)/shard_map/ppermute | solution.py:38
  8.6 0.0 collective-permute-start.1
  8.7 0.0 copy-done.2
  8.7 0.0 copy-done.3
  8.7 0.1 copy.24
  8.8 0.1 select_maximum_fusion.refs_7_
  8.9 3.7 %collective-permute-done.1.refs_2_ = bf16[8,2048]{1,0:T(8,128)(2,1)S(1)} collective-permute-done((bf16[8,2048]{1,0:T(8,128)(2,1)S(1)}, bf16[8,2048]{1,0:T(8,128)(2,1)S(1)}, u32[]{:S(2)}, u32[]{:S(2)}) %collective-permute-start.1) | collective-permute-done | bytes 32800 | tf_op jit(solution)/shard_map/ppermute | solution.py:38
  12.5 0.0 collective-permute-done.2.refs_3_
  12.5 0.0 collective-permute-done.refs_1_
  12.5 0.0 copy-done
  12.5 0.0 copy-done.1
  12.6 0.2 norm.1
  12.8 3.6 %collective-permute-start.5 = (bf16[8,2176]{1,0:T(8,128)(2,1)S(1)}, bf16[8,2176]{1,0:T(8,128)(2,1)S(1)}, u32[]{:S(2)}, u32[]{:S(2)}) collective-permute-start(bf16[8,2176]{1,0:T(8,128)(2,1)S(1)} %get-tuple-element.33.after_ref), channel_id=1, source_target_pairs={{0,24},{4,28},{8,16},{12,20},{16,8},{20,12},{24,0},{28,4},{1,25},{... | collective-permute-start | bytes 104456 | tf_op jit(solution)/shard_map/ppermute | solution.py:38
  16.4 0.0 collective-permute-start.4
  16.4 0.8 %collective-permute-start.3 = (bf16[8,2176]{1,0:T(8,128)(2,1)S(1)}, bf16[8,2176]{1,0:T(8,128)(2,1)S(1)}, u32[]{:S(2)}, u32[]{:S(2)}) collective-permute-start(bf16[8,2176]{1,0:T(8,128)(2,1)S(1)} %get-tuple-element.33.after_ref), channel_id=1, source_target_pairs={{0,8},{4,12},{8,0},{12,4},{16,24},{20,28},{24,16},{28,20},{1,9},{5... | collective-permute-start | bytes 104456 | tf_op jit(solution)/shard_map/ppermute | solution.py:38
  17.2 3.3 %load.1 = (bf16[1,2048,512]{2,1,0:T(8,128)(2,1)S(1)}, bf16[1,2048,512]{2,1,0:T(8,128)(2,1)S(1)}, bf16[1,512,2048]{2,1,0:T(8,128)(2,1)S(1)}, bf16[2048,256]{1,0:T(8,128)(2,1)S(1)}, bf16[128,2048]{1,0:T(8,128)(2,1)S(1)}) custom-call(bf16[8,2176]{1,0:T(8,128)(2,1)S(1)} %get-tuple-element.33.after_ref, bf16[1,2048,512]{2,1,0:T(8,128)(2,1)} %refs_0_.1, ...), custom_call_target="tpu_custom_call" | custom-call | flops 4000000000 | bytes 33554432 | tf_op jit(solution)/shard_map/load/pallas_call | solution.py:284
  20.5 0.0 collective-permute-done.5
  20.5 0.7 %collective-permute-done.4 = bf16[8,2176]{1,0:T(8,128)(2,1)S(1)} collective-permute-done((bf16[8,2176]{1,0:T(8,128)(2,1)S(1)}, bf16[8,2176]{1,0:T(8,128)(2,1)S(1)}, u32[]{:S(2)}, u32[]{:S(2)}) %collective-permute-start.4) | collective-permute-done | bytes 34848 | tf_op jit(solution)/shard_map/ppermute | solution.py:38
  21.2 0.0 collective-permute-done.3
  21.3 1.6 %collective-permute-start.6 = (bf16[32,2176]{1,0:T(8,128)(2,1)S(1)}, bf16[32,2176]{1,0:T(8,128)(2,1)S(1)}, u32[]{:S(2)}, u32[]{:S(2)}) collective-permute-start(bf16[32,2176]{1,0:T(8,128)(2,1)S(1)} %pad_maximum_fusion.1), channel_id=1, source_target_pairs={{0,4},{4,0},{8,12},{12,8},{16,20},{20,16},{24,28},{28,24},{1,5},{5... | collective-permute-start | bytes 417800 | tf_op jit(solution)/shard_map/ppermute | solution.py:38
  22.8 0.0 collective-permute-start.7
  22.8 3.6 %collective-permute-done.6 = bf16[32,2176]{1,0:T(8,128)(2,1)S(1)} collective-permute-done((bf16[32,2176]{1,0:T(8,128)(2,1)S(1)}, bf16[32,2176]{1,0:T(8,128)(2,1)S(1)}, u32[]{:S(2)}, u32[]{:S(2)}) %collective-permute-start.6) | collective-permute-done | bytes 139296 | tf_op jit(solution)/shard_map/ppermute | solution.py:38
  26.4 0.0 collective-permute-start.8
  26.4 0.0 collective-permute-done.7
  26.4 1.4 %collective-permute-done.8 = bf16[32,2176]{1,0:T(8,128)(2,1)S(1)} collective-permute-done((bf16[32,2176]{1,0:T(8,128)(2,1)S(1)}, bf16[32,2176]{1,0:T(8,128)(2,1)S(1)}, u32[]{:S(2)}, u32[]{:S(2)}) %collective-permute-start.8) | collective-permute-done | bytes 139296 | tf_op jit(solution)/shard_map/ppermute | solution.py:38
  27.8 1.5 %ffn.1 = (f32[32,2048]{1,0:T(8,128)S(1)}, f32[32,2048]{1,0:T(8,128)S(1)}, bf16[32,2048]{1,0:T(8,128)(2,1)S(1)}, bf16[32,2048]{1,0:T(8,128)(2,1)S(1)}) custom-call(bf16[128,2176]{1,0:T(8,128)(2,1)S(1)} %pad_maximum_fusion.rows_ref, bf16[1,2048,512]{2,1,0:T(8,128)(2,1)S(1)} %get-tuple-element.40.gate_ref, bf16[1,2048,512]{2,1,0:T(8,128)(2,1)S(1)} %get-tuple-element.41.up_ref, ...), custom_call_target="tpu_custom_call" | custom-call | tf_op jit(solution)/shard_map/ffn/pallas_call | solution.py:358
  29.3 0.2 collective-permute-start.9
  29.5 0.4 collective-permute-start.11
  29.9 0.8 %collective-permute-done.9.received_ref = bf16[32,2048]{1,0:T(8,128)(2,1)S(1)} collective-permute-done((bf16[32,2048]{1,0:T(8,128)(2,1)S(1)}, bf16[32,2048]{1,0:T(8,128)(2,1)S(1)}, u32[]{:S(2)}, u32[]{:S(2)}) %collective-permute-start.9) | collective-permute-done | bytes 131104 | tf_op jit(solution)/shard_map/ppermute | solution.py:38
  30.8 0.6 %collective-permute-start.10 = (bf16[16,2048]{1,0:T(8,128)(2,1)S(1)}, bf16[16,2048]{1,0:T(8,128)(2,1)S(1)}, u32[]{:S(2)}, u32[]{:S(2)}) collective-permute-start(bf16[16,2048]{1,0:T(8,128)(2,1)S(1)} %get-tuple-element.48), channel_id=1, source_target_pairs={{0,2},{1,3},{2,0},{3,1},{4,6},{5,7},{6,4},{7,5},{8,10},{9,11},{10,... | collective-permute-start | bytes 196616 | tf_op jit(solution)/shard_map/ppermute | solution.py:48
  31.4 0.0 collective-permute-done.11.received_ref
  31.4 1.6 %collective-permute-start.12 = (bf16[16,2048]{1,0:T(8,128)(2,1)S(1)}, bf16[16,2048]{1,0:T(8,128)(2,1)S(1)}, u32[]{:S(2)}, u32[]{:S(2)}) collective-permute-start(bf16[16,2048]{1,0:T(8,128)(2,1)S(1)} %get-tuple-element.51), channel_id=1, source_target_pairs={{0,4},{1,5},{2,6},{3,7},{4,0},{5,1},{6,2},{7,3},{8,12},{9,13},{10,... | collective-permute-start | bytes 196616 | tf_op jit(solution)/shard_map/ppermute | solution.py:48
  33.0 1.5 %collective-permute-start.13 = (bf16[16,2048]{1,0:T(8,128)(2,1)S(1)}, bf16[16,2048]{1,0:T(8,128)(2,1)S(1)}, u32[]{:S(2)}, u32[]{:S(2)}) collective-permute-start(bf16[16,2048]{1,0:T(8,128)(2,1)S(1)} %get-tuple-element.52), channel_id=1, source_target_pairs={{0,6},{1,7},{2,4},{3,5},{4,2},{5,3},{6,0},{7,1},{8,14},{9,15},{10,... | collective-permute-start | bytes 196616 | tf_op jit(solution)/shard_map/ppermute | solution.py:48
  34.5 0.7 %collective-permute-done.10 = bf16[16,2048]{1,0:T(8,128)(2,1)S(1)} collective-permute-done((bf16[16,2048]{1,0:T(8,128)(2,1)S(1)}, bf16[16,2048]{1,0:T(8,128)(2,1)S(1)}, u32[]{:S(2)}, u32[]{:S(2)}) %collective-permute-start.10) | collective-permute-done | bytes 65568 | tf_op jit(solution)/shard_map/ppermute | solution.py:48
  35.1 0.6 %collective-permute-done.12 = bf16[16,2048]{1,0:T(8,128)(2,1)S(1)} collective-permute-done((bf16[16,2048]{1,0:T(8,128)(2,1)S(1)}, bf16[16,2048]{1,0:T(8,128)(2,1)S(1)}, u32[]{:S(2)}, u32[]{:S(2)}) %collective-permute-start.12) | collective-permute-done | bytes 65568 | tf_op jit(solution)/shard_map/ppermute | solution.py:48
  35.7 2.4 %collective-permute-done.13 = bf16[16,2048]{1,0:T(8,128)(2,1)S(1)} collective-permute-done((bf16[16,2048]{1,0:T(8,128)(2,1)S(1)}, bf16[16,2048]{1,0:T(8,128)(2,1)S(1)}, u32[]{:S(2)}, u32[]{:S(2)}) %collective-permute-start.13) | collective-permute-done | bytes 65568 | tf_op jit(solution)/shard_map/ppermute | solution.py:48
  38.2 0.6 %collective-permute-start.14 = (bf16[1,4,2048]{2,1,0:T(4,128)(2,1)S(1)}, bf16[1,4,2048]{2,1,0:T(4,128)(2,1)S(1)}, u32[]{:S(2)}, u32[]{:S(2)}) collective-permute-start(bf16[1,4,2048]{2,1,0:T(4,128)(2,1)S(1)} %get-tuple-element.55), channel_id=1, source_target_pairs={{0,8},{4,12},{8,0},{12,4},{16,24},{20,28},{24,16},{28,20},{1,9},{5... | collective-permute-start | bytes 49160 | tf_op jit(solution)/shard_map/ppermute | solution.py:38
  38.8 3.0 %collective-permute-start.16 = (bf16[1,4,2048]{2,1,0:T(4,128)(2,1)S(1)}, bf16[1,4,2048]{2,1,0:T(4,128)(2,1)S(1)}, u32[]{:S(2)}, u32[]{:S(2)}) collective-permute-start(bf16[1,4,2048]{2,1,0:T(4,128)(2,1)S(1)} %get-tuple-element.56), channel_id=1, source_target_pairs={{0,24},{4,28},{8,16},{12,20},{16,8},{20,12},{24,0},{28,4},{1,25},{... | collective-permute-start | bytes 49160 | tf_op jit(solution)/shard_map/ppermute | solution.py:38
  41.8 0.0 collective-permute-start.15
  41.8 0.3 collective-permute-done.14
  42.0 2.3 %collective-permute-done.16 = bf16[1,4,2048]{2,1,0:T(4,128)(2,1)S(1)} collective-permute-done((bf16[1,4,2048]{2,1,0:T(4,128)(2,1)S(1)}, bf16[1,4,2048]{2,1,0:T(4,128)(2,1)S(1)}, u32[]{:S(2)}, u32[]{:S(2)}) %collective-permute-start.16) | collective-permute-done | bytes 16416 | tf_op jit(solution)/shard_map/ppermute | solution.py:38
  44.3 2.2 %collective-permute-done.15 = bf16[1,4,2048]{2,1,0:T(4,128)(2,1)S(1)} collective-permute-done((bf16[1,4,2048]{2,1,0:T(4,128)(2,1)S(1)}, bf16[1,4,2048]{2,1,0:T(4,128)(2,1)S(1)}, u32[]{:S(2)}, u32[]{:S(2)}) %collective-permute-start.15) | collective-permute-done | bytes 16416 | tf_op jit(solution)/shard_map/ppermute | solution.py:38
  46.5 0.6 %fusion.3 = bf16[4,2048]{1,0:T(4,128)(2,1)} fusion(f32[16,2048]{1,0:T(8,128)S(1)} %get-tuple-element.54, bf16[1,4,2048]{2,1,0:T(4,128)(2,1)S(1)} %collective-permute-done.16, bf16[1,4,2048]{2,1,0:T(4,128)(2,1)S(1)} %collective-permute-done.15, bf16[1,4,2048]{2,1,0:T(4,128)(2,1)S(1)} %collective-permute-done.14, f32[8,2048]{1,0:T(8,128)S(1)} %get-tuple-element.32), kind=kLoop, calls=%fused_computation.7 | loop fusion | flops 65536 | bytes 131072 | tf_op jit(solution)/shard_map/convert_element_type | solution.py:539
  (13 shorter events, 0.2 us)
Async XLA Ops:
  0.0 8.7 %copy-start.2 = (f32[16,4]{0,1:T(4,128)S(1)}, f32[16,4]{0,1:T(4,128)}, u32[]{:S(2)}) copy-start(f32[16,4]{0,1:T(4,128)} %param.34) | copy-start | bytes 772
  0.0 8.7 %copy-start.3 = (s32[16,4]{0,1:T(4,128)S(1)}, s32[16,4]{0,1:T(4,128)}, u32[]{:S(2)}) copy-start(s32[16,4]{0,1:T(4,128)} %param.33) | copy-start | bytes 772
  0.0 12.5 %copy-start = (f32[2048]{0:T(1024)S(1)}, f32[2048]{0:T(1024)}, u32[]{:S(2)}) copy-start(f32[2048]{0:T(1024)} %param.32) | copy-start | bytes 24580
  0.0 12.5 %copy-start.1 = (f32[2048]{0:T(1024)S(1)}, f32[2048]{0:T(1024)}, u32[]{:S(2)}) copy-start(f32[2048]{0:T(1024)} %param.41) | copy-start | bytes 24580
  5.4 7.1 %collective-permute-start.2 = (bf16[8,2048]{1,0:T(8,128)(2,1)S(1)}, bf16[8,2048]{1,0:T(8,128)(2,1)S(1)}, u32[]{:S(2)}, u32[]{:S(2)}) collective-permute-start(bf16[8,2048]{1,0:T(8,128)(2,1)S(1)} %get-tuple-element.30), channel_id=1, source_target_pairs={{0,3},{1,2},{2,1},{3,0},{4,7},{5,6},{6,5},{7,4},{8,11},{9,10},{10,... | collective-permute-start | bytes 98312 | tf_op jit(solution)/shard_map/ppermute | solution.py:38
  7.9 4.6 %collective-permute-start = (bf16[8,2048]{1,0:T(8,128)(2,1)S(1)}, bf16[8,2048]{1,0:T(8,128)(2,1)S(1)}, u32[]{:S(2)}, u32[]{:S(2)}) collective-permute-start(bf16[8,2048]{1,0:T(8,128)(2,1)S(1)} %get-tuple-element.30), channel_id=1, source_target_pairs={{0,1},{1,0},{2,3},{3,2},{4,5},{5,4},{6,7},{7,6},{8,9},{9,8},{10,11... | collective-permute-start | bytes 98312 | tf_op jit(solution)/shard_map/ppermute | solution.py:38
  8.6 3.9 %collective-permute-start.1 = (bf16[8,2048]{1,0:T(8,128)(2,1)S(1)}, bf16[8,2048]{1,0:T(8,128)(2,1)S(1)}, u32[]{:S(2)}, u32[]{:S(2)}) collective-permute-start(bf16[8,2048]{1,0:T(8,128)(2,1)S(1)} %get-tuple-element.29.refs_0_), channel_id=1, source_target_pairs={{0,2},{1,3},{2,0},{3,1},{4,6},{5,7},{6,4},{7,5},{8,10},{9,11},{10,... | collective-permute-start | bytes 98312 | tf_op jit(solution)/shard_map/ppermute | solution.py:38
  12.8 7.7 %collective-permute-start.5 = (bf16[8,2176]{1,0:T(8,128)(2,1)S(1)}, bf16[8,2176]{1,0:T(8,128)(2,1)S(1)}, u32[]{:S(2)}, u32[]{:S(2)}) collective-permute-start(bf16[8,2176]{1,0:T(8,128)(2,1)S(1)} %get-tuple-element.33.after_ref), channel_id=1, source_target_pairs={{0,24},{4,28},{8,16},{12,20},{16,8},{20,12},{24,0},{28,4},{1,25},{... | collective-permute-start | bytes 104456 | tf_op jit(solution)/shard_map/ppermute | solution.py:38
  16.4 4.8 %collective-permute-start.4 = (bf16[8,2176]{1,0:T(8,128)(2,1)S(1)}, bf16[8,2176]{1,0:T(8,128)(2,1)S(1)}, u32[]{:S(2)}, u32[]{:S(2)}) collective-permute-start(bf16[8,2176]{1,0:T(8,128)(2,1)S(1)} %get-tuple-element.33.after_ref), channel_id=1, source_target_pairs={{0,16},{4,20},{8,24},{12,28},{16,0},{20,4},{24,8},{28,12},{1,17},{... | collective-permute-start | bytes 104456 | tf_op jit(solution)/shard_map/ppermute | solution.py:38
  16.4 4.8 %collective-permute-start.3 = (bf16[8,2176]{1,0:T(8,128)(2,1)S(1)}, bf16[8,2176]{1,0:T(8,128)(2,1)S(1)}, u32[]{:S(2)}, u32[]{:S(2)}) collective-permute-start(bf16[8,2176]{1,0:T(8,128)(2,1)S(1)} %get-tuple-element.33.after_ref), channel_id=1, source_target_pairs={{0,8},{4,12},{8,0},{12,4},{16,24},{20,28},{24,16},{28,20},{1,9},{5... | collective-permute-start | bytes 104456 | tf_op jit(solution)/shard_map/ppermute | solution.py:38
  21.3 5.1 %collective-permute-start.6 = (bf16[32,2176]{1,0:T(8,128)(2,1)S(1)}, bf16[32,2176]{1,0:T(8,128)(2,1)S(1)}, u32[]{:S(2)}, u32[]{:S(2)}) collective-permute-start(bf16[32,2176]{1,0:T(8,128)(2,1)S(1)} %pad_maximum_fusion.1), channel_id=1, source_target_pairs={{0,4},{4,0},{8,12},{12,8},{16,20},{20,16},{24,28},{28,24},{1,5},{5... | collective-permute-start | bytes 417800 | tf_op jit(solution)/shard_map/ppermute | solution.py:38
  22.8 3.6 %collective-permute-start.7 = (bf16[32,2176]{1,0:T(8,128)(2,1)S(1)}, bf16[32,2176]{1,0:T(8,128)(2,1)S(1)}, u32[]{:S(2)}, u32[]{:S(2)}) collective-permute-start(bf16[32,2176]{1,0:T(8,128)(2,1)S(1)} %pad_maximum_fusion.1), channel_id=1, source_target_pairs={{0,1},{1,0},{2,3},{3,2},{4,5},{5,4},{6,7},{7,6},{8,9},{9,8},{10,11... | collective-permute-start | bytes 417800 | tf_op jit(solution)/shard_map/ppermute | solution.py:38
  26.4 1.4 %collective-permute-start.8 = (bf16[32,2176]{1,0:T(8,128)(2,1)S(1)}, bf16[32,2176]{1,0:T(8,128)(2,1)S(1)}, u32[]{:S(2)}, u32[]{:S(2)}) collective-permute-start(bf16[32,2176]{1,0:T(8,128)(2,1)S(1)} %collective-permute-done.6), channel_id=1, source_target_pairs={{0,1},{1,0},{2,3},{3,2},{4,5},{5,4},{6,7},{7,6},{8,9},{9,8},{10,11... | collective-permute-start | bytes 417800 | tf_op jit(solution)/shard_map/ppermute | solution.py:38
  29.3 1.4 %collective-permute-start.9 = (bf16[32,2048]{1,0:T(8,128)(2,1)S(1)}, bf16[32,2048]{1,0:T(8,128)(2,1)S(1)}, u32[]{:S(2)}, u32[]{:S(2)}) collective-permute-start(bf16[32,2048]{1,0:T(8,128)(2,1)S(1)} %get-tuple-element.46), channel_id=1, source_target_pairs={{0,1},{1,0},{2,3},{3,2},{4,5},{5,4},{6,7},{7,6},{8,9},{9,8},{10,11... | collective-permute-start | bytes 393224 | tf_op jit(solution)/shard_map/ppermute | solution.py:38
  29.5 1.8 %collective-permute-start.11 = (bf16[32,2048]{1,0:T(8,128)(2,1)S(1)}, bf16[32,2048]{1,0:T(8,128)(2,1)S(1)}, u32[]{:S(2)}, u32[]{:S(2)}) collective-permute-start(bf16[32,2048]{1,0:T(8,128)(2,1)S(1)} %get-tuple-element.50), channel_id=1, source_target_pairs={{0,1},{1,0},{2,3},{3,2},{4,5},{5,4},{6,7},{7,6},{8,9},{9,8},{10,11... | collective-permute-start | bytes 393224 | tf_op jit(solution)/shard_map/ppermute | solution.py:38
  30.8 4.3 %collective-permute-start.10 = (bf16[16,2048]{1,0:T(8,128)(2,1)S(1)}, bf16[16,2048]{1,0:T(8,128)(2,1)S(1)}, u32[]{:S(2)}, u32[]{:S(2)}) collective-permute-start(bf16[16,2048]{1,0:T(8,128)(2,1)S(1)} %get-tuple-element.48), channel_id=1, source_target_pairs={{0,2},{1,3},{2,0},{3,1},{4,6},{5,7},{6,4},{7,5},{8,10},{9,11},{10,... | collective-permute-start | bytes 196616 | tf_op jit(solution)/shard_map/ppermute | solution.py:48
  31.4 4.3 %collective-permute-start.12 = (bf16[16,2048]{1,0:T(8,128)(2,1)S(1)}, bf16[16,2048]{1,0:T(8,128)(2,1)S(1)}, u32[]{:S(2)}, u32[]{:S(2)}) collective-permute-start(bf16[16,2048]{1,0:T(8,128)(2,1)S(1)} %get-tuple-element.51), channel_id=1, source_target_pairs={{0,4},{1,5},{2,6},{3,7},{4,0},{5,1},{6,2},{7,3},{8,12},{9,13},{10,... | collective-permute-start | bytes 196616 | tf_op jit(solution)/shard_map/ppermute | solution.py:48
  33.0 5.2 %collective-permute-start.13 = (bf16[16,2048]{1,0:T(8,128)(2,1)S(1)}, bf16[16,2048]{1,0:T(8,128)(2,1)S(1)}, u32[]{:S(2)}, u32[]{:S(2)}) collective-permute-start(bf16[16,2048]{1,0:T(8,128)(2,1)S(1)} %get-tuple-element.52), channel_id=1, source_target_pairs={{0,6},{1,7},{2,4},{3,5},{4,2},{5,3},{6,0},{7,1},{8,14},{9,15},{10,... | collective-permute-start | bytes 196616 | tf_op jit(solution)/shard_map/ppermute | solution.py:48
  38.2 3.8 %collective-permute-start.14 = (bf16[1,4,2048]{2,1,0:T(4,128)(2,1)S(1)}, bf16[1,4,2048]{2,1,0:T(4,128)(2,1)S(1)}, u32[]{:S(2)}, u32[]{:S(2)}) collective-permute-start(bf16[1,4,2048]{2,1,0:T(4,128)(2,1)S(1)} %get-tuple-element.55), channel_id=1, source_target_pairs={{0,8},{4,12},{8,0},{12,4},{16,24},{20,28},{24,16},{28,20},{1,9},{5... | collective-permute-start | bytes 49160 | tf_op jit(solution)/shard_map/ppermute | solution.py:38
  38.8 5.5 %collective-permute-start.16 = (bf16[1,4,2048]{2,1,0:T(4,128)(2,1)S(1)}, bf16[1,4,2048]{2,1,0:T(4,128)(2,1)S(1)}, u32[]{:S(2)}, u32[]{:S(2)}) collective-permute-start(bf16[1,4,2048]{2,1,0:T(4,128)(2,1)S(1)} %get-tuple-element.56), channel_id=1, source_target_pairs={{0,24},{4,28},{8,16},{12,20},{16,8},{20,12},{24,0},{28,4},{1,25},{... | collective-permute-start | bytes 49160 | tf_op jit(solution)/shard_map/ppermute | solution.py:38
  41.8 4.8 %collective-permute-start.15 = (bf16[1,4,2048]{2,1,0:T(4,128)(2,1)S(1)}, bf16[1,4,2048]{2,1,0:T(4,128)(2,1)S(1)}, u32[]{:S(2)}, u32[]{:S(2)}) collective-permute-start(bf16[1,4,2048]{2,1,0:T(4,128)(2,1)S(1)} %get-tuple-element.57), channel_id=1, source_target_pairs={{0,16},{4,20},{8,24},{12,28},{16,0},{20,4},{24,8},{28,12},{1,17},{... | collective-permute-start | bytes 49160 | tf_op jit(solution)/shard_map/ppermute | solution.py:38
